TPU v7x, 128 devices: a whole 4x4x4 slice. The times are simulated.
128 devices in a mesh: rep: 2 (over z_hi), fs: 32 (over z_lo, y, x), tp: 2 (over core).
Axes of the slice: x: 4, y: 4, z: 4 (z_hi: 2, z_lo: 2; z = z_hi * 2 + z_lo), core: 2. Of those that a mesh axis runs over, the one named last changes fastest.
Arguments:
- inputs: bfloat16 [32768, 1024], P(('rep', 'fs', 'tp')), may hold values from -6 to 6
- up_proj: bfloat16 [1024, 4096], P('fs', 'tp'), may hold values from -0.1875 to 0.1875
- down_proj: bfloat16 [4096, 1024], P('tp', 'fs'), may hold values from -0.09375 to 0.09375
- out_cotangent: bfloat16 [32768, 1024], P(('rep', 'fs', 'tp')), may hold values from -24 to 24
Outputs:
- grad_inputs: bfloat16 [32768, 1024], P(('rep', 'fs', 'tp'))
- grad_up: float32 [1024, 4096], P('fs', 'tp')
- grad_down: float32 [4096, 1024], P('tp', 'fs')
- energy_up: float32 [1024], P('fs')
- energy_down: float32 [4096], P('tp')
All inputs are finite; a program needn't handle non-finite values.
Results may differ from a plain program's by a relative error of at most 0.001.
Values may be sent and summed in bfloat16 or wider, within the bound.
A program may use at most 128 MiB of HBM per device.

v0:
```python
import jax
import jax.numpy as jnp
from jax import lax
from jax.sharding import Mesh
from jax.sharding import PartitionSpec as P

D = 1024
FF = 4096
FS = ("fs_0", "fs_1", "fs_2")
REP_FS_TP = ("rep", "fs_0", "fs_1", "fs_2", "tp")


def laid_out(tiles, dim):
    tiles = jnp.moveaxis(tiles, 0, dim)
    dims = tiles.shape
    return tiles.reshape(*dims[:dim], dims[dim] * dims[dim + 1], *dims[dim + 2 :])


def gather_packed(arrays, axis, dims):
    vector = jnp.concatenate([a.reshape(-1) for a in arrays])
    lines, at, gathered = lax.all_gather(vector, axis), 0, []
    for a, dim in zip(arrays, dims):
        tiles = lines[:, at : at + a.size].reshape(-1, *a.shape)
        gathered.append(laid_out(tiles, dim))
        at += a.size
    return tuple(gathered)


def folded(array, axis, dim, take_in, carry):
    whole = jax.tree.map(lambda part: lax.all_gather(part, axis, axis=dim, tiled=True), array)
    return take_in(carry, whole, jnp.int32(0))


def over_all(share, axis, dim, apply):
    everything = lax.all_gather(share, axis, axis=dim, tiled=True)
    return apply(everything, jnp.int32(0))


def summed_rows(product, span, axis):
    whole = product(jnp.int32(0), span * lax.axis_size(axis))
    return lax.psum_scatter(whole, axis, scatter_dimension=0, tiled=True)


def over_pieces(array, axis):
    tiles = lax.all_gather(array, axis)
    return tiles.sum(axis=0)


def one_axis_at_a_time(array, axes):
    for axis in axes:
        array = lax.psum(array, axis)
    return array


def contract(left, right, left_dim, right_dim):
    return lax.dot_general(
        left, right, (((left_dim,), (right_dim,)), ((), ())), preferred_element_type=jnp.float32
    )


def per_device(inputs, up_proj, down_proj, out_cotangent):
    factor = float(
        inputs.shape[0] * lax.axis_size("rep") * lax.axis_size(FS) * lax.axis_size("tp")
    ) ** (-0.5)
    all_inputs, all_cotangent = gather_packed((inputs, out_cotangent), "tp", (0, 0))
    hidden_cols = up_proj.shape[1]
    group_rows = all_inputs.shape[0]

    def add_rows(total, piece, start):
        columns = lax.dynamic_slice_in_dim(all_inputs, start, piece.shape[0], 1)
        return total + jnp.dot(columns, piece, preferred_element_type=jnp.float32)

    pre = folded(up_proj, FS, 0, add_rows, jnp.zeros((group_rows, hidden_cols), jnp.float32))
    active = jnp.square(jax.nn.relu(pre)).astype(jnp.bfloat16)

    def add_cols(total, piece, start):
        columns = lax.dynamic_slice_in_dim(all_cotangent, start, piece.shape[1], 1)
        return total + contract(columns, piece, 1, 1)

    back = folded(down_proj, FS, 1, add_cols, jnp.zeros((group_rows, hidden_cols), jnp.float32))
    grad_pre = (2.0 * jax.nn.relu(pre) * back).astype(jnp.bfloat16)

    def project(piece, start):
        return contract(grad_pre, piece, 1, 1)

    partial_in = over_all(up_proj, FS, 0, project)
    grad_inputs = lax.psum_scatter(partial_in, "tp", scatter_dimension=0, tiled=True)
    grad_inputs = grad_inputs.astype(jnp.bfloat16)
    shard_rows = up_proj.shape[0]

    def up_part(start, count):
        columns = lax.dynamic_slice_in_dim(all_inputs, start, count, 1)
        return contract(columns, grad_pre, 0, 0) * factor

    def down_part(start, count):
        columns = lax.dynamic_slice_in_dim(all_cotangent, start, count, 1)
        return contract(columns, active, 0, 0) * factor

    def joint_part(start, count):
        return jnp.concatenate([up_part(start, count), down_part(start, count)], axis=1)

    joint_local = summed_rows(joint_part, shard_rows, FS)
    joint_sum = over_pieces(joint_local, "rep")
    grad_up = joint_sum[:, :hidden_cols]
    down_flip = joint_sum[:, hidden_cols:]
    grad_down = jnp.transpose(down_flip)
    energy_up = over_pieces(jnp.sum(grad_up * grad_up, axis=1), "tp") / FF
    energy_down = one_axis_at_a_time(jnp.sum(grad_down * grad_down, axis=1), FS) / D
    return (grad_inputs, grad_up, grad_down, energy_up, energy_down)


def solution(mesh):
    torus = Mesh(
        mesh.devices.reshape(mesh.shape["rep"], 2, 4, 4, mesh.shape["tp"]),
        ("rep", "fs_0", "fs_1", "fs_2", "tp"),
    )
    placed = (P(REP_FS_TP, None), P(FS, "tp"), P("tp", FS), P(REP_FS_TP, None))
    return jax.shard_map(
        per_device,
        mesh=torus,
        in_specs=placed,
        out_specs=(P(REP_FS_TP, None), P(FS, "tp"), P("tp", FS), P(FS), P("tp")),
        check_vma=False,
    )
```

profile of v0, /device:TPU:1, one launch (start us, length us, event | category | flops | bytes accessed | tf_op | source)
XLA Modules:
  0.0 649.6 jit_solution(5333946201292279292)
XLA Ops:
  12.1 15.5 %all-gather.12.cloned.1.call-done = bf16[1048576]{0:T(1024)(128)(2,1)} async-done(((bf16[524288]{0:T(1024)(128)(2,1)}), bf16[1048576]{0:T(1024)(128)(2,1)}) %all-gather.12.cloned.1.call-update) | async-done | bytes 2097168 | tf_op jit(solution)/shard_map/all_gather | solution.py:21
  27.6 2.1 reshape.18
  29.8 2.3 fusion.2
  32.1 2.2 reshape_reshape.6
  35.3 130.7 %all-gather.8.cloned.1.call-done = bf16[1024,2048]{1,0:T(8,128)(2,1)} async-done(((bf16[32,2048]{1,0:T(8,128)(2,1)}), bf16[1024,2048]{1,0:T(8,128)(2,1)}) %all-gather.8.cloned.1.call-update) | async-done | bytes 4194320 | tf_op jit(solution)/shard_map/all_gather | solution.py:30
  166.0 4.5 fusion.3
  170.5 1.9 copy-done.1
  172.5 5.6 convolution_multiply_fusion
  178.1 145.9 %all-gather.10.cloned.1.call-done = bf16[2048,1024]{0,1:T(8,128)(2,1)} async-done(((bf16[2048,32]{0,1:T(8,128)(2,1)}), bf16[2048,1024]{0,1:T(8,128)(2,1)}) %all-gather.10.cloned.1.call-update) | async-done | bytes 4194320 | tf_op jit(solution)/shard_map/all_gather | solution.py:30
  324.0 5.8 multiply_convert_fusion.1
  329.9 1.3 copy-done.3
  331.2 2.4 convolution_multiply_fusion.1
  334.6 6.2 pad_maximum_fusion
  341.0 1.3 copy-done.4
  342.3 6.0 fusion.4
  348.4 210.2 %reduce-scatter.5.cloned.1.call-done = f32[32,4096]{1,0:T(8,128)} async-done(((f32[1024,4096]{1,0:T(8,128)}), f32[32,4096]{1,0:T(8,128)}) %reduce-scatter.5.cloned.1.call-update) | async-done | bytes 524304 | tf_op jit(solution)/shard_map/reduce_scatter | solution.py:41
  559.9 26.6 %reduce-scatter.3.cloned.1.call-done = f32[256,1024]{1,0:T(8,128)} async-done(((f32[512,1024]{1,0:T(8,128)}), f32[256,1024]{1,0:T(8,128)}) %reduce-scatter.3.cloned.1.call-update) | async-done | bytes 1048592 | tf_op jit(solution)/shard_map/reduce_scatter | solution.py:87
  586.5 2.1 convert_element_type.10
  588.6 25.7 %all-gather.14.cloned.1.call-done = f32[64,4096]{1,0:T(8,128)} async-done(((f32[32,4096]{1,0:T(8,128)}), f32[64,4096]{1,0:T(8,128)}) %all-gather.14.cloned.1.call-update) | async-done | bytes 1048592 | tf_op jit(solution)/shard_map/all_gather | solution.py:45
  614.3 1.3 reduce_sum.36
  617.4 3.2 all-reduce
  621.3 3.8 psum.21
  625.1 8.5 %psum.22 = f32[2048]{0:T(1024)S(1)} all-reduce(f32[2048]{0:T(1024)S(1)} %psum.21), channel_id=1, replica_groups=mesh['rep'=2,'fs_0'=2,'fs_1'=4,'fs_2'=4,'tp'=2] {'fs_1'}, use_global_device_ids=true, to_apply=%region_7.8 | all-reduce | flops 2048 | bytes 16384 | tf_op jit(solution)/shard_map/psum | solution.py:51
  633.7 8.5 %psum.23 = f32[2048]{0:T(1024)S(1)} all-reduce(f32[2048]{0:T(1024)S(1)} %psum.22), channel_id=1, replica_groups=mesh['rep'=2,'fs_0'=2,'fs_1'=4,'fs_2'=4,'tp'=2] {'fs_2'}, use_global_device_ids=true, to_apply=%region_8.9 | all-reduce | flops 2048 | bytes 16384 | tf_op jit(solution)/shard_map/psum | solution.py:51
  (32 shorter events, 10.7 us)
Async XLA Ops:
  7.2 20.5 %all-gather.12.cloned.1.call-start = ((), (), s32[]{:S(2)}) async-start(), calls=%async_computation.6 | async-start | bytes 3145728 | tf_op jit(solution)/shard_map/all_gather | solution.py:21
  10.6 155.4 %all-gather.8.cloned.1.call-start = ((), (), s32[]{:S(2)}) async-start(), calls=%async_computation.2 | async-start | bytes 4325376 | tf_op jit(solution)/shard_map/all_gather | solution.py:30
  11.3 312.7 %all-gather.10.cloned.1.call-start = ((), (), s32[]{:S(2)}) async-start(), calls=%async_computation.3 | async-start | bytes 4325376 | tf_op jit(solution)/shard_map/all_gather | solution.py:30
  12.1 546.6 %reduce-scatter.5.cloned.1.call-start = ((), (), s32[]{:S(2)}) async-start(), calls=%async_computation.5 | async-start | bytes 17301504 | tf_op jit(solution)/shard_map/reduce_scatter | solution.py:41
  170.5 2.0 copy-start.1
  329.9 1.3 copy-start.3
  331.2 3.4 copy-start
  340.8 1.6 copy-start.4
  340.8 217.9 %copy-start.2 = (u32[128]{0:T(128)S(1)}, u32[128]{0:T(128)}, u32[]{:S(2)}) copy-start(u32[128]{0:T(128)} %constant.17) | copy-start | bytes 1540
  340.8 245.7 %reduce-scatter.3.cloned.1.call-start = ((), (), s32[]{:S(2)}) async-start(), calls=%async_computation.4 | async-start | bytes 3145728 | tf_op jit(solution)/shard_map/reduce_scatter | solution.py:87
  348.4 266.0 %all-gather.14.cloned.1.call-start = ((), (), s32[]{:S(2)}) async-start(), calls=%async_computation.7 | async-start | bytes 1572864 | tf_op jit(solution)/shard_map/all_gather | solution.py:45
Sparse Core Ops, SparseCore 0:
  10.7 16.9 all-gather.11
  29.3 136.6 all-gather.7
  167.7 156.3 all-gather.9
  340.9 217.6 reduce-scatter.4
  560.8 25.6 reduce-scatter.2
  588.0 26.2 all-gather.13
where the time goes:
time: 654 us; the launch traced here: 650 us
  waiting for transfers between devices  556 us (85%)
  matrix products  24.3 us (4%)
  blocking collectives  24.1 us (4%)
  local copies, waits for them, and re-layouts  16.4 us (3%)
  between operations  14.9 us (2%)
  other arithmetic  13.4 us (2%)
    all_gather x2, waiting for transfers between devices, folded(): lax.all_gather(part, axis, axis=dim, tiled=True)  277 us
    reduce_scatter x1, waiting for transfers between devices, summed_rows(): return lax.psum_scatter(whole, axis, scatter_dimension=0, tiled=True)  210 us
    reduce_scatter x1, waiting for transfers between devices, per_device(): lax.psum_scatter(partial_in, 'tp', scatter_dimension=0, tiled=True)  26.6 us
    all_gather x1, waiting for transfers between devices, over_pieces(): tiles = lax.all_gather(array, axis)  25.7 us
    psum x3, blocking collectives, one_axis_at_a_time(): array = lax.psum(array, axis)  20.9 us
    dot_general x4, matrix products, contract(): lax.dot_general(left, right, (((left_dim,), (right_dim,)), ((), ())), pre...  19.8 us
    all_gather x1, waiting for transfers between devices, gather_packed(): lines, at, gathered = (lax.all_gather(vector, axis), 0, [])  15.5 us
  transfers between devices with their start and end apart: 6, of which 6 were waited for; matrix products, arithmetic and copies ran while one was open for 4% of the time, Pallas kernels for 0%

commit v1 on v0

v1 whole, which is shorter than its diff:
```python
import jax
import jax.numpy as jnp
from jax import lax
from jax.experimental import pallas as pl
from jax.experimental.pallas import tpu as pltpu
from jax.sharding import Mesh
from jax.sharding import PartitionSpec as P

FS = ("fs_0", "fs_1", "fs_2")
REP_FS_TP = ("rep", "fs_0", "fs_1", "fs_2", "tp")
MESH = pl.DeviceIdType.MESH
BF = jnp.bfloat16
F32 = jnp.float32
RIGHT, LEFT = 0, 1
UP, DN = 0, 1
COPIES = 240


def make_kernel(tokens, width, cols, ff, factor):
    lanes = [pl.ds(c * 128, 128) for c in range(cols // 128)]

    def kernel(
        x_ref, up_ref, dn_ref, cot_ref,
        gin_ref, gup_ref, gdn_ref, eup_ref, edn_ref,
        X, C, XT, CT, W, RP, ACT, GP, G,
        s1s, s1r, c1s, c1r, R1, s2s, s2r, c2s, c2r, R2, s3s, s3r, c3s, c3r,
        PART, DR, ZR, EX, EY, EZ, EU,
        ssem, rsem, lsem,
    ):
        r = lax.axis_index("rep")
        j = lax.axis_index("fs_0")
        y = lax.axis_index("fs_1")
        x = lax.axis_index("fs_2")
        t = lax.axis_index("tp")

        def at(pos, d):
            return lax.rem(pos + d, 4)

        def xdev(d):
            return {"fs_2": at(x, d)}

        def ydev(d):
            return {"fs_1": at(y, d)}

        zpeer = {"fs_0": 1 - j}
        rpeer = {"rep": 1 - r}
        rzpeer = {"rep": 1 - r, "fs_0": 1 - j}
        tpeer = {"tp": 1 - t}

        barrier = pltpu.get_barrier_semaphore()
        peers = [xdev(1), xdev(2), xdev(3), ydev(1), ydev(2), ydev(3), zpeer, rpeer, rzpeer, tpeer]
        for dev in peers:
            pl.semaphore_signal(barrier, inc=1, device_id=dev, device_id_type=MESH)
        pl.semaphore_wait(barrier, len(peers))

        copies = {}

        def send(key, src, dst, dev):
            n = len(copies)
            c = pltpu.make_async_remote_copy(
                src_ref=src, dst_ref=dst, send_sem=ssem.at[n], recv_sem=rsem.at[n],
                device_id=dev, device_id_type=MESH,
            )
            c.start()
            copies[key] = c

        def recv(key):
            copies[key].wait_recv()

        half = tokens // 2
        own = pl.ds(pl.multiple_of(j * cols, cols), cols)
        other = pl.ds(pl.multiple_of((1 - j) * cols, cols), cols)
        w_refs = (up_ref, dn_ref)

        for w in (UP, DN):
            send(("a2a", w), w_refs[w].at[:, :, other], W.at[w, j, y, x], zpeer)
        locals_ = [
            pltpu.make_async_copy(up_ref.at[:, :, own], W.at[UP, j, y, x], lsem.at[0]),
            pltpu.make_async_copy(dn_ref.at[:, :, own], W.at[DN, j, y, x], lsem.at[1]),
            pltpu.make_async_copy(x_ref, X.at[0], lsem.at[2]),
            pltpu.make_async_copy(cot_ref, C.at[0], lsem.at[3]),
        ]
        for c in locals_:
            c.start()

        def blk(ref, w, h, a, b):
            z = j if h == 0 else 1 - j
            return ref.at[w, z, b, a] if h == 0 else ref.at[w, z, a, b]

        def axes(h):
            return (x, y, xdev, ydev) if h == 0 else (y, x, ydev, xdev)

        def init(w, h):
            a, b, adev, bdev = axes(h)
            src = w_refs[w].at[:, :, own] if h == 0 else blk(W, w, h, a, b)
            dst = blk(W, w, h, a, b)
            send((1, w, h, 0), src, dst, adev(1))
            send((1, w, h, 1), src, dst, adev(3))
            send((2, w, h, 0, 0), src, dst, bdev(1))
            send((2, w, h, 0, 1), src, dst, bdev(3))

        def spread(w, h, s, a2):
            _, b, _, bdev = axes(h)
            ref = blk(W, w, h, a2, b)
            send((2, w, h, s, 0), ref, ref, bdev(1))
            send((2, w, h, s, 1), ref, ref, bdev(3))

        def step1(w, h):
            a, b, adev, _ = axes(h)
            recv((1, w, h, 0))
            ref = blk(W, w, h, at(a, 3), b).at[0]
            send((1, w, h, 2), ref, ref, adev(1))
            spread(w, h, 1, at(a, 3))
            recv((1, w, h, 1))
            ref = blk(W, w, h, at(a, 1), b).at[1]
            send((1, w, h, 3), ref, ref, adev(3))
            spread(w, h, 2, at(a, 1))

        def step2(w, h):
            a = axes(h)[0]
            recv((1, w, h, 2))
            recv((1, w, h, 3))
            spread(w, h, 3, at(a, 2))

        def fwd(w, h, s):
            a, b, _, bdev = axes(h)
            a2 = at(a, (0, 3, 1, 2)[s])
            recv((2, w, h, s, 0))
            ref = blk(W, w, h, a2, at(b, 3)).at[0]
            send((2, w, h, s, 2), ref, ref, bdev(1))
            recv((2, w, h, s, 1))
            ref = blk(W, w, h, a2, at(b, 1)).at[1]
            send((2, w, h, s, 3), ref, ref, bdev(3))

        def fin(w):
            for h in (0, 1):
                for s in range(4):
                    recv((2, w, h, s, 2))
                    recv((2, w, h, s, 3))

        def pass_on(name, buf, i):
            recv((name, "z", i))
            part = buf.at[2, pl.ds(i * half, half)]
            send((name, "zt", i), part, buf.at[3, pl.ds(i * half, half)], tpeer)

        def arrived(name, slot):
            if slot == 1:
                recv((name, "t"))
            if slot == 3:
                recv((name, "zt", 0))
                recv((name, "zt", 1))

        def turn(src, dst, slot):
            v = src[slot].T
            dst[:, :, :, :, slot * tokens:(slot + 1) * tokens] = v.reshape(2, 4, 4, width // 32, tokens)

        tile = min(512, cols)

        def weight(w, n):
            return W[w, :, :, :, :, :, pl.ds(pl.multiple_of(n * tile, tile), tile)].reshape(width, tile)

        def project(slot):
            def body(n, _):
                col = pl.ds(pl.multiple_of(n * tile, tile), tile)
                pre = jnp.maximum(jnp.dot(X[slot], weight(UP, n), preferred_element_type=F32), 0.0)
                RP[slot, :, col] = pre
                ACT[slot, :, col] = (pre * pre).astype(BF)
                return 0
            lax.fori_loop(0, cols // tile, body, 0)

        def pull_back(slot):
            def body(n, _):
                col = pl.ds(pl.multiple_of(n * tile, tile), tile)
                back = jnp.dot(C[slot], weight(DN, n), preferred_element_type=F32)
                GP[slot, :, col] = (2.0 * RP[slot, :, col] * back).astype(BF)
                return 0
            lax.fori_loop(0, cols // tile, body, 0)

        init(UP, 0)
        init(DN, 0)
        for name, src, dst in (("x", x_ref, X), ("c", cot_ref, C)):
            for i in (0, 1):
                rows = pl.ds(i * half, half)
                send((name, "z", i), src.at[rows], dst.at[2, rows], zpeer)
            send((name, "t"), src, dst.at[1], tpeer)
        recv(("a2a", UP))
        init(UP, 1)
        step1(UP, 0)
        fwd(UP, 0, 0)
        recv(("a2a", DN))
        init(DN, 1)
        step1(UP, 1)
        fwd(UP, 1, 0)
        step2(UP, 0)
        fwd(UP, 0, 1)
        fwd(UP, 0, 2)
        step1(DN, 0)
        fwd(DN, 0, 0)
        step2(UP, 1)
        fwd(UP, 1, 1)
        fwd(UP, 1, 2)
        step1(DN, 1)
        fwd(DN, 1, 0)
        for c in locals_:
            c.wait()
        turn(X, XT, 0)
        fwd(UP, 0, 3)
        fwd(UP, 1, 3)
        arrived("x", 1)
        turn(X, XT, 1)
        step2(DN, 0)
        fwd(DN, 0, 1)
        fwd(DN, 0, 2)
        pass_on("x", X, 0)
        turn(C, CT, 0)
        step2(DN, 1)
        fwd(DN, 1, 1)
        fwd(DN, 1, 2)
        arrived("c", 1)
        turn(C, CT, 1)
        pass_on("x", X, 1)
        fin(UP)
        project(0)
        project(1)
        turn(X, XT, 2)
        project(2)
        fwd(DN, 0, 3)
        fwd(DN, 1, 3)
        arrived("x", 3)
        turn(X, XT, 3)
        project(3)
        pass_on("c", C, 0)
        fin(DN)
        pull_back(0)
        pull_back(1)
        pass_on("c", C, 1)
        turn(C, CT, 2)
        arrived("c", 3)
        turn(C, CT, 3)

        lhs_of = (XT, CT)
        rhs_of = (GP, ACT)

        def gblk(w, h, a, b):
            z = j if h == 0 else 1 - j
            return G.at[w, z, a, b] if h == 0 else G.at[w, z, b, a]

        def raxes(h):
            return (y, x, ydev, xdev) if h == 0 else (x, y, xdev, ydev)

        def multiply(w, h, a1, a2):
            z = j if h == 0 else 1 - j
            lhs = lhs_of[w]
            if h == 0:
                l1, l2 = lhs[z, a1], lhs[z, a2]
            else:
                l1, l2 = lhs[z, :, a1], lhs[z, :, a2]
            rows = 4 * (width // 32)
            left = jnp.concatenate([l1.reshape(rows, -1), l2.reshape(rows, -1)], axis=0)

            def body(n, _):
                col = pl.ds(pl.multiple_of(n * tile, tile), tile)
                right = rhs_of[w][:, :, col].reshape(4 * tokens, tile)
                out = jnp.dot(left, right, preferred_element_type=F32)
                for k, a in enumerate((a1, a2)):
                    part = out[k * rows:(k + 1) * rows].reshape(4, width // 32, tile)
                    if h == 0:
                        G[w, z, a, :, :, col] = part
                    else:
                        G[w, z, :, a, :, col] = part
                return 0
            lax.fori_loop(0, cols // tile, body, 0)

        def encode(srcs, dst, scale):
            top = None
            for src in srcs:
                for c in lanes:
                    m = jnp.max(jnp.abs(src[:, c]).reshape(-1, 8, 128), axis=0)
                    top = m if top is None else jnp.maximum(top, m)
            top = jnp.maximum(top, 2e-34)
            scale[...] = top
            inv = 32768.0 / top
            for i, src in enumerate(srcs):
                for c in lanes:
                    v = src[:, c]
                    v3 = v.reshape(-1, 8, 128) * inv
                    for _ in range(3):
                        v3 = v3 * jnp.abs(v3)
                    dst[i, :, c] = v3.reshape(v.shape).astype(BF)

        def decode(buf, scale, i, c):
            v = buf[i, :, c].astype(F32)
            m = jnp.exp2(jnp.log2(jnp.abs(v)) * 0.125)
            m = jnp.where(v < 0, -m, m).reshape(-1, 8, 128) * (scale[...] * (1.0 / 32768.0))
            return m.reshape(v.shape)

        class Ring:
            def __init__(self, stage, w, h, pos, dev, parts, bufs):
                self.k = (stage, w, h)
                self.pos, self.dev, self.parts = pos, dev, parts
                self.sb, self.rb, self.sc, self.rc = (b.at[2 * w + h] for b in bufs)

            def post(self, i, srcs, d):
                encode(srcs, self.sb.at[i], self.sc.at[i])
                send(self.k + (i, "s"), self.sc.at[i], self.rc.at[i], self.dev(d))
                send(self.k + (i, "v"), self.sb.at[i], self.rb.at[i], self.dev(d))

            def take(self, i, refs):
                recv(self.k + (i, "s"))
                recv(self.k + (i, "v"))
                for n, ref in enumerate(refs):
                    for c in lanes:
                        ref[:, c] = ref[:, c] + decode(self.rb.at[i], self.rc.at[i], n, c)

            def far(self):
                self.post(0, self.parts(at(self.pos, 2), 0), 1)
                self.post(1, self.parts(at(self.pos, 2), 1), 3)

            def near_right(self):
                self.post(2, self.parts(at(self.pos, 1), 1), 1)

            def near_left(self):
                self.post(3, self.parts(at(self.pos, 3), 0), 3)

            def relay(self):
                p = self.parts(at(self.pos, 1), 0)
                self.take(0, p)
                self.post(4, p, 1)
                p = self.parts(at(self.pos, 3), 1)
                self.take(1, p)
                self.post(5, p, 3)

            def near_in(self):
                self.take(3, self.parts(self.pos, 0))
                self.take(2, self.parts(self.pos, 1))

            def last_in(self):
                self.take(4, self.parts(self.pos, 0))
                self.take(5, self.parts(self.pos, 1))

        def ring1(w, h):
            a, b, adev, bdev = raxes(h)
            return Ring(1, w, h, a, adev,
                        lambda place, side: [gblk(w, h, place, 2 * side + i) for i in (0, 1)],
                        (s1s, s1r, c1s, c1r))

        hr = width // 64

        def ring2(w, h):
            a, b, adev, bdev = raxes(h)
            return Ring(2, w, h, b, bdev,
                        lambda place, side: [gblk(w, h, a, place).at[pl.ds(side * hr, hr)]],
                        (s2s, s2r, c2s, c2r))

        first = {(w, h): ring1(w, h) for w in (UP, DN) for h in (0, 1)}
        second = {(w, h): ring2(w, h) for w in (UP, DN) for h in (0, 1)}

        def launch(w):
            for h in (0, 1):
                a = raxes(h)[0]
                multiply(w, h, at(a, 2), at(a, 1))
                first[w, h].far()
                first[w, h].near_right()
            for h in (0, 1):
                a = raxes(h)[0]
                multiply(w, h, at(a, 3), a)
                first[w, h].near_left()

        def launch2(w):
            for h in (0, 1):
                first[w, h].near_in()
            for h in (0, 1):
                first[w, h].last_in()
                second[w, h].far()
                second[w, h].near_right()
                second[w, h].near_left()

        def relay2(w):
            for h in (0, 1):
                second[w, h].relay()

        def launch3(w):
            for h in (0, 1):
                second[w, h].near_in()
                second[w, h].last_in()
                a, b, _, _ = raxes(h)
                encode([gblk(w, h, a, b)], s3s.at[w, h], c3s.at[w, h])
                peers_ = [(0, rpeer)] if h == 0 else [(1, zpeer), (2, rzpeer)]
                for i, dev in peers_:
                    send((3, w, i, "s"), c3s.at[w, h], c3r.at[w, i], dev)
                    send((3, w, i, "v"), s3s.at[w, h], s3r.at[w, i], dev)

        def finish(w, out):
            for i in range(3):
                recv((3, w, i, "s"))
                recv((3, w, i, "v"))
            for c in range(len(lanes)):
                lane = lanes[c]
                mine = decode(s3s.at[w, 0], c3s.at[w, 0], 0, lane)
                mine = mine + decode(s3r.at[w, 0], c3r.at[w, 0], 0, lane)
                out[:, pl.ds(pl.multiple_of(j * cols + c * 128, 128), 128)] = mine * factor
                theirs = decode(s3r.at[w, 1], c3r.at[w, 1], 0, lane)
                theirs = theirs + decode(s3r.at[w, 2], c3r.at[w, 2], 0, lane)
                out[:, pl.ds(pl.multiple_of((1 - j) * cols + c * 128, 128), 128)] = theirs * factor

        def input_part(slot, out):
            def body(n, _):
                w = W[UP, n // 2, pl.ds(2 * lax.rem(n, 2), 2)].reshape(width // 4, cols)
                v = lax.dot_general(GP[slot], w, (((1,), (1,)), ((), ())), preferred_element_type=F32)
                out[:, pl.ds(pl.multiple_of(n * (width // 4), width // 4), width // 4)] = v
                return 0
            lax.fori_loop(0, 4, body, 0)

        launch(DN)
        pull_back(2)
        pull_back(3)
        input_part(3, PART.at[0])
        send(("g", "t", 0), PART.at[0], DR.at[0], tpeer)
        input_part(2, PART.at[1])
        recv(("g", "t", 0))
        PART[1] = PART[1] + DR[0]
        send(("g", "z"), PART.at[1], ZR, zpeer)
        for h in (0, 1):
            first[DN, h].relay()
        launch(UP)
        input_part(1, PART.at[2])
        send(("g", "t", 1), PART.at[2], DR.at[1], tpeer)
        launch2(DN)
        for h in (0, 1):
            first[UP, h].relay()
        input_part(0, PART.at[3])
        recv(("g", "t", 1))
        relay2(DN)
        launch2(UP)
        launch3(DN)
        relay2(UP)
        finish(DN, gdn_ref)

        EX[x] = jnp.sum(gdn_ref[...] * gdn_ref[...], axis=0, keepdims=True)
        for d in (1, 2, 3):
            send(("e", "x", d), EX.at[x], EX.at[x], xdev(d))
        launch3(UP)
        for d in (1, 2, 3):
            recv(("e", "x", d))
        EY[y] = EX[0] + EX[1] + EX[2] + EX[3]
        for d in (1, 2, 3):
            send(("e", "y", d), EY.at[y], EY.at[y], ydev(d))
        recv(("g", "z"))
        gin_ref[...] = (PART[3] + DR[1] + ZR[...]).astype(BF)
        for d in (1, 2, 3):
            recv(("e", "y", d))
        EZ[0] = EY[0] + EY[1] + EY[2] + EY[3]
        send(("e", "z"), EZ.at[0], EZ.at[1], zpeer)
        finish(UP, gup_ref)
        total = None
        for c in range(2 * len(lanes)):
            v = gup_ref[:, c * 128:(c + 1) * 128]
            total = v * v if total is None else total + v * v
        EU[0] = total
        send(("e", "t"), EU.at[0], EU.at[1], tpeer)
        recv(("e", "z"))
        edn_ref[...] = (EZ[0] + EZ[1]) * (1.0 / width)
        recv(("e", "t"))
        both = jnp.sum(EU[0] + EU[1], axis=1, keepdims=True) * (1.0 / ff)
        eup_ref[...] = jnp.broadcast_to(both, eup_ref.shape)
        for c in copies.values():
            c.wait_send()

    return kernel


def per_device(inputs, up_proj, down_proj, out_cotangent):
    tokens, width = inputs.shape
    rows, hidden = up_proj.shape
    cols = hidden // 2
    ff = hidden * lax.axis_size("tp")
    all_tokens = tokens * lax.axis_size("rep") * lax.axis_size(FS) * lax.axis_size("tp")
    factor = float(all_tokens) ** (-0.5)
    up3 = up_proj.reshape(2, rows // 2, hidden)
    dn3 = down_proj.T.reshape(2, rows // 2, hidden)
    vm = pl.BlockSpec(memory_space=pltpu.VMEM)
    full = (2, 4, 4, rows)
    gin, gup, gdn, eup, edn = pl.pallas_call(
        make_kernel(tokens, width, cols, ff, factor),
        out_shape=(
            jax.ShapeDtypeStruct((tokens, width), BF),
            jax.ShapeDtypeStruct((rows, hidden), F32),
            jax.ShapeDtypeStruct((rows, hidden), F32),
            jax.ShapeDtypeStruct((rows, 128), F32),
            jax.ShapeDtypeStruct((1, hidden), F32),
        ),
        in_specs=[vm] * 4,
        out_specs=(vm,) * 5,
        scratch_shapes=[
            pltpu.VMEM((4, tokens, width), BF),
            pltpu.VMEM((4, tokens, width), BF),
            pltpu.VMEM(full + (4 * tokens,), BF),
            pltpu.VMEM(full + (4 * tokens,), BF),
            pltpu.VMEM((2, 2, 4, 4, 2, rows // 2, cols), BF),
            pltpu.VMEM((4, tokens, cols), F32),
            pltpu.VMEM((4, tokens, cols), BF),
            pltpu.VMEM((4, tokens, cols), BF),
            pltpu.VMEM((2,) + full + (cols,), F32),
            pltpu.VMEM((4, 6, 2, rows, cols), BF),
            pltpu.VMEM((4, 6, 2, rows, cols), BF),
            pltpu.VMEM((4, 6, 8, 128), F32),
            pltpu.VMEM((4, 6, 8, 128), F32),
            pltpu.VMEM((8, 128), F32),
            pltpu.VMEM((4, 6, 1, rows // 2, cols), BF),
            pltpu.VMEM((4, 6, 1, rows // 2, cols), BF),
            pltpu.VMEM((4, 6, 8, 128), F32),
            pltpu.VMEM((4, 6, 8, 128), F32),
            pltpu.VMEM((8, 128), F32),
            pltpu.VMEM((2, 2, 1, rows, cols), BF),
            pltpu.VMEM((2, 3, 1, rows, cols), BF),
            pltpu.VMEM((2, 2, 8, 128), F32),
            pltpu.VMEM((2, 3, 8, 128), F32),
            pltpu.VMEM((4, tokens, width), F32),
            pltpu.VMEM((2, tokens, width), F32),
            pltpu.VMEM((tokens, width), F32),
            pltpu.VMEM((4, 1, hidden), F32),
            pltpu.VMEM((4, 1, hidden), F32),
            pltpu.VMEM((2, 1, hidden), F32),
            pltpu.VMEM((2, rows, 128), F32),
            pltpu.SemaphoreType.DMA((COPIES,)),
            pltpu.SemaphoreType.DMA((COPIES,)),
            pltpu.SemaphoreType.DMA((4,)),
        ],
        compiler_params=pltpu.CompilerParams(
            collective_id=0, has_side_effects=True, vmem_limit_bytes=63 * 1024 * 1024
        ),
    )(inputs, up3, dn3, out_cotangent)
    return gin, gup, gdn.T, eup[:, 0], edn.reshape(hidden)


def solution(mesh):
    torus = Mesh(
        mesh.devices.reshape(mesh.shape["rep"], 2, 4, 4, mesh.shape["tp"]),
        ("rep", "fs_0", "fs_1", "fs_2", "tp"),
    )
    placed = (P(REP_FS_TP, None), P(FS, "tp"), P("tp", FS), P(REP_FS_TP, None))
    return jax.shard_map(
        per_device,
        mesh=torus,
        in_specs=placed,
        out_specs=(P(REP_FS_TP, None), P(FS, "tp"), P("tp", FS), P(FS), P("tp")),
        check_vma=False,
    )
```

time: 654 us -> 98.4 us (0.15)
  waiting for transfers between devices: 556 us -> 0 us
  Pallas kernels: 0 us -> 91.8 us
  matrix products: 24.3 us -> 0 us
  blocking collectives: 24.1 us -> 0 us
  between operations: 14.9 us -> 0.65 us
  other arithmetic: 13.4 us -> 0 us
  local copies, waits for them, and re-layouts: 16.4 us -> 5.61 us
    all_gather x4 -> x0, waiting for transfers between devices: 318 us -> none  [the longest x2 277 us: folded(): lax.all_gather(part, axis, axis=dim, tiled=True)]
    reduce_scatter x2 -> x0, waiting for transfers between devices: 237 us -> none  [the longest x1 210 us: summed_rows(): return lax.psum_scatter(whole, axis, scatter_dimension=0, tiled=True)]
    pallas_call x0 -> x1, Pallas kernels: none -> 91.8 us  [per_device(): pl.pallas_call(make_kernel(tokens, width, cols, ff, factor), out_shape=(j...]
    dot_general x5 -> x0, matrix products: 24.3 us -> none  [the longest x4 19.8 us: contract(): lax.dot_general(left, right, (((left_dim,), (right_dim,)), ((), ())), pre...]
    psum x3 -> x0, blocking collectives: 20.9 us -> none  [one_axis_at_a_time(): array = lax.psum(array, axis)]
    concatenate x2 -> x0, other arithmetic: 7.23 us -> none  [the longest x1 6.18 us: joint_part(): jnp.concatenate([up_part(start, count), down_part(start, count)], axis=1)]
  transfers between devices with their start and end apart: 6 -> 0, of which waited for: 6 -> 0; matrix products, arithmetic and copies ran while one was open for 4% -> 0% of each run, Pallas kernels for 0% -> 0%
where the time goes in v1:
time: 98.4 us; the launch traced here: 98.1 us
  Pallas kernels  91.8 us (93%)
  local copies, waits for them, and re-layouts  5.61 us (6%)
    pallas_call x1, Pallas kernels, per_device(): pl.pallas_call(make_kernel(tokens, width, cols, ff, factor), out_shape=(j...  91.8 us
    unnamed x10, local copies, waits for them, and re-layouts  4.26 us

profile of v1, /device:TPU:1, one launch (start us, length us, event | category | flops | bytes accessed | tf_op | source)
XLA Modules:
  0.0 98.1 jit_solution(11593875558378455715)
XLA Ops:
  0.6 91.8 %shard_map.83 = (bf16[256,1024]{1,0:T(8,128)(2,1)}, f32[32,2048]{1,0:T(8,128)}, f32[32,2048]{1,0:T(8,128)}, f32[32,128]{1,0:T(8,128)}, f32[1,2048]{1,0:T(1,128)}) custom-call(bf16[256,1024]{1,0:T(8,128)(2,1)} %x_ref.1, bf16[2,16,2048]{2,1,0:T(8,128)(2,1)} %bitcast.7, bf16[2,16,2048]{2,1,0:T(8,128)(2,1)} %bitcast.8, bf16[256,1024]{1,0:T(8,128)(2,1)} %cot_ref.1), custom_call_target="tpu_custom_call" | custom-call | tf_op jit(solution)/shard_map/pallas_call | solution.py:483
  92.5 1.3 %slice_reduce_fusion = f32[32]{0:T(128)} fusion(f32[32,128]{1,0:T(8,128)} %get-tuple-element.13), kind=kLoop, calls=%fused_computation | loop fusion | bytes 256 | tf_op jit(solution)/shard_map/slice | solution.py:533
  93.8 0.0 copy-start.1
  93.8 1.9 %copy.13 = bf16[256,1024]{1,0:T(8,128)(2,1)} copy(bf16[256,1024]{1,0:T(8,128)(2,1)} %get-tuple-element.20) | data formatting | bytes 1048576
  95.7 0.0 copy-done.1
  95.7 0.0 copy-start
  95.7 0.7 copy.14
  96.4 0.3 copy-done
  96.8 0.0 copy-start.2
  96.8 0.7 copy.15
  97.5 0.0 copy-done.2
  97.5 0.6 copy.16
Async XLA Ops:
  93.8 1.9 %copy-start.1 = (f32[32,2048]{1,0:T(8,128)S(1)}, f32[32,2048]{1,0:T(8,128)}, u32[]{:S(2)}) copy-start(f32[32,2048]{1,0:T(8,128)} %get-tuple-element.21) | copy-start | bytes 786436
  95.7 1.0 %copy-start = (f32[32,2048]{1,0:T(8,128)S(1)}, f32[32,2048]{1,0:T(8,128)}, u32[]{:S(2)}) copy-start(f32[32,2048]{1,0:T(8,128)} %get-tuple-element.12) | copy-start | bytes 786436
  96.8 0.7 copy-start.2

commit v2 on v1

--- a/solution.py
+++ b/solution.py
@@ -23,8 +23,8 @@
         x_ref, up_ref, dn_ref, cot_ref,
         gin_ref, gup_ref, gdn_ref, eup_ref, edn_ref,
         X, C, XT, CT, W, RP, ACT, GP, G,
-        s1s, s1r, c1s, c1r, R1, s2s, s2r, c2s, c2r, R2, s3s, s3r, c3s, c3r,
-        PART, DR, ZR, EX, EY, EZ, EU,
+        s1s, s1r, c1s, c1r, s2s, s2r, c2s, c2r, s3s, s3r, c3s, c3r,
+        PART, DR, ZS, ZR, zsc, EX, EY, EZ, EU,
         ssem, rsem, lsem,
     ):
         r = lax.axis_index("rep")
@@ -105,16 +105,13 @@
             send((2, w, h, s, 0), ref, ref, bdev(1))
             send((2, w, h, s, 1), ref, ref, bdev(3))
 
-        def step1(w, h):
+        def near(w, h, side):
             a, b, adev, _ = axes(h)
-            recv((1, w, h, 0))
-            ref = blk(W, w, h, at(a, 3), b).at[0]
-            send((1, w, h, 2), ref, ref, adev(1))
-            spread(w, h, 1, at(a, 3))
-            recv((1, w, h, 1))
-            ref = blk(W, w, h, at(a, 1), b).at[1]
-            send((1, w, h, 3), ref, ref, adev(3))
-            spread(w, h, 2, at(a, 1))
+            recv((1, w, h, side))
+            place, away = ((at(a, 3), 1), (at(a, 1), 3))[side]
+            ref = blk(W, w, h, place, b).at[side]
+            send((1, w, h, 2 + side), ref, ref, adev(away))
+            spread(w, h, 1 + side, place)
 
         def step2(w, h):
             a = axes(h)[0]
@@ -154,27 +151,23 @@
             v = src[slot].T
             dst[:, :, :, :, slot * tokens:(slot + 1) * tokens] = v.reshape(2, 4, 4, width // 32, tokens)
 
-        tile = min(512, cols)
-
-        def weight(w, n):
-            return W[w, :, :, :, :, :, pl.ds(pl.multiple_of(n * tile, tile), tile)].reshape(width, tile)
-
-        def project(slot):
-            def body(n, _):
-                col = pl.ds(pl.multiple_of(n * tile, tile), tile)
-                pre = jnp.maximum(jnp.dot(X[slot], weight(UP, n), preferred_element_type=F32), 0.0)
-                RP[slot, :, col] = pre
-                ACT[slot, :, col] = (pre * pre).astype(BF)
-                return 0
-            lax.fori_loop(0, cols // tile, body, 0)
-
-        def pull_back(slot):
-            def body(n, _):
-                col = pl.ds(pl.multiple_of(n * tile, tile), tile)
-                back = jnp.dot(C[slot], weight(DN, n), preferred_element_type=F32)
-                GP[slot, :, col] = (2.0 * RP[slot, :, col] * back).astype(BF)
-                return 0
-            lax.fori_loop(0, cols // tile, body, 0)
+        def weight(w):
+            return W[w].reshape(width, cols)
+
+        def both(ref, s1, s2):
+            return jnp.concatenate([ref[s1], ref[s2]], axis=0)
+
+        def project(s1, s2):
+            pre = jnp.maximum(jnp.dot(both(X, s1, s2), weight(UP), preferred_element_type=F32), 0.0)
+            for n, slot in enumerate((s1, s2)):
+                v = pre[n * tokens:(n + 1) * tokens]
+                RP[slot] = v
+                ACT[slot] = (v * v).astype(BF)
+
+        def pull_back(s1, s2):
+            back = jnp.dot(both(C, s1, s2), weight(DN), preferred_element_type=F32)
+            for n, slot in enumerate((s1, s2)):
+                GP[slot] = (2.0 * RP[slot] * back[n * tokens:(n + 1) * tokens]).astype(BF)
 
         init(UP, 0)
         init(DN, 0)
@@ -183,56 +176,57 @@
                 rows = pl.ds(i * half, half)
                 send((name, "z", i), src.at[rows], dst.at[2, rows], zpeer)
             send((name, "t"), src, dst.at[1], tpeer)
-        recv(("a2a", UP))
-        init(UP, 1)
-        step1(UP, 0)
-        fwd(UP, 0, 0)
-        recv(("a2a", DN))
-        init(DN, 1)
-        step1(UP, 1)
-        fwd(UP, 1, 0)
-        step2(UP, 0)
-        fwd(UP, 0, 1)
-        fwd(UP, 0, 2)
-        step1(DN, 0)
-        fwd(DN, 0, 0)
-        step2(UP, 1)
-        fwd(UP, 1, 1)
-        fwd(UP, 1, 2)
-        step1(DN, 1)
-        fwd(DN, 1, 0)
         for c in locals_:
             c.wait()
         turn(X, XT, 0)
-        fwd(UP, 0, 3)
-        fwd(UP, 1, 3)
+        turn(C, CT, 0)
+        recv(("a2a", UP))
+        init(UP, 1)
+        recv(("a2a", DN))
+        init(DN, 1)
+        near(UP, 0, 0)
+        near(UP, 0, 1)
+        near(UP, 1, 0)
+        near(UP, 1, 1)
+        near(DN, 0, 0)
+        step2(UP, 0)
+        near(DN, 0, 1)
+        fwd(UP, 0, 0)
+        near(DN, 1, 0)
+        step2(UP, 1)
+        fwd(UP, 1, 2)
+        fwd(UP, 1, 0)
+        near(DN, 1, 1)
+        fwd(UP, 0, 1)
+        pass_on("x", X, 0)
         arrived("x", 1)
         turn(X, XT, 1)
+        fwd(UP, 0, 3)
+        fwd(UP, 1, 1)
+        fwd(UP, 1, 3)
+        fwd(UP, 0, 2)
         step2(DN, 0)
-        fwd(DN, 0, 1)
+        fwd(DN, 0, 0)
         fwd(DN, 0, 2)
-        pass_on("x", X, 0)
-        turn(C, CT, 0)
         step2(DN, 1)
-        fwd(DN, 1, 1)
-        fwd(DN, 1, 2)
+        pass_on("x", X, 1)
         arrived("c", 1)
         turn(C, CT, 1)
-        pass_on("x", X, 1)
+        fwd(DN, 1, 1)
+        fwd(DN, 0, 1)
+        turn(X, XT, 2)
+        arrived("x", 3)
+        turn(X, XT, 3)
         fin(UP)
-        project(0)
-        project(1)
-        turn(X, XT, 2)
-        project(2)
+        project(0, 1)
+        fwd(DN, 1, 2)
+        fwd(DN, 1, 0)
+        project(2, 3)
         fwd(DN, 0, 3)
         fwd(DN, 1, 3)
-        arrived("x", 3)
-        turn(X, XT, 3)
-        project(3)
         pass_on("c", C, 0)
         fin(DN)
-        pull_back(0)
-        pull_back(1)
+        pull_back(0, 1)
         pass_on("c", C, 1)
         turn(C, CT, 2)
         arrived("c", 3)
@@ -248,30 +242,14 @@
         def raxes(h):
             return (y, x, ydev, xdev) if h == 0 else (x, y, xdev, ydev)
 
-        def multiply(w, h, a1, a2):
+        def multiply(w, h):
             z = j if h == 0 else 1 - j
-            lhs = lhs_of[w]
-            if h == 0:
-                l1, l2 = lhs[z, a1], lhs[z, a2]
-            else:
-                l1, l2 = lhs[z, :, a1], lhs[z, :, a2]
             rows = 4 * (width // 32)
-            left = jnp.concatenate([l1.reshape(rows, -1), l2.reshape(rows, -1)], axis=0)
-
-            def body(n, _):
-                col = pl.ds(pl.multiple_of(n * tile, tile), tile)
-                right = rhs_of[w][:, :, col].reshape(4 * tokens, tile)
-                out = jnp.dot(left, right, preferred_element_type=F32)
-                for k, a in enumerate((a1, a2)):
-                    part = out[k * rows:(k + 1) * rows].reshape(4, width // 32, tile)
-                    if h == 0:
-                        G[w, z, a, :, :, col] = part
-                    else:
-                        G[w, z, :, a, :, col] = part
-                return 0
-            lax.fori_loop(0, cols // tile, body, 0)
-
-        def encode(srcs, dst, scale):
+            left = lhs_of[w][z].reshape(4 * rows, 4 * tokens)
+            out = jnp.dot(left, rhs_of[w][...].reshape(4 * tokens, cols), preferred_element_type=F32)
+            G[w, z] = out.reshape(4, 4, width // 32, cols)
+
+        def encode(srcs, dst, scale, steps=3):
             top = None
             for src in srcs:
                 for c in lanes:
@@ -279,19 +257,19 @@
                     top = m if top is None else jnp.maximum(top, m)
             top = jnp.maximum(top, 2e-34)
             scale[...] = top
-            inv = 32768.0 / top
+            inv = 2.0 ** (120 >> steps) / top
             for i, src in enumerate(srcs):
                 for c in lanes:
                     v = src[:, c]
                     v3 = v.reshape(-1, 8, 128) * inv
-                    for _ in range(3):
+                    for _ in range(steps):
                         v3 = v3 * jnp.abs(v3)
                     dst[i, :, c] = v3.reshape(v.shape).astype(BF)
 
-        def decode(buf, scale, i, c):
+        def decode(buf, scale, i, c, steps=3):
             v = buf[i, :, c].astype(F32)
-            m = jnp.exp2(jnp.log2(jnp.abs(v)) * 0.125)
-            m = jnp.where(v < 0, -m, m).reshape(-1, 8, 128) * (scale[...] * (1.0 / 32768.0))
+            m = jnp.exp2(jnp.log2(jnp.abs(v)) * 0.5 ** steps)
+            m = jnp.where(v < 0, -m, m).reshape(-1, 8, 128) * (scale[...] * 0.5 ** (120 >> steps))
             return m.reshape(v.shape)
 
         class Ring:
@@ -355,16 +333,11 @@
         first = {(w, h): ring1(w, h) for w in (UP, DN) for h in (0, 1)}
         second = {(w, h): ring2(w, h) for w in (UP, DN) for h in (0, 1)}
 
-        def launch(w):
-            for h in (0, 1):
-                a = raxes(h)[0]
-                multiply(w, h, at(a, 2), at(a, 1))
-                first[w, h].far()
-                first[w, h].near_right()
-            for h in (0, 1):
-                a = raxes(h)[0]
-                multiply(w, h, at(a, 3), a)
-                first[w, h].near_left()
+        def launch(w, h):
+            multiply(w, h)
+            first[w, h].far()
+            first[w, h].near_right()
+            first[w, h].near_left()
 
         def launch2(w):
             for h in (0, 1):
@@ -403,33 +376,31 @@
                 theirs = theirs + decode(s3r.at[w, 2], c3r.at[w, 2], 0, lane)
                 out[:, pl.ds(pl.multiple_of((1 - j) * cols + c * 128, 128), 128)] = theirs * factor
 
-        def input_part(slot, out):
-            def body(n, _):
-                w = W[UP, n // 2, pl.ds(2 * lax.rem(n, 2), 2)].reshape(width // 4, cols)
-                v = lax.dot_general(GP[slot], w, (((1,), (1,)), ((), ())), preferred_element_type=F32)
-                out[:, pl.ds(pl.multiple_of(n * (width // 4), width // 4), width // 4)] = v
-                return 0
-            lax.fori_loop(0, 4, body, 0)
-
-        launch(DN)
-        pull_back(2)
-        pull_back(3)
-        input_part(3, PART.at[0])
-        send(("g", "t", 0), PART.at[0], DR.at[0], tpeer)
-        input_part(2, PART.at[1])
-        recv(("g", "t", 0))
-        PART[1] = PART[1] + DR[0]
-        send(("g", "z"), PART.at[1], ZR, zpeer)
+        def input_part(s1, s2):
+            w = W[UP].reshape(width, cols)
+            v = lax.dot_general(both(GP, s1, s2), w, (((1,), (1,)), ((), ())), preferred_element_type=F32)
+            PART[s1] = v[:tokens]
+            PART[s2] = v[tokens:]
+
+        launch(DN, 0)
+        launch(DN, 1)
+        pull_back(2, 3)
+        launch(UP, 0)
         for h in (0, 1):
             first[DN, h].relay()
-        launch(UP)
-        input_part(1, PART.at[2])
-        send(("g", "t", 1), PART.at[2], DR.at[1], tpeer)
+        launch(UP, 1)
+        input_part(3, 1)
+        for n, slot in enumerate((3, 1)):
+            send(("g", "t", n), PART.at[slot], DR.at[n], tpeer)
+        input_part(2, 0)
         launch2(DN)
+        recv(("g", "t", 0))
+        PART[2] = PART[2] + DR[0]
+        encode([PART.at[2]], ZS, zsc.at[0], 4)
+        send(("g", "zs"), zsc.at[0], zsc.at[1], zpeer)
+        send(("g", "z"), ZS, ZR, zpeer)
         for h in (0, 1):
             first[UP, h].relay()
-        input_part(0, PART.at[3])
-        recv(("g", "t", 1))
         relay2(DN)
         launch2(UP)
         launch3(DN)
@@ -445,8 +416,12 @@
         EY[y] = EX[0] + EX[1] + EX[2] + EX[3]
         for d in (1, 2, 3):
             send(("e", "y", d), EY.at[y], EY.at[y], ydev(d))
+        recv(("g", "t", 1))
+        recv(("g", "zs"))
         recv(("g", "z"))
-        gin_ref[...] = (PART[3] + DR[1] + ZR[...]).astype(BF)
+        for c in lanes:
+            far = decode(ZR, zsc.at[1], 0, c, 4)
+            gin_ref[:, c] = (PART[0, :, c] + DR[1, :, c] + far).astype(BF)
         for d in (1, 2, 3):
             recv(("e", "y", d))
         EZ[0] = EY[0] + EY[1] + EY[2] + EY[3]
@@ -461,12 +436,24 @@
         recv(("e", "z"))
         edn_ref[...] = (EZ[0] + EZ[1]) * (1.0 / width)
         recv(("e", "t"))
-        both = jnp.sum(EU[0] + EU[1], axis=1, keepdims=True) * (1.0 / ff)
-        eup_ref[...] = jnp.broadcast_to(both, eup_ref.shape)
+        eup_ref[...] = jnp.sum((EU[0] + EU[1]).T, axis=0, keepdims=True) * (1.0 / ff)
         for c in copies.values():
             c.wait_send()
 
     return kernel
+
+
+def hand_over(results):
+    vm = pl.BlockSpec(memory_space=pltpu.VMEM)
+    shapes = [jax.ShapeDtypeStruct(v.shape, v.dtype) for v in results]
+    shapes[4] = jax.ShapeDtypeStruct(results[4].shape[1:], F32)
+
+    def kernel(*refs):
+        for src, dst in zip(refs[:4], refs[5:9]):
+            dst[...] = src[...]
+        refs[9][...] = refs[4][0]
+
+    return pl.pallas_call(kernel, out_shape=tuple(shapes), in_specs=[vm] * 5, out_specs=(vm,) * 5)(*results)
 
 
 def per_device(inputs, up_proj, down_proj, out_cotangent):
@@ -480,13 +467,13 @@
     dn3 = down_proj.T.reshape(2, rows // 2, hidden)
     vm = pl.BlockSpec(memory_space=pltpu.VMEM)
     full = (2, 4, 4, rows)
-    gin, gup, gdn, eup, edn = pl.pallas_call(
+    results = pl.pallas_call(
         make_kernel(tokens, width, cols, ff, factor),
         out_shape=(
             jax.ShapeDtypeStruct((tokens, width), BF),
             jax.ShapeDtypeStruct((rows, hidden), F32),
             jax.ShapeDtypeStruct((rows, hidden), F32),
-            jax.ShapeDtypeStruct((rows, 128), F32),
+            jax.ShapeDtypeStruct((1, rows), F32),
             jax.ShapeDtypeStruct((1, hidden), F32),
         ),
         in_specs=[vm] * 4,
@@ -505,19 +492,19 @@
             pltpu.VMEM((4, 6, 2, rows, cols), BF),
             pltpu.VMEM((4, 6, 8, 128), F32),
             pltpu.VMEM((4, 6, 8, 128), F32),
-            pltpu.VMEM((8, 128), F32),
             pltpu.VMEM((4, 6, 1, rows // 2, cols), BF),
             pltpu.VMEM((4, 6, 1, rows // 2, cols), BF),
             pltpu.VMEM((4, 6, 8, 128), F32),
             pltpu.VMEM((4, 6, 8, 128), F32),
-            pltpu.VMEM((8, 128), F32),
             pltpu.VMEM((2, 2, 1, rows, cols), BF),
             pltpu.VMEM((2, 3, 1, rows, cols), BF),
             pltpu.VMEM((2, 2, 8, 128), F32),
             pltpu.VMEM((2, 3, 8, 128), F32),
             pltpu.VMEM((4, tokens, width), F32),
             pltpu.VMEM((2, tokens, width), F32),
-            pltpu.VMEM((tokens, width), F32),
+            pltpu.VMEM((1, tokens, width), BF),
+            pltpu.VMEM((1, tokens, width), BF),
+            pltpu.VMEM((2, 8, 128), F32),
             pltpu.VMEM((4, 1, hidden), F32),
             pltpu.VMEM((4, 1, hidden), F32),
             pltpu.VMEM((2, 1, hidden), F32),
@@ -530,7 +517,8 @@
             collective_id=0, has_side_effects=True, vmem_limit_bytes=63 * 1024 * 1024
         ),
     )(inputs, up3, dn3, out_cotangent)
-    return gin, gup, gdn.T, eup[:, 0], edn.reshape(hidden)
+    gin, gup, gdn, eup, edn = hand_over(results)
+    return gin, gup, gdn.T, eup.reshape(rows), edn
 
 
 def solution(mesh):

time: 98.4 us -> 91.3 us (0.928)
  local copies, waits for them, and re-layouts: 5.61 us -> 0 us
  Pallas kernels: 91.8 us -> 90.5 us
    unnamed x10 -> x0, local copies, waits for them, and re-layouts: 4.26 us -> none
    pallas_call x1, Pallas kernels: 91.8 us -> 88.3 us  [per_device(): pl.pallas_call(make_kernel(tokens, width, cols, ff, factor), out_shape=(j...]
    pallas_call x0 -> x1, Pallas kernels: none -> 2.18 us  [hand_over(): pl.pallas_call(kernel, out_shape=tuple(shapes), in_specs=[vm] * 5, out_sp...]
    slice x1 -> x0, local copies, waits for them, and re-layouts: 1.34 us -> none  [per_device(): return (gin, gup, gdn.T, eup[:, 0], edn.reshape(hidden))]
where the time goes in v2:
time: 91.3 us; the launch traced here: 91.1 us
  Pallas kernels  90.5 us (99%)
    pallas_call x1, Pallas kernels, per_device(): pl.pallas_call(make_kernel(tokens, width, cols, ff, factor), out_shape=(j...  88.3 us
    pallas_call x1, Pallas kernels, hand_over(): pl.pallas_call(kernel, out_shape=tuple(shapes), in_specs=[vm] * 5, out_sp...  2.18 us

profile of v2, /device:TPU:1, one launch (start us, length us, event | category | flops | bytes accessed | tf_op | source)
XLA Modules:
  0.0 91.1 jit_solution(276322000739540319)
XLA Ops:
  0.6 88.3 %shard_map.83 = (bf16[256,1024]{1,0:T(8,128)(2,1)}, f32[32,2048]{1,0:T(8,128)}, f32[32,2048]{1,0:T(8,128)}, f32[1,32]{1,0:T(1,128)}, f32[1,2048]{1,0:T(1,128)}) custom-call(bf16[256,1024]{1,0:T(8,128)(2,1)} %x_ref.1, bf16[2,16,2048]{2,1,0:T(8,128)(2,1)} %bitcast.6, bf16[2,16,2048]{2,1,0:T(8,128)(2,1)} %bitcast.7, bf16[256,1024]{1,0:T(8,128)(2,1)} %cot_ref.1), custom_call_target="tpu_custom_call" | custom-call | tf_op jit(solution)/shard_map/pallas_call | solution.py:470
  88.9 2.2 %shard_map.84 = (bf16[256,1024]{1,0:T(8,128)(2,1)}, f32[32,2048]{1,0:T(8,128)}, f32[32,2048]{1,0:T(8,128)}, f32[1,32]{1,0:T(1,128)}, f32[2048]{0:T(1024)}) custom-call(bf16[256,1024]{1,0:T(8,128)(2,1)} %get-tuple-element.15.refs_0_, f32[32,2048]{1,0:T(8,128)} %get-tuple-element.16.refs_1_, f32[32,2048]{1,0:T(8,128)} %get-tuple-element.17.refs_2_, ...), custom_call_target="tpu_custom_call" | custom-call | tf_op jit(solution)/shard_map/pallas_call | solution.py:456

commit v3 on v2

--- a/solution.py
+++ b/solution.py
@@ -16,6 +16,31 @@
 COPIES = 240
 
 
+ORDER = [
+    ("init", 1, 0), ("init", 0, 0), ("init", 0, 1), ("near", 1, 0, 0), ("init", 1, 1), ("near", 0, 0, 1),
+    ("near", 0, 0, 0), ("near", 0, 1, 0), ("near", 0, 1, 1), ("fwd", 0, 0, 0, 1), ("near", 1, 1, 1),
+    ("step2", 0, 0), ("near", 1, 1, 0), ("fwd", 0, 0, 0, 0), ("pass", "x", 1), ("near", 1, 0, 1),
+    ("fwd", 0, 0, 1, 0), ("fwd", 0, 1, 1, 0), ("fwd", 0, 1, 2, 1), ("fwd", 0, 0, 1, 1), ("fwd", 0, 1, 0, 1),
+    ("turn", "x", 0), ("step2", 0, 1), ("fwd", 0, 0, 2, 0), ("fwd", 0, 0, 2, 1), ("fwd", 1, 1, 2, 0),
+    ("fwd", 0, 1, 0, 0), ("fwd", 0, 1, 2, 0), ("turn", "c", 1), ("fwd", 1, 1, 1, 1), ("fwd", 0, 1, 1, 1),
+    ("fwd", 1, 0, 1, 0), ("pass", "x", 0), ("fwd", 0, 1, 3, 0), ("step2", 1, 1), ("fwd", 0, 0, 3, 1),
+    ("turn", "x", 2), ("fwd", 1, 1, 1, 0), ("step2", 1, 0), ("fwd", 1, 0, 2, 1), ("fwd", 0, 0, 3, 0),
+    ("fwd", 1, 1, 0, 0), ("fwd", 0, 1, 3, 1), ("turn", "x", 1), ("fwd", 1, 0, 3, 0), ("fwd", 1, 0, 2, 0),
+    ("fwd", 1, 0, 3, 1), ("fwd", 1, 1, 3, 0), ("pass", "c", 0), ("fwd", 1, 1, 2, 1), ("proj", 0),
+    ("fwd", 1, 0, 1, 1), ("fwd", 1, 1, 3, 1), ("pass", "c", 1), ("turn", "c", 2), ("turn", "x", 3), ("proj", 1),
+    ("fwd", 1, 0, 0, 1), ("turn", "c", 0), ("fwd", 1, 1, 0, 1), ("fwd", 1, 0, 0, 0), ("turn", "c", 3),
+    ("mult", 1, 1), ("mult", 1, 0), ("far", 1, 0), ("far", 1, 1), ("nr", 1, 0), ("nr", 1, 1), ("nl", 1, 1),
+    ("pull", 1), ("pull", 0), ("nl", 1, 0), ("ip", 0), ("mult", 0, 1), ("far", 0, 1), ("rl", 1, 0, 0),
+    ("rl", 1, 0, 1), ("rl", 1, 1, 1), ("ip", 1), ("rl", 1, 1, 0), ("mult", 0, 0), ("far", 0, 0), ("ni", 1, 0),
+    ("gz",), ("st2", 1, 0), ("nl", 0, 1), ("nl", 0, 0), ("nr", 0, 0), ("rl", 0, 1, 0), ("ni", 1, 1),
+    ("st2", 1, 1), ("rl2", 1, 0, 1), ("rl", 0, 0, 1), ("rl2", 1, 0, 0), ("rl", 0, 0, 0), ("ni", 0, 0),
+    ("rl", 0, 1, 1), ("st3", 1, 0), ("nr", 0, 1), ("rl2", 1, 1, 0), ("rl2", 1, 1, 1), ("st2", 0, 0),
+    ("st3", 1, 1), ("gin",), ("ni", 0, 1), ("st2", 0, 1), ("rl2", 0, 0, 1), ("rl2", 0, 0, 0), ("fin", 1), ("ex",),
+    ("rl2", 0, 1, 0), ("rl2", 0, 1, 1), ("st3", 0, 0), ("ey",), ("st3", 0, 1), ("ez",), ("fin", 0), ("eu",),
+    ("eup",), ("edn",),
+]
+
+
 def make_kernel(tokens, width, cols, ff, factor):
     lanes = [pl.ds(c * 128, 128) for c in range(cols // 128)]
 
@@ -25,7 +50,7 @@
         X, C, XT, CT, W, RP, ACT, GP, G,
         s1s, s1r, c1s, c1r, s2s, s2r, c2s, c2r, s3s, s3r, c3s, c3r,
         PART, DR, ZS, ZR, zsc, EX, EY, EZ, EU,
-        ssem, rsem, lsem,
+        OTH, ssem, rsem, lsem,
     ):
         r = lax.axis_index("rep")
         j = lax.axis_index("fs_0")
@@ -46,6 +71,19 @@
         rpeer = {"rep": 1 - r}
         rzpeer = {"rep": 1 - r, "fs_0": 1 - j}
         tpeer = {"tp": 1 - t}
+
+        own = pl.ds(pl.multiple_of(j * cols, cols), cols)
+        other = pl.ds(pl.multiple_of((1 - j) * cols, cols), cols)
+        loads = [
+            pltpu.make_async_copy(up_ref.at[:, :, other], OTH.at[UP], lsem.at[0]),
+            pltpu.make_async_copy(dn_ref.at[:, :, other], OTH.at[DN], lsem.at[1]),
+            pltpu.make_async_copy(up_ref.at[:, :, own], W.at[UP, j, y, x], lsem.at[2]),
+            pltpu.make_async_copy(dn_ref.at[:, :, own], W.at[DN, j, y, x], lsem.at[3]),
+            pltpu.make_async_copy(x_ref, X.at[0], lsem.at[4]),
+            pltpu.make_async_copy(cot_ref, C.at[0], lsem.at[5]),
+        ]
+        for c in loads:
+            c.start()
 
         barrier = pltpu.get_barrier_semaphore()
         peers = [xdev(1), xdev(2), xdev(3), ydev(1), ydev(2), ydev(3), zpeer, rpeer, rzpeer, tpeer]
@@ -68,20 +106,6 @@
             copies[key].wait_recv()
 
         half = tokens // 2
-        own = pl.ds(pl.multiple_of(j * cols, cols), cols)
-        other = pl.ds(pl.multiple_of((1 - j) * cols, cols), cols)
-        w_refs = (up_ref, dn_ref)
-
-        for w in (UP, DN):
-            send(("a2a", w), w_refs[w].at[:, :, other], W.at[w, j, y, x], zpeer)
-        locals_ = [
-            pltpu.make_async_copy(up_ref.at[:, :, own], W.at[UP, j, y, x], lsem.at[0]),
-            pltpu.make_async_copy(dn_ref.at[:, :, own], W.at[DN, j, y, x], lsem.at[1]),
-            pltpu.make_async_copy(x_ref, X.at[0], lsem.at[2]),
-            pltpu.make_async_copy(cot_ref, C.at[0], lsem.at[3]),
-        ]
-        for c in locals_:
-            c.start()
 
         def blk(ref, w, h, a, b):
             z = j if h == 0 else 1 - j
@@ -92,8 +116,9 @@
 
         def init(w, h):
             a, b, adev, bdev = axes(h)
-            src = w_refs[w].at[:, :, own] if h == 0 else blk(W, w, h, a, b)
-            dst = blk(W, w, h, a, b)
+            if h == 1:
+                recv(("a2a", w))
+            src = dst = blk(W, w, h, a, b)
             send((1, w, h, 0), src, dst, adev(1))
             send((1, w, h, 1), src, dst, adev(3))
             send((2, w, h, 0, 0), src, dst, bdev(1))
@@ -119,35 +144,40 @@
             recv((1, w, h, 3))
             spread(w, h, 3, at(a, 2))
 
-        def fwd(w, h, s):
+        def fwd(w, h, s, side):
             a, b, _, bdev = axes(h)
             a2 = at(a, (0, 3, 1, 2)[s])
-            recv((2, w, h, s, 0))
-            ref = blk(W, w, h, a2, at(b, 3)).at[0]
-            send((2, w, h, s, 2), ref, ref, bdev(1))
-            recv((2, w, h, s, 1))
-            ref = blk(W, w, h, a2, at(b, 1)).at[1]
-            send((2, w, h, s, 3), ref, ref, bdev(3))
+            recv((2, w, h, s, side))
+            place, away = ((at(b, 3), 1), (at(b, 1), 3))[side]
+            ref = blk(W, w, h, a2, place).at[side]
+            send((2, w, h, s, 2 + side), ref, ref, bdev(away))
+
+        whole = set()
 
         def fin(w):
+            if w in whole:
+                return
+            whole.add(w)
             for h in (0, 1):
                 for s in range(4):
                     recv((2, w, h, s, 2))
                     recv((2, w, h, s, 3))
 
-        def pass_on(name, buf, i):
+        stock = {"x": (X, XT), "c": (C, CT)}
+
+        def pass_on(name, i):
             recv((name, "z", i))
-            part = buf.at[2, pl.ds(i * half, half)]
-            send((name, "zt", i), part, buf.at[3, pl.ds(i * half, half)], tpeer)
-
-        def arrived(name, slot):
+            rows = pl.ds(i * half, half)
+            buf = stock[name][0]
+            send((name, "zt", i), buf.at[2, rows], buf.at[3, rows], tpeer)
+
+        def turn(name, slot):
             if slot == 1:
                 recv((name, "t"))
             if slot == 3:
                 recv((name, "zt", 0))
                 recv((name, "zt", 1))
-
-        def turn(src, dst, slot):
+            src, dst = stock[name]
             v = src[slot].T
             dst[:, :, :, :, slot * tokens:(slot + 1) * tokens] = v.reshape(2, 4, 4, width // 32, tokens)
 
@@ -157,80 +187,21 @@
         def both(ref, s1, s2):
             return jnp.concatenate([ref[s1], ref[s2]], axis=0)
 
-        def project(s1, s2):
+        def project(n):
+            s1, s2 = 2 * n, 2 * n + 1
+            fin(UP)
             pre = jnp.maximum(jnp.dot(both(X, s1, s2), weight(UP), preferred_element_type=F32), 0.0)
             for n, slot in enumerate((s1, s2)):
                 v = pre[n * tokens:(n + 1) * tokens]
                 RP[slot] = v
                 ACT[slot] = (v * v).astype(BF)
 
-        def pull_back(s1, s2):
+        def pull_back(n):
+            s1, s2 = 2 * n, 2 * n + 1
+            fin(DN)
             back = jnp.dot(both(C, s1, s2), weight(DN), preferred_element_type=F32)
             for n, slot in enumerate((s1, s2)):
                 GP[slot] = (2.0 * RP[slot] * back[n * tokens:(n + 1) * tokens]).astype(BF)
-
-        init(UP, 0)
-        init(DN, 0)
-        for name, src, dst in (("x", x_ref, X), ("c", cot_ref, C)):
-            for i in (0, 1):
-                rows = pl.ds(i * half, half)
-                send((name, "z", i), src.at[rows], dst.at[2, rows], zpeer)
-            send((name, "t"), src, dst.at[1], tpeer)
-        for c in locals_:
-            c.wait()
-        turn(X, XT, 0)
-        turn(C, CT, 0)
-        recv(("a2a", UP))
-        init(UP, 1)
-        recv(("a2a", DN))
-        init(DN, 1)
-        near(UP, 0, 0)
-        near(UP, 0, 1)
-        near(UP, 1, 0)
-        near(UP, 1, 1)
-        near(DN, 0, 0)
-        step2(UP, 0)
-        near(DN, 0, 1)
-        fwd(UP, 0, 0)
-        near(DN, 1, 0)
-        step2(UP, 1)
-        fwd(UP, 1, 2)
-        fwd(UP, 1, 0)
-        near(DN, 1, 1)
-        fwd(UP, 0, 1)
-        pass_on("x", X, 0)
-        arrived("x", 1)
-        turn(X, XT, 1)
-        fwd(UP, 0, 3)
-        fwd(UP, 1, 1)
-        fwd(UP, 1, 3)
-        fwd(UP, 0, 2)
-        step2(DN, 0)
-        fwd(DN, 0, 0)
-        fwd(DN, 0, 2)
-        step2(DN, 1)
-        pass_on("x", X, 1)
-        arrived("c", 1)
-        turn(C, CT, 1)
-        fwd(DN, 1, 1)
-        fwd(DN, 0, 1)
-        turn(X, XT, 2)
-        arrived("x", 3)
-        turn(X, XT, 3)
-        fin(UP)
-        project(0, 1)
-        fwd(DN, 1, 2)
-        fwd(DN, 1, 0)
-        project(2, 3)
-        fwd(DN, 0, 3)
-        fwd(DN, 1, 3)
-        pass_on("c", C, 0)
-        fin(DN)
-        pull_back(0, 1)
-        pass_on("c", C, 1)
-        turn(C, CT, 2)
-        arrived("c", 3)
-        turn(C, CT, 3)
 
         lhs_of = (XT, CT)
         rhs_of = (GP, ACT)
@@ -300,13 +271,10 @@
             def near_left(self):
                 self.post(3, self.parts(at(self.pos, 3), 0), 3)
 
-            def relay(self):
-                p = self.parts(at(self.pos, 1), 0)
-                self.take(0, p)
-                self.post(4, p, 1)
-                p = self.parts(at(self.pos, 3), 1)
-                self.take(1, p)
-                self.post(5, p, 3)
+            def relay(self, side):
+                p = self.parts(at(self.pos, (1, 3)[side]), side)
+                self.take(side, p)
+                self.post(4 + side, p, (1, 3)[side])
 
             def near_in(self):
                 self.take(3, self.parts(self.pos, 0))
@@ -333,37 +301,24 @@
         first = {(w, h): ring1(w, h) for w in (UP, DN) for h in (0, 1)}
         second = {(w, h): ring2(w, h) for w in (UP, DN) for h in (0, 1)}
 
-        def launch(w, h):
-            multiply(w, h)
-            first[w, h].far()
-            first[w, h].near_right()
-            first[w, h].near_left()
-
-        def launch2(w):
-            for h in (0, 1):
-                first[w, h].near_in()
-            for h in (0, 1):
-                first[w, h].last_in()
-                second[w, h].far()
-                second[w, h].near_right()
-                second[w, h].near_left()
-
-        def relay2(w):
-            for h in (0, 1):
-                second[w, h].relay()
-
-        def launch3(w):
-            for h in (0, 1):
-                second[w, h].near_in()
-                second[w, h].last_in()
-                a, b, _, _ = raxes(h)
-                encode([gblk(w, h, a, b)], s3s.at[w, h], c3s.at[w, h])
-                peers_ = [(0, rpeer)] if h == 0 else [(1, zpeer), (2, rzpeer)]
-                for i, dev in peers_:
-                    send((3, w, i, "s"), c3s.at[w, h], c3r.at[w, i], dev)
-                    send((3, w, i, "v"), s3s.at[w, h], s3r.at[w, i], dev)
-
-        def finish(w, out):
+        def second_start(w, h):
+            first[w, h].last_in()
+            second[w, h].far()
+            second[w, h].near_right()
+            second[w, h].near_left()
+
+        def third_start(w, h):
+            second[w, h].near_in()
+            second[w, h].last_in()
+            a, b, _, _ = raxes(h)
+            encode([gblk(w, h, a, b)], s3s.at[w, h], c3s.at[w, h])
+            peers_ = [(0, rpeer)] if h == 0 else [(1, zpeer), (2, rzpeer)]
+            for i, dev in peers_:
+                send((3, w, i, "s"), c3s.at[w, h], c3r.at[w, i], dev)
+                send((3, w, i, "v"), s3s.at[w, h], s3r.at[w, i], dev)
+
+        def finish(w):
+            out = (gup_ref, gdn_ref)[w]
             for i in range(3):
                 recv((3, w, i, "s"))
                 recv((3, w, i, "v"))
@@ -376,67 +331,93 @@
                 theirs = theirs + decode(s3r.at[w, 2], c3r.at[w, 2], 0, lane)
                 out[:, pl.ds(pl.multiple_of((1 - j) * cols + c * 128, 128), 128)] = theirs * factor
 
-        def input_part(s1, s2):
+        def input_part(n):
+            s1, s2 = ((3, 1), (2, 0))[n]
             w = W[UP].reshape(width, cols)
             v = lax.dot_general(both(GP, s1, s2), w, (((1,), (1,)), ((), ())), preferred_element_type=F32)
             PART[s1] = v[:tokens]
             PART[s2] = v[tokens:]
-
-        launch(DN, 0)
-        launch(DN, 1)
-        pull_back(2, 3)
-        launch(UP, 0)
-        for h in (0, 1):
-            first[DN, h].relay()
-        launch(UP, 1)
-        input_part(3, 1)
-        for n, slot in enumerate((3, 1)):
-            send(("g", "t", n), PART.at[slot], DR.at[n], tpeer)
-        input_part(2, 0)
-        launch2(DN)
-        recv(("g", "t", 0))
-        PART[2] = PART[2] + DR[0]
-        encode([PART.at[2]], ZS, zsc.at[0], 4)
-        send(("g", "zs"), zsc.at[0], zsc.at[1], zpeer)
-        send(("g", "z"), ZS, ZR, zpeer)
-        for h in (0, 1):
-            first[UP, h].relay()
-        relay2(DN)
-        launch2(UP)
-        launch3(DN)
-        relay2(UP)
-        finish(DN, gdn_ref)
-
-        EX[x] = jnp.sum(gdn_ref[...] * gdn_ref[...], axis=0, keepdims=True)
-        for d in (1, 2, 3):
-            send(("e", "x", d), EX.at[x], EX.at[x], xdev(d))
-        launch3(UP)
-        for d in (1, 2, 3):
-            recv(("e", "x", d))
-        EY[y] = EX[0] + EX[1] + EX[2] + EX[3]
-        for d in (1, 2, 3):
-            send(("e", "y", d), EY.at[y], EY.at[y], ydev(d))
-        recv(("g", "t", 1))
-        recv(("g", "zs"))
-        recv(("g", "z"))
-        for c in lanes:
-            far = decode(ZR, zsc.at[1], 0, c, 4)
-            gin_ref[:, c] = (PART[0, :, c] + DR[1, :, c] + far).astype(BF)
-        for d in (1, 2, 3):
-            recv(("e", "y", d))
-        EZ[0] = EY[0] + EY[1] + EY[2] + EY[3]
-        send(("e", "z"), EZ.at[0], EZ.at[1], zpeer)
-        finish(UP, gup_ref)
-        total = None
-        for c in range(2 * len(lanes)):
-            v = gup_ref[:, c * 128:(c + 1) * 128]
-            total = v * v if total is None else total + v * v
-        EU[0] = total
-        send(("e", "t"), EU.at[0], EU.at[1], tpeer)
-        recv(("e", "z"))
-        edn_ref[...] = (EZ[0] + EZ[1]) * (1.0 / width)
-        recv(("e", "t"))
-        eup_ref[...] = jnp.sum((EU[0] + EU[1]).T, axis=0, keepdims=True) * (1.0 / ff)
+            if n == 0:
+                for i, slot in enumerate((3, 1)):
+                    send(("g", "t", i), PART.at[slot], DR.at[i], tpeer)
+
+        def input_send():
+            recv(("g", "t", 0))
+            PART[2] = PART[2] + DR[0]
+            encode([PART.at[2]], ZS, zsc.at[0], 4)
+            send(("g", "zs"), zsc.at[0], zsc.at[1], zpeer)
+            send(("g", "z"), ZS, ZR, zpeer)
+
+        def input_sum():
+            recv(("g", "t", 1))
+            recv(("g", "zs"))
+            recv(("g", "z"))
+            for c in lanes:
+                far = decode(ZR, zsc.at[1], 0, c, 4)
+                gin_ref[:, c] = (PART[0, :, c] + DR[1, :, c] + far).astype(BF)
+
+        def energy_x():
+            EX[x] = jnp.sum(gdn_ref[...] * gdn_ref[...], axis=0, keepdims=True)
+            for d in (1, 2, 3):
+                send(("e", "x", d), EX.at[x], EX.at[x], xdev(d))
+
+        def energy_y():
+            for d in (1, 2, 3):
+                recv(("e", "x", d))
+            EY[y] = EX[0] + EX[1] + EX[2] + EX[3]
+            for d in (1, 2, 3):
+                send(("e", "y", d), EY.at[y], EY.at[y], ydev(d))
+
+        def energy_z():
+            for d in (1, 2, 3):
+                recv(("e", "y", d))
+            EZ[0] = EY[0] + EY[1] + EY[2] + EY[3]
+            send(("e", "z"), EZ.at[0], EZ.at[1], zpeer)
+
+        def energy_down():
+            recv(("e", "z"))
+            edn_ref[...] = (EZ[0] + EZ[1]) * (1.0 / width)
+
+        def energy_pair():
+            total = None
+            for c in range(2 * len(lanes)):
+                v = gup_ref[:, c * 128:(c + 1) * 128]
+                total = v * v if total is None else total + v * v
+            EU[0] = total
+            send(("e", "t"), EU.at[0], EU.at[1], tpeer)
+
+        def energy_up():
+            recv(("e", "t"))
+            eup_ref[...] = jnp.sum((EU[0] + EU[1]).T, axis=0, keepdims=True) * (1.0 / ff)
+
+        loads[0].wait()
+        send(("a2a", UP), OTH.at[UP], W.at[UP, j, y, x], rzpeer)
+        loads[1].wait()
+        send(("a2a", DN), OTH.at[DN], W.at[DN, j, y, x], rzpeer)
+        for c in loads[2:]:
+            c.wait()
+        for name in ("x", "c"):
+            buf = stock[name][0]
+            for i in (0, 1):
+                rows = pl.ds(i * half, half)
+                send((name, "z", i), buf.at[0, rows], buf.at[2, rows], zpeer)
+            send((name, "t"), buf.at[0], buf.at[1], tpeer)
+        todo = {
+            "init": init, "near": near, "step2": step2, "fwd": fwd, "pass": pass_on, "turn": turn,
+            "proj": project, "pull": pull_back, "mult": multiply,
+            "far": lambda w, h: first[w, h].far(),
+            "nr": lambda w, h: first[w, h].near_right(),
+            "nl": lambda w, h: first[w, h].near_left(),
+            "rl": lambda w, h, side: first[w, h].relay(side),
+            "ni": lambda w, h: first[w, h].near_in(),
+            "st2": second_start,
+            "rl2": lambda w, h, side: second[w, h].relay(side),
+            "st3": third_start, "fin": finish, "ip": input_part, "gz": input_send, "gin": input_sum,
+            "ex": energy_x, "ey": energy_y, "ez": energy_z, "edn": energy_down,
+            "eu": energy_pair, "eup": energy_up,
+        }
+        for name, *where in ORDER:
+            todo[name](*where)
         for c in copies.values():
             c.wait_send()
 
@@ -476,7 +457,7 @@
             jax.ShapeDtypeStruct((1, rows), F32),
             jax.ShapeDtypeStruct((1, hidden), F32),
         ),
-        in_specs=[vm] * 4,
+        in_specs=[pl.BlockSpec(memory_space=pl.ANY)] * 4,
         out_specs=(vm,) * 5,
         scratch_shapes=[
             pltpu.VMEM((4, tokens, width), BF),
@@ -509,9 +490,10 @@
             pltpu.VMEM((4, 1, hidden), F32),
             pltpu.VMEM((2, 1, hidden), F32),
             pltpu.VMEM((2, rows, 128), F32),
+            pltpu.VMEM((2, 2, rows // 2, cols), BF),
             pltpu.SemaphoreType.DMA((COPIES,)),
             pltpu.SemaphoreType.DMA((COPIES,)),
-            pltpu.SemaphoreType.DMA((4,)),
+            pltpu.SemaphoreType.DMA((6,)),
         ],
         compiler_params=pltpu.CompilerParams(
             collective_id=0, has_side_effects=True, vmem_limit_bytes=63 * 1024 * 1024

time: 91.3 us -> 82.7 us (0.906)
  Pallas kernels: 90.5 us -> 81.9 us
    pallas_call x1, Pallas kernels: 88.3 us -> 79.7 us  [per_device(): pl.pallas_call(make_kernel(tokens, width, cols, ff, factor), out_shape=(j...]
where the time goes in v3:
time: 82.7 us; the launch traced here: 82.6 us
  Pallas kernels  81.9 us (99%)
    pallas_call x1, Pallas kernels, per_device(): pl.pallas_call(make_kernel(tokens, width, cols, ff, factor), out_shape=(j...  79.7 us
    pallas_call x1, Pallas kernels, hand_over(): pl.pallas_call(kernel, out_shape=tuple(shapes), in_specs=[vm] * 5, out_sp...  2.18 us

profile of v3, /device:TPU:1, one launch (start us, length us, event | category | flops | bytes accessed | tf_op | source)
XLA Modules:
  0.0 82.6 jit_solution(15708440962291353282)
XLA Ops:
  0.6 79.7 %shard_map.83 = (bf16[256,1024]{1,0:T(8,128)(2,1)}, f32[32,2048]{1,0:T(8,128)}, f32[32,2048]{1,0:T(8,128)}, f32[1,32]{1,0:T(1,128)}, f32[1,2048]{1,0:T(1,128)}) custom-call(bf16[256,1024]{1,0:T(8,128)(2,1)} %x_ref.1, bf16[2,16,2048]{2,1,0:T(8,128)(2,1)} %bitcast.6, bf16[2,16,2048]{2,1,0:T(8,128)(2,1)} %bitcast.7, bf16[256,1024]{1,0:T(8,128)(2,1)} %cot_ref.1), custom_call_target="tpu_custom_call" | custom-call | tf_op jit(solution)/shard_map/pallas_call | solution.py:451
  80.4 2.2 %shard_map.84 = (bf16[256,1024]{1,0:T(8,128)(2,1)}, f32[32,2048]{1,0:T(8,128)}, f32[32,2048]{1,0:T(8,128)}, f32[1,32]{1,0:T(1,128)}, f32[2048]{0:T(1024)}) custom-call(bf16[256,1024]{1,0:T(8,128)(2,1)} %get-tuple-element.15.refs_0_, f32[32,2048]{1,0:T(8,128)} %get-tuple-element.16.refs_1_, f32[32,2048]{1,0:T(8,128)} %get-tuple-element.17.refs_2_, ...), custom_call_target="tpu_custom_call" | custom-call | tf_op jit(solution)/shard_map/pallas_call | solution.py:437

commit v4 on v3

--- a/solution.py
+++ b/solution.py
@@ -13,31 +13,34 @@
 F32 = jnp.float32
 RIGHT, LEFT = 0, 1
 UP, DN = 0, 1
-COPIES = 240
+COPIES = 280
+LAG = 30
 
 
 ORDER = [
-    ("init", 1, 0), ("init", 0, 0), ("init", 0, 1), ("near", 1, 0, 0), ("init", 1, 1), ("near", 0, 0, 1),
-    ("near", 0, 0, 0), ("near", 0, 1, 0), ("near", 0, 1, 1), ("fwd", 0, 0, 0, 1), ("near", 1, 1, 1),
-    ("step2", 0, 0), ("near", 1, 1, 0), ("fwd", 0, 0, 0, 0), ("pass", "x", 1), ("near", 1, 0, 1),
-    ("fwd", 0, 0, 1, 0), ("fwd", 0, 1, 1, 0), ("fwd", 0, 1, 2, 1), ("fwd", 0, 0, 1, 1), ("fwd", 0, 1, 0, 1),
-    ("turn", "x", 0), ("step2", 0, 1), ("fwd", 0, 0, 2, 0), ("fwd", 0, 0, 2, 1), ("fwd", 1, 1, 2, 0),
-    ("fwd", 0, 1, 0, 0), ("fwd", 0, 1, 2, 0), ("turn", "c", 1), ("fwd", 1, 1, 1, 1), ("fwd", 0, 1, 1, 1),
-    ("fwd", 1, 0, 1, 0), ("pass", "x", 0), ("fwd", 0, 1, 3, 0), ("step2", 1, 1), ("fwd", 0, 0, 3, 1),
-    ("turn", "x", 2), ("fwd", 1, 1, 1, 0), ("step2", 1, 0), ("fwd", 1, 0, 2, 1), ("fwd", 0, 0, 3, 0),
-    ("fwd", 1, 1, 0, 0), ("fwd", 0, 1, 3, 1), ("turn", "x", 1), ("fwd", 1, 0, 3, 0), ("fwd", 1, 0, 2, 0),
-    ("fwd", 1, 0, 3, 1), ("fwd", 1, 1, 3, 0), ("pass", "c", 0), ("fwd", 1, 1, 2, 1), ("proj", 0),
-    ("fwd", 1, 0, 1, 1), ("fwd", 1, 1, 3, 1), ("pass", "c", 1), ("turn", "c", 2), ("turn", "x", 3), ("proj", 1),
-    ("fwd", 1, 0, 0, 1), ("turn", "c", 0), ("fwd", 1, 1, 0, 1), ("fwd", 1, 0, 0, 0), ("turn", "c", 3),
-    ("mult", 1, 1), ("mult", 1, 0), ("far", 1, 0), ("far", 1, 1), ("nr", 1, 0), ("nr", 1, 1), ("nl", 1, 1),
-    ("pull", 1), ("pull", 0), ("nl", 1, 0), ("ip", 0), ("mult", 0, 1), ("far", 0, 1), ("rl", 1, 0, 0),
-    ("rl", 1, 0, 1), ("rl", 1, 1, 1), ("ip", 1), ("rl", 1, 1, 0), ("mult", 0, 0), ("far", 0, 0), ("ni", 1, 0),
-    ("gz",), ("st2", 1, 0), ("nl", 0, 1), ("nl", 0, 0), ("nr", 0, 0), ("rl", 0, 1, 0), ("ni", 1, 1),
-    ("st2", 1, 1), ("rl2", 1, 0, 1), ("rl", 0, 0, 1), ("rl2", 1, 0, 0), ("rl", 0, 0, 0), ("ni", 0, 0),
-    ("rl", 0, 1, 1), ("st3", 1, 0), ("nr", 0, 1), ("rl2", 1, 1, 0), ("rl2", 1, 1, 1), ("st2", 0, 0),
-    ("st3", 1, 1), ("gin",), ("ni", 0, 1), ("st2", 0, 1), ("rl2", 0, 0, 1), ("rl2", 0, 0, 0), ("fin", 1), ("ex",),
-    ("rl2", 0, 1, 0), ("rl2", 0, 1, 1), ("st3", 0, 0), ("ey",), ("st3", 0, 1), ("ez",), ("fin", 0), ("eu",),
-    ("eup",), ("edn",),
+    ("init", 0, 0), ("init", 1, 0), ("turn", "x", 1), ("init", 0, 1), ("init", 1, 1), ("near", 0, 1, 0),
+    ("turn", "c", 1), ("fwd", 0, 0, 0, 0), ("near", 0, 1, 1), ("near", 0, 0, 0), ("near", 1, 0, 1),
+    ("fwd", 0, 0, 0, 1), ("near", 0, 0, 1), ("step2", 0, 1), ("near", 1, 1, 0), ("near", 1, 1, 1),
+    ("near", 1, 0, 0), ("pass", "x", 0), ("fwd", 0, 1, 0, 0), ("fwd", 0, 1, 0, 1), ("pass", "x", 1),
+    ("step2", 0, 0), ("fwd", 0, 1, 3, 0), ("fwd", 0, 1, 3, 1), ("fwd", 0, 1, 1, 0), ("turn", "x", 3),
+    ("fwd", 1, 0, 0, 1), ("fwd", 0, 0, 1, 1), ("turn", "x", 0), ("fwd", 1, 1, 0, 0), ("fwd", 0, 0, 2, 0),
+    ("fwd", 0, 1, 1, 1), ("turn", "c", 0), ("fwd", 0, 1, 2, 1), ("fwd", 0, 1, 2, 0), ("fwd", 1, 0, 2, 1),
+    ("fwd", 0, 0, 1, 0), ("step2", 1, 1), ("fwd", 1, 1, 2, 1), ("fwd", 1, 1, 0, 1), ("fwd", 1, 1, 1, 0),
+    ("fwd", 0, 0, 3, 0), ("fwd", 0, 0, 2, 1), ("fwd", 1, 1, 1, 1), ("fwd", 0, 0, 3, 1), ("turn", "x", 2),
+    ("pass", "c", 0), ("step2", 1, 0), ("proj", 0), ("fwd", 1, 0, 0, 0), ("fwd", 1, 0, 2, 0), ("fwd", 1, 0, 1, 1),
+    ("fwd", 1, 0, 3, 0), ("pass", "c", 1), ("ma", 1, 1), ("fwd", 1, 1, 3, 0), ("fwd", 1, 1, 3, 1),
+    ("fwd", 1, 0, 1, 0), ("fwd", 1, 0, 3, 1), ("proj", 1), ("fwd", 1, 1, 2, 0), ("turn", "c", 2),
+    ("turn", "c", 3), ("mult", 1, 0), ("mult", 1, 1), ("far", 1, 1, 1), ("far", 1, 0, 0), ("nl", 1, 0),
+    ("far", 1, 1, 0), ("nr", 1, 1), ("far", 1, 0, 1), ("pull", 1), ("pull", 0), ("nr", 1, 0), ("nl", 1, 1),
+    ("ip", 0), ("mult", 0, 0), ("rl", 1, 0, 0, 0), ("rl", 1, 1, 1, 1), ("rl", 1, 1, 0, 1), ("rl", 1, 0, 1, 0),
+    ("rl", 1, 1, 0, 0), ("far", 0, 0, 0), ("rl", 1, 1, 1, 0), ("far", 0, 0, 1), ("rl", 1, 0, 0, 1),
+    ("mult", 0, 1), ("far", 0, 1, 0), ("ip", 1), ("gz",), ("nr", 0, 1), ("nl", 0, 1), ("rl", 1, 0, 1, 1),
+    ("ni", 1, 1), ("rl", 0, 0, 0, 0), ("rl", 0, 0, 1, 0), ("far", 0, 1, 1), ("ni", 1, 0), ("nl", 0, 0),
+    ("st2", 1, 1), ("nr", 0, 0), ("rl", 0, 0, 1, 1), ("rl", 0, 0, 0, 1), ("st2", 1, 0), ("ni", 0, 1),
+    ("rl2", 1, 0, 1), ("rl2", 1, 0, 0), ("rl", 0, 1, 1, 1), ("rl", 0, 1, 0, 0), ("rl2", 1, 1, 1),
+    ("rl", 0, 1, 0, 1), ("rl2", 1, 1, 0), ("rl", 0, 1, 1, 0), ("ni", 0, 0), ("st3", 1, 0), ("st2", 0, 0),
+    ("st3", 1, 1), ("st2", 0, 1), ("rl2", 0, 0, 0), ("rl2", 0, 0, 1), ("rl2", 0, 1, 1), ("rl2", 0, 1, 0),
+    ("st3", 0, 0), ("fin", 1), ("ex",), ("st3", 0, 1), ("ey",), ("fin", 0), ("eu",), ("gin",), ("eup",), ("edn",),
 ]
 
 
@@ -46,11 +49,11 @@
 
     def kernel(
         x_ref, up_ref, dn_ref, cot_ref,
-        gin_ref, gup_ref, gdn_ref, eup_ref, edn_ref,
+        gin_out, gup_out, gdn_out, eup_ref, edn_ref,
         X, C, XT, CT, W, RP, ACT, GP, G,
         s1s, s1r, c1s, c1r, s2s, s2r, c2s, c2r, s3s, s3r, c3s, c3r,
-        PART, DR, ZS, ZR, zsc, EX, EY, EZ, EU,
-        OTH, ssem, rsem, lsem,
+        PART, DR, ZS, ZR, zsc, EX, EY, EU,
+        OTH, gin_ref, gup_ref, gdn_ref, ssem, rsem, lsem,
     ):
         r = lax.axis_index("rep")
         j = lax.axis_index("fs_0")
@@ -66,6 +69,9 @@
 
         def ydev(d):
             return {"fs_1": at(y, d)}
+
+        def yzdev(d):
+            return {"fs_0": 1 - j, "fs_1": at(y, d)}
 
         zpeer = {"fs_0": 1 - j}
         rpeer = {"rep": 1 - r}
@@ -86,12 +92,18 @@
             c.start()
 
         barrier = pltpu.get_barrier_semaphore()
-        peers = [xdev(1), xdev(2), xdev(3), ydev(1), ydev(2), ydev(3), zpeer, rpeer, rzpeer, tpeer]
+        peers = [xdev(1), xdev(2), xdev(3), ydev(1), ydev(2), ydev(3), zpeer, rpeer, rzpeer, tpeer, yzdev(1), yzdev(2), yzdev(3)]
         for dev in peers:
             pl.semaphore_signal(barrier, inc=1, device_id=dev, device_id_type=MESH)
         pl.semaphore_wait(barrier, len(peers))
 
         copies = {}
+        stores = []
+
+        def store(src, dst):
+            c = pltpu.make_async_copy(src, dst, lsem.at[6 + len(stores)])
+            c.start()
+            stores.append(c)
 
         def send(key, src, dst, dev):
             n = len(copies)
@@ -213,12 +225,27 @@
         def raxes(h):
             return (y, x, ydev, xdev) if h == 0 else (x, y, xdev, ydev)
 
+        def product(w, h, lo, n):
+            z = j if h == 0 else 1 - j
+            left = lhs_of[w][z, :, :, :, lo * tokens:(lo + n) * tokens].reshape(width // 2, n * tokens)
+            right = rhs_of[w][lo:lo + n].reshape(n * tokens, cols)
+            out = jnp.dot(left, right, preferred_element_type=F32)
+            return G.at[w, z], out.reshape(4, 4, width // 32, cols)
+
+        begun = set()
+
+        def multiply_early(w, h):
+            ref, out = product(w, h, 0, 2)
+            ref[...] = out
+            begun.add((w, h))
+
         def multiply(w, h):
-            z = j if h == 0 else 1 - j
-            rows = 4 * (width // 32)
-            left = lhs_of[w][z].reshape(4 * rows, 4 * tokens)
-            out = jnp.dot(left, rhs_of[w][...].reshape(4 * tokens, cols), preferred_element_type=F32)
-            G[w, z] = out.reshape(4, 4, width // 32, cols)
+            if (w, h) in begun:
+                ref, out = product(w, h, 2, 2)
+                ref[...] = ref[...] + out
+            else:
+                ref, out = product(w, h, 0, 4)
+                ref[...] = out
 
         def encode(srcs, dst, scale, steps=3):
             top = None
@@ -244,51 +271,55 @@
             return m.reshape(v.shape)
 
         class Ring:
-            def __init__(self, stage, w, h, pos, dev, parts, bufs):
+            def __init__(self, stage, w, h, pos, dev, parts, bufs, subs):
                 self.k = (stage, w, h)
+                self.subs = subs
                 self.pos, self.dev, self.parts = pos, dev, parts
                 self.sb, self.rb, self.sc, self.rc = (b.at[2 * w + h] for b in bufs)
 
-            def post(self, i, srcs, d):
-                encode(srcs, self.sb.at[i], self.sc.at[i])
-                send(self.k + (i, "s"), self.sc.at[i], self.rc.at[i], self.dev(d))
-                send(self.k + (i, "v"), self.sb.at[i], self.rb.at[i], self.dev(d))
-
-            def take(self, i, refs):
-                recv(self.k + (i, "s"))
-                recv(self.k + (i, "v"))
-                for n, ref in enumerate(refs):
+            def post(self, i, srcs, d, lo, n):
+                for m in range(lo, lo + n):
+                    encode([srcs[m]], self.sb.at[i, pl.ds(m, 1)], self.sc.at[i, m])
+                at_ = pl.ds(lo, n)
+                send(self.k + (i, lo, "s"), self.sc.at[i, at_], self.rc.at[i, at_], self.dev(d))
+                send(self.k + (i, lo, "v"), self.sb.at[i, at_], self.rb.at[i, at_], self.dev(d))
+
+            def take(self, i, refs, lo, n):
+                recv(self.k + (i, lo, "s"))
+                recv(self.k + (i, lo, "v"))
+                for m in range(lo, lo + n):
                     for c in lanes:
-                        ref[:, c] = ref[:, c] + decode(self.rb.at[i], self.rc.at[i], n, c)
-
-            def far(self):
-                self.post(0, self.parts(at(self.pos, 2), 0), 1)
-                self.post(1, self.parts(at(self.pos, 2), 1), 3)
+                        refs[m][:, c] = refs[m][:, c] + decode(self.rb.at[i], self.rc.at[i, m], m, c)
+
+            def far(self, lo=0, n=1):
+                self.post(0, self.parts(at(self.pos, 2), 0), 1, lo, n)
+                self.post(1, self.parts(at(self.pos, 2), 1), 3, lo, n)
 
             def near_right(self):
-                self.post(2, self.parts(at(self.pos, 1), 1), 1)
+                self.post(2, self.parts(at(self.pos, 1), 1), 1, 0, self.subs)
 
             def near_left(self):
-                self.post(3, self.parts(at(self.pos, 3), 0), 3)
-
-            def relay(self, side):
+                self.post(3, self.parts(at(self.pos, 3), 0), 3, 0, self.subs)
+
+            def relay(self, side, lo=0, n=1):
                 p = self.parts(at(self.pos, (1, 3)[side]), side)
-                self.take(side, p)
-                self.post(4 + side, p, (1, 3)[side])
+                self.take(side, p, lo, n)
+                self.post(4 + side, p, (1, 3)[side], lo, n)
 
             def near_in(self):
-                self.take(3, self.parts(self.pos, 0))
-                self.take(2, self.parts(self.pos, 1))
+                self.take(3, self.parts(self.pos, 0), 0, self.subs)
+                self.take(2, self.parts(self.pos, 1), 0, self.subs)
 
             def last_in(self):
-                self.take(4, self.parts(self.pos, 0))
-                self.take(5, self.parts(self.pos, 1))
+                for lo in range(self.subs):
+                    self.take(4, self.parts(self.pos, 0), lo, 1)
+                    self.take(5, self.parts(self.pos, 1), lo, 1)
 
         def ring1(w, h):
             a, b, adev, bdev = raxes(h)
             return Ring(1, w, h, a, adev,
                         lambda place, side: [gblk(w, h, place, 2 * side + i) for i in (0, 1)],
-                        (s1s, s1r, c1s, c1r))
+                        (s1s, s1r, c1s, c1r), 2)
 
         hr = width // 64
 
@@ -296,7 +327,7 @@
             a, b, adev, bdev = raxes(h)
             return Ring(2, w, h, b, bdev,
                         lambda place, side: [gblk(w, h, a, place).at[pl.ds(side * hr, hr)]],
-                        (s2s, s2r, c2s, c2r))
+                        (s2s, s2r, c2s, c2r), 1)
 
         first = {(w, h): ring1(w, h) for w in (UP, DN) for h in (0, 1)}
         second = {(w, h): ring2(w, h) for w in (UP, DN) for h in (0, 1)}
@@ -330,6 +361,7 @@
                 theirs = decode(s3r.at[w, 1], c3r.at[w, 1], 0, lane)
                 theirs = theirs + decode(s3r.at[w, 2], c3r.at[w, 2], 0, lane)
                 out[:, pl.ds(pl.multiple_of((1 - j) * cols + c * 128, 128), 128)] = theirs * factor
+            store(out, (gup_out, gdn_out)[w])
 
         def input_part(n):
             s1, s2 = ((3, 1), (2, 0))[n]
@@ -355,6 +387,7 @@
             for c in lanes:
                 far = decode(ZR, zsc.at[1], 0, c, 4)
                 gin_ref[:, c] = (PART[0, :, c] + DR[1, :, c] + far).astype(BF)
+            store(gin_ref, gin_out)
 
         def energy_x():
             EX[x] = jnp.sum(gdn_ref[...] * gdn_ref[...], axis=0, keepdims=True)
@@ -364,19 +397,19 @@
         def energy_y():
             for d in (1, 2, 3):
                 recv(("e", "x", d))
-            EY[y] = EX[0] + EX[1] + EX[2] + EX[3]
+            EY[j, y] = EX[0] + EX[1] + EX[2] + EX[3]
+            send(("e", "y", 4), EY.at[j, y], EY.at[j, y], zpeer)
             for d in (1, 2, 3):
-                send(("e", "y", d), EY.at[y], EY.at[y], ydev(d))
-
-        def energy_z():
-            for d in (1, 2, 3):
+                send(("e", "y", d), EY.at[j, y], EY.at[j, y], ydev(d))
+                send(("e", "y", 4 + d), EY.at[j, y], EY.at[j, y], yzdev(d))
+
+        def energy_down():
+            for d in range(1, 8):
                 recv(("e", "y", d))
-            EZ[0] = EY[0] + EY[1] + EY[2] + EY[3]
-            send(("e", "z"), EZ.at[0], EZ.at[1], zpeer)
-
-        def energy_down():
-            recv(("e", "z"))
-            edn_ref[...] = (EZ[0] + EZ[1]) * (1.0 / width)
+            total = EY[0, 0]
+            for n in range(1, 8):
+                total = total + EY[n // 4, n % 4]
+            edn_ref[...] = total * (1.0 / width)
 
         def energy_pair():
             total = None
@@ -404,22 +437,29 @@
             send((name, "t"), buf.at[0], buf.at[1], tpeer)
         todo = {
             "init": init, "near": near, "step2": step2, "fwd": fwd, "pass": pass_on, "turn": turn,
-            "proj": project, "pull": pull_back, "mult": multiply,
-            "far": lambda w, h: first[w, h].far(),
+            "proj": project, "pull": pull_back, "mult": multiply, "ma": multiply_early,
+            "far": lambda w, h, lo: first[w, h].far(lo),
             "nr": lambda w, h: first[w, h].near_right(),
             "nl": lambda w, h: first[w, h].near_left(),
-            "rl": lambda w, h, side: first[w, h].relay(side),
+            "rl": lambda w, h, side, lo: first[w, h].relay(side, lo),
             "ni": lambda w, h: first[w, h].near_in(),
             "st2": second_start,
             "rl2": lambda w, h, side: second[w, h].relay(side),
             "st3": third_start, "fin": finish, "ip": input_part, "gz": input_send, "gin": input_sum,
-            "ex": energy_x, "ey": energy_y, "ez": energy_z, "edn": energy_down,
+            "ex": energy_x, "ey": energy_y, "edn": energy_down,
             "eu": energy_pair, "eup": energy_up,
         }
+        drained, marks = 0, [0] * LAG
         for name, *where in ORDER:
             todo[name](*where)
-        for c in copies.values():
-            c.wait_send()
+            marks.append(len(copies))
+            for key in list(copies)[drained:marks[-LAG]]:
+                copies[key].wait_send()
+            drained = max(drained, marks[-LAG])
+        for key in list(copies)[drained:]:
+            copies[key].wait_send()
+        for c in stores:
+            c.wait()
 
     return kernel
 
@@ -458,7 +498,7 @@
             jax.ShapeDtypeStruct((1, hidden), F32),
         ),
         in_specs=[pl.BlockSpec(memory_space=pl.ANY)] * 4,
-        out_specs=(vm,) * 5,
+        out_specs=(pl.BlockSpec(memory_space=pl.ANY),) * 3 + (vm, vm),
         scratch_shapes=[
             pltpu.VMEM((4, tokens, width), BF),
             pltpu.VMEM((4, tokens, width), BF),
@@ -471,12 +511,12 @@
             pltpu.VMEM((2,) + full + (cols,), F32),
             pltpu.VMEM((4, 6, 2, rows, cols), BF),
             pltpu.VMEM((4, 6, 2, rows, cols), BF),
-            pltpu.VMEM((4, 6, 8, 128), F32),
-            pltpu.VMEM((4, 6, 8, 128), F32),
+            pltpu.VMEM((4, 6, 2, 8, 128), F32),
+            pltpu.VMEM((4, 6, 2, 8, 128), F32),
             pltpu.VMEM((4, 6, 1, rows // 2, cols), BF),
             pltpu.VMEM((4, 6, 1, rows // 2, cols), BF),
-            pltpu.VMEM((4, 6, 8, 128), F32),
-            pltpu.VMEM((4, 6, 8, 128), F32),
+            pltpu.VMEM((4, 6, 1, 8, 128), F32),
+            pltpu.VMEM((4, 6, 1, 8, 128), F32),
             pltpu.VMEM((2, 2, 1, rows, cols), BF),
             pltpu.VMEM((2, 3, 1, rows, cols), BF),
             pltpu.VMEM((2, 2, 8, 128), F32),
@@ -487,13 +527,15 @@
             pltpu.VMEM((1, tokens, width), BF),
             pltpu.VMEM((2, 8, 128), F32),
             pltpu.VMEM((4, 1, hidden), F32),
-            pltpu.VMEM((4, 1, hidden), F32),
-            pltpu.VMEM((2, 1, hidden), F32),
+            pltpu.VMEM((2, 4, 1, hidden), F32),
             pltpu.VMEM((2, rows, 128), F32),
             pltpu.VMEM((2, 2, rows // 2, cols), BF),
+            pltpu.VMEM((tokens, width), BF),
+            pltpu.VMEM((rows, hidden), F32),
+            pltpu.VMEM((rows, hidden), F32),
             pltpu.SemaphoreType.DMA((COPIES,)),
             pltpu.SemaphoreType.DMA((COPIES,)),
-            pltpu.SemaphoreType.DMA((6,)),
+            pltpu.SemaphoreType.DMA((9,)),
         ],
         compiler_params=pltpu.CompilerParams(
             collective_id=0, has_side_effects=True, vmem_limit_bytes=63 * 1024 * 1024

time: 82.7 us -> 88.3 us (1.068)
  Pallas kernels: 81.9 us -> 87.5 us
    pallas_call x1, Pallas kernels: 79.7 us -> 85.4 us  [per_device(): pl.pallas_call(make_kernel(tokens, width, cols, ff, factor), out_shape=(j...]
where the time goes in v4:
time: 88.3 us; the launch traced here: 88.2 us
  Pallas kernels  87.5 us (99%)
    pallas_call x1, Pallas kernels, per_device(): pl.pallas_call(make_kernel(tokens, width, cols, ff, factor), out_shape=(j...  85.4 us
    pallas_call x1, Pallas kernels, hand_over(): pl.pallas_call(kernel, out_shape=tuple(shapes), in_specs=[vm] * 5, out_sp...  2.18 us

profile of v4, /device:TPU:1, one launch (start us, length us, event | category | flops | bytes accessed | tf_op | source)
XLA Modules:
  0.0 88.2 jit_solution(11070879154965666331)
XLA Ops:
  0.6 85.4 %shard_map.83 = (bf16[256,1024]{1,0:T(8,128)(2,1)}, f32[32,2048]{1,0:T(8,128)}, f32[32,2048]{1,0:T(8,128)}, f32[1,32]{1,0:T(1,128)}, f32[1,2048]{1,0:T(1,128)}) custom-call(bf16[256,1024]{1,0:T(8,128)(2,1)} %x_ref.1, bf16[2,16,2048]{2,1,0:T(8,128)(2,1)} %bitcast.6, bf16[2,16,2048]{2,1,0:T(8,128)(2,1)} %bitcast.7, bf16[256,1024]{1,0:T(8,128)(2,1)} %cot_ref.1), custom_call_target="tpu_custom_call" | custom-call | tf_op jit(solution)/shard_map/pallas_call | solution.py:491
  86.0 2.2 %shard_map.84 = (bf16[256,1024]{1,0:T(8,128)(2,1)}, f32[32,2048]{1,0:T(8,128)}, f32[32,2048]{1,0:T(8,128)}, f32[1,32]{1,0:T(1,128)}, f32[2048]{0:T(1024)}) custom-call(bf16[256,1024]{1,0:T(8,128)(2,1)} %get-tuple-element.15.refs_0_, f32[32,2048]{1,0:T(8,128)} %get-tuple-element.16.refs_1_, f32[32,2048]{1,0:T(8,128)} %get-tuple-element.17.refs_2_, ...), custom_call_target="tpu_custom_call" | custom-call | tf_op jit(solution)/shard_map/pallas_call | solution.py:477

commit v5 on v4

--- a/solution.py
+++ b/solution.py
@@ -13,8 +13,7 @@
 F32 = jnp.float32
 RIGHT, LEFT = 0, 1
 UP, DN = 0, 1
-COPIES = 280
-LAG = 30
+WAITS, BATCHES = 110, 26
 
 
 ORDER = [
@@ -51,8 +50,8 @@
         x_ref, up_ref, dn_ref, cot_ref,
         gin_out, gup_out, gdn_out, eup_ref, edn_ref,
         X, C, XT, CT, W, RP, ACT, GP, G,
-        s1s, s1r, c1s, c1r, s2s, s2r, c2s, c2r, s3s, s3r, c3s, c3r,
-        PART, DR, ZS, ZR, zsc, EX, EY, EU,
+        s1s, s1r, s2s, s2r, s3s, s3r,
+        PART, DR, ZS, ZR, EX, EY, EU,
         OTH, gin_ref, gup_ref, gdn_ref, ssem, rsem, lsem,
     ):
         r = lax.axis_index("rep")
@@ -97,7 +96,6 @@
             pl.semaphore_signal(barrier, inc=1, device_id=dev, device_id_type=MESH)
         pl.semaphore_wait(barrier, len(peers))
 
-        copies = {}
         stores = []
 
         def store(src, dst):
@@ -105,17 +103,23 @@
             c.start()
             stores.append(c)
 
-        def send(key, src, dst, dev):
-            n = len(copies)
-            c = pltpu.make_async_remote_copy(
-                src_ref=src, dst_ref=dst, send_sem=ssem.at[n], recv_sem=rsem.at[n],
+        arrivals, departures = {}, {}
+
+        def slot_of(table, group):
+            return table.setdefault(group, len(table))
+
+        def send(group, src, dst, dev, batch):
+            pltpu.make_async_remote_copy(
+                src_ref=src, dst_ref=dst,
+                send_sem=ssem.at[slot_of(departures, batch)], recv_sem=rsem.at[slot_of(arrivals, group)],
                 device_id=dev, device_id_type=MESH,
-            )
-            c.start()
-            copies[key] = c
-
-        def recv(key):
-            copies[key].wait_recv()
+            ).start()
+
+        def recv(group, ref):
+            pltpu.make_async_copy(ref, ref, rsem.at[arrivals[group]]).wait()
+
+        def sent(batch, ref):
+            pltpu.make_async_copy(ref, ref, ssem.at[departures[batch]]).wait()
 
         half = tokens // 2
 
@@ -128,68 +132,61 @@
 
         def init(w, h):
             a, b, adev, bdev = axes(h)
+            ref = blk(W, w, h, a, b)
             if h == 1:
-                recv(("a2a", w))
-            src = dst = blk(W, w, h, a, b)
-            send((1, w, h, 0), src, dst, adev(1))
-            send((1, w, h, 1), src, dst, adev(3))
-            send((2, w, h, 0, 0), src, dst, bdev(1))
-            send((2, w, h, 0, 1), src, dst, bdev(3))
+                recv(("a2a", w), ref)
+            send((1, w, h, 0), ref, ref, adev(1), (w, h))
+            send((1, w, h, 1), ref, ref, adev(3), (w, h))
+            spread(w, h, 0, a)
 
         def spread(w, h, s, a2):
             _, b, _, bdev = axes(h)
             ref = blk(W, w, h, a2, b)
-            send((2, w, h, s, 0), ref, ref, bdev(1))
-            send((2, w, h, s, 1), ref, ref, bdev(3))
+            send((2, w, h, s, 0), ref, ref, bdev(1), (w, h))
+            send((2, w, h, s, 1), ref, ref, bdev(3), (w, h))
 
         def near(w, h, side):
             a, b, adev, _ = axes(h)
-            recv((1, w, h, side))
             place, away = ((at(a, 3), 1), (at(a, 1), 3))[side]
-            ref = blk(W, w, h, place, b).at[side]
-            send((1, w, h, 2 + side), ref, ref, adev(away))
+            ref = blk(W, w, h, place, b)
+            recv((1, w, h, side), ref)
+            send((1, w, h, 2), ref.at[side], ref.at[side], adev(away), (w, h))
             spread(w, h, 1 + side, place)
 
         def step2(w, h):
-            a = axes(h)[0]
-            recv((1, w, h, 2))
-            recv((1, w, h, 3))
+            a, b, _, _ = axes(h)
+            recv((1, w, h, 2), blk(W, w, h, at(a, 2), b))
             spread(w, h, 3, at(a, 2))
 
         def fwd(w, h, s, side):
             a, b, _, bdev = axes(h)
             a2 = at(a, (0, 3, 1, 2)[s])
-            recv((2, w, h, s, side))
             place, away = ((at(b, 3), 1), (at(b, 1), 3))[side]
-            ref = blk(W, w, h, a2, place).at[side]
-            send((2, w, h, s, 2 + side), ref, ref, bdev(away))
+            ref = blk(W, w, h, a2, place)
+            recv((2, w, h, s, side), ref)
+            send((3, w), ref.at[side], ref.at[side], bdev(away), (w, h))
 
         whole = set()
 
         def fin(w):
-            if w in whole:
-                return
-            whole.add(w)
-            for h in (0, 1):
-                for s in range(4):
-                    recv((2, w, h, s, 2))
-                    recv((2, w, h, s, 3))
+            if w not in whole:
+                whole.add(w)
+                recv((3, w), W.at[w, 0, pl.ds(0, 2)])
 
         stock = {"x": (X, XT), "c": (C, CT)}
 
         def pass_on(name, i):
-            recv((name, "z", i))
             rows = pl.ds(i * half, half)
             buf = stock[name][0]
-            send((name, "zt", i), buf.at[2, rows], buf.at[3, rows], tpeer)
+            recv((name, "z", i), buf.at[2, rows])
+            send((name, "zt"), buf.at[2, rows], buf.at[3, rows], tpeer, (name, "zt"))
 
         def turn(name, slot):
+            src, dst = stock[name]
             if slot == 1:
-                recv((name, "t"))
+                recv((name, "t"), src.at[1])
             if slot == 3:
-                recv((name, "zt", 0))
-                recv((name, "zt", 1))
-            src, dst = stock[name]
+                recv((name, "zt"), src.at[3])
             v = src[slot].T
             dst[:, :, :, :, slot * tokens:(slot + 1) * tokens] = v.reshape(2, 4, 4, width // 32, tokens)
 
@@ -247,79 +244,86 @@
                 ref, out = product(w, h, 0, 4)
                 ref[...] = out
 
-        def encode(srcs, dst, scale, steps=3):
+        def tiles(rows):
+            return [(n, pl.ds(16 * (n % (rows // 16)), 16), lanes[n // (rows // 16)])
+                    for n in range(rows // 16 * len(lanes))]
+
+        def encode(src, dst, steps=3):
+            every = tiles(src.shape[0])
             top = None
-            for src in srcs:
-                for c in lanes:
-                    m = jnp.max(jnp.abs(src[:, c]).reshape(-1, 8, 128), axis=0)
-                    top = m if top is None else jnp.maximum(top, m)
-            top = jnp.maximum(top, 2e-34)
-            scale[...] = top
-            inv = 2.0 ** (120 >> steps) / top
-            for i, src in enumerate(srcs):
-                for c in lanes:
-                    v = src[:, c]
-                    v3 = v.reshape(-1, 8, 128) * inv
-                    for _ in range(steps):
-                        v3 = v3 * jnp.abs(v3)
-                    dst[i, :, c] = v3.reshape(v.shape).astype(BF)
-
-        def decode(buf, scale, i, c, steps=3):
-            v = buf[i, :, c].astype(F32)
-            m = jnp.exp2(jnp.log2(jnp.abs(v)) * 0.5 ** steps)
-            m = jnp.where(v < 0, -m, m).reshape(-1, 8, 128) * (scale[...] * 0.5 ** (120 >> steps))
-            return m.reshape(v.shape)
+            for _, q, c in every:
+                m = jnp.abs(src[q, c])
+                top = m if top is None else jnp.maximum(top, m)
+            top = jnp.maximum(top, 2e-34).astype(BF)
+            dst[len(every)] = top
+            inv = 2.0 ** (120 >> steps) / top.astype(F32)
+            for n, q, c in every:
+                v = src[q, c] * inv
+                for _ in range(steps):
+                    v = v * jnp.abs(v)
+                dst[n] = v.astype(BF)
+
+        def decoder(buf, rows, steps=3):
+            every = tiles(rows)
+            unit = buf[len(every)].astype(F32) * 0.5 ** (120 >> steps)
+
+            def tile(n):
+                v = buf[n].astype(F32)
+                m = jnp.exp2(jnp.log2(jnp.abs(v)) * 0.5 ** steps)
+                return jnp.where(v < 0, -m, m) * unit
+            return every, tile
+
+        def add(ref, buf):
+            every, tile = decoder(buf, ref.shape[0])
+            for n, q, c in every:
+                ref[q, c] = ref[q, c] + tile(n)
 
         class Ring:
             def __init__(self, stage, w, h, pos, dev, parts, bufs, subs):
                 self.k = (stage, w, h)
                 self.subs = subs
                 self.pos, self.dev, self.parts = pos, dev, parts
-                self.sb, self.rb, self.sc, self.rc = (b.at[2 * w + h] for b in bufs)
-
-            def post(self, i, srcs, d, lo, n):
+                self.sb, self.rb = (b.at[2 * w + h] for b in bufs)
+
+            def post(self, i, srcs, d, lo, n, group):
                 for m in range(lo, lo + n):
-                    encode([srcs[m]], self.sb.at[i, pl.ds(m, 1)], self.sc.at[i, m])
-                at_ = pl.ds(lo, n)
-                send(self.k + (i, lo, "s"), self.sc.at[i, at_], self.rc.at[i, at_], self.dev(d))
-                send(self.k + (i, lo, "v"), self.sb.at[i, at_], self.rb.at[i, at_], self.dev(d))
-
-            def take(self, i, refs, lo, n):
-                recv(self.k + (i, lo, "s"))
-                recv(self.k + (i, lo, "v"))
-                for m in range(lo, lo + n):
-                    for c in lanes:
-                        refs[m][:, c] = refs[m][:, c] + decode(self.rb.at[i], self.rc.at[i, m], m, c)
-
-            def far(self, lo=0, n=1):
-                self.post(0, self.parts(at(self.pos, 2), 0), 1, lo, n)
-                self.post(1, self.parts(at(self.pos, 2), 1), 3, lo, n)
+                    encode(srcs[m], self.sb.at[i, m])
+                some = pl.ds(lo, n)
+                send(self.k + group, self.sb.at[i, some], self.rb.at[i, some], self.dev(d), self.k)
+
+            def far(self, lo=0):
+                self.post(0, self.parts(at(self.pos, 2), 0), 1, lo, 1, ("far", 0, lo))
+                self.post(1, self.parts(at(self.pos, 2), 1), 3, lo, 1, ("far", 1, lo))
 
             def near_right(self):
-                self.post(2, self.parts(at(self.pos, 1), 1), 1, 0, self.subs)
+                self.post(2, self.parts(at(self.pos, 1), 1), 1, 0, self.subs, ("near",))
 
             def near_left(self):
-                self.post(3, self.parts(at(self.pos, 3), 0), 3, 0, self.subs)
-
-            def relay(self, side, lo=0, n=1):
+                self.post(3, self.parts(at(self.pos, 3), 0), 3, 0, self.subs, ("near",))
+
+            def relay(self, side, lo=0):
                 p = self.parts(at(self.pos, (1, 3)[side]), side)
-                self.take(side, p, lo, n)
-                self.post(4 + side, p, (1, 3)[side], lo, n)
+                recv(self.k + ("far", side, lo), self.rb.at[side, pl.ds(lo, 1)])
+                add(p[lo], self.rb.at[side, lo])
+                self.post(4 + side, p, (1, 3)[side], lo, 1, ("last", lo))
 
             def near_in(self):
-                self.take(3, self.parts(self.pos, 0), 0, self.subs)
-                self.take(2, self.parts(self.pos, 1), 0, self.subs)
+                recv(self.k + ("near",), self.rb.at[pl.ds(2, 2)])
+                for m in range(self.subs):
+                    add(self.parts(self.pos, 0)[m], self.rb.at[3, m])
+                    add(self.parts(self.pos, 1)[m], self.rb.at[2, m])
 
             def last_in(self):
-                for lo in range(self.subs):
-                    self.take(4, self.parts(self.pos, 0), lo, 1)
-                    self.take(5, self.parts(self.pos, 1), lo, 1)
+                for m in range(self.subs):
+                    recv(self.k + ("last", m), self.rb.at[pl.ds(4, 2), m])
+                    add(self.parts(self.pos, 0)[m], self.rb.at[4, m])
+                    add(self.parts(self.pos, 1)[m], self.rb.at[5, m])
 
         def ring1(w, h):
             a, b, adev, bdev = raxes(h)
             return Ring(1, w, h, a, adev,
                         lambda place, side: [gblk(w, h, place, 2 * side + i) for i in (0, 1)],
-                        (s1s, s1r, c1s, c1r), 2)
+                        (s1s, s1r), 2)
 
         hr = width // 64
 
@@ -327,7 +331,7 @@
             a, b, adev, bdev = raxes(h)
             return Ring(2, w, h, b, bdev,
                         lambda place, side: [gblk(w, h, a, place).at[pl.ds(side * hr, hr)]],
-                        (s2s, s2r, c2s, c2r), 1)
+                        (s2s, s2r), 1)
 
         first = {(w, h): ring1(w, h) for w in (UP, DN) for h in (0, 1)}
         second = {(w, h): ring2(w, h) for w in (UP, DN) for h in (0, 1)}
@@ -342,25 +346,20 @@
             second[w, h].near_in()
             second[w, h].last_in()
             a, b, _, _ = raxes(h)
-            encode([gblk(w, h, a, b)], s3s.at[w, h], c3s.at[w, h])
+            encode(gblk(w, h, a, b), s3s.at[w, h])
             peers_ = [(0, rpeer)] if h == 0 else [(1, zpeer), (2, rzpeer)]
             for i, dev in peers_:
-                send((3, w, i, "s"), c3s.at[w, h], c3r.at[w, i], dev)
-                send((3, w, i, "v"), s3s.at[w, h], s3r.at[w, i], dev)
+                send((5, w), s3s.at[w, h], s3r.at[w, i], dev, (5, w))
 
         def finish(w):
             out = (gup_ref, gdn_ref)[w]
-            for i in range(3):
-                recv((3, w, i, "s"))
-                recv((3, w, i, "v"))
-            for c in range(len(lanes)):
-                lane = lanes[c]
-                mine = decode(s3s.at[w, 0], c3s.at[w, 0], 0, lane)
-                mine = mine + decode(s3r.at[w, 0], c3r.at[w, 0], 0, lane)
-                out[:, pl.ds(pl.multiple_of(j * cols + c * 128, 128), 128)] = mine * factor
-                theirs = decode(s3r.at[w, 1], c3r.at[w, 1], 0, lane)
-                theirs = theirs + decode(s3r.at[w, 2], c3r.at[w, 2], 0, lane)
-                out[:, pl.ds(pl.multiple_of((1 - j) * cols + c * 128, 128), 128)] = theirs * factor
+            recv((5, w), s3r.at[w])
+            for side, one, two in ((j, s3s.at[w, 0], s3r.at[w, 0]), (1 - j, s3r.at[w, 1], s3r.at[w, 2])):
+                every, tile1 = decoder(one, width // 32)
+                _, tile2 = decoder(two, width // 32)
+                for n, q, c in every:
+                    col = pl.ds(pl.multiple_of(side * cols + n // (width // 512) * 128, 128), 128)
+                    out[q, col] = (tile1(n) + tile2(n)) * factor
             store(out, (gup_out, gdn_out)[w])
 
         def input_part(n):
@@ -371,44 +370,39 @@
             PART[s2] = v[tokens:]
             if n == 0:
                 for i, slot in enumerate((3, 1)):
-                    send(("g", "t", i), PART.at[slot], DR.at[i], tpeer)
+                    send(("g", "t", i), PART.at[slot], DR.at[i], tpeer, "gt")
 
         def input_send():
-            recv(("g", "t", 0))
+            recv(("g", "t", 0), DR.at[0])
             PART[2] = PART[2] + DR[0]
-            encode([PART.at[2]], ZS, zsc.at[0], 4)
-            send(("g", "zs"), zsc.at[0], zsc.at[1], zpeer)
-            send(("g", "z"), ZS, ZR, zpeer)
+            encode(PART.at[2], ZS, 4)
+            send("gz", ZS, ZR, zpeer, "gz")
 
         def input_sum():
-            recv(("g", "t", 1))
-            recv(("g", "zs"))
-            recv(("g", "z"))
-            for c in lanes:
-                far = decode(ZR, zsc.at[1], 0, c, 4)
-                gin_ref[:, c] = (PART[0, :, c] + DR[1, :, c] + far).astype(BF)
+            recv(("g", "t", 1), DR.at[1])
+            recv("gz", ZR)
+            every, tile = decoder(ZR, tokens, 4)
+            for n, q, c in every:
+                gin_ref[q, c] = (PART[0, q, c] + DR[1, q, c] + tile(n)).astype(BF)
             store(gin_ref, gin_out)
 
         def energy_x():
             EX[x] = jnp.sum(gdn_ref[...] * gdn_ref[...], axis=0, keepdims=True)
             for d in (1, 2, 3):
-                send(("e", "x", d), EX.at[x], EX.at[x], xdev(d))
+                send("ex", EX.at[x], EX.at[x], xdev(d), "ex")
 
         def energy_y():
-            for d in (1, 2, 3):
-                recv(("e", "x", d))
-            EY[j, y] = EX[0] + EX[1] + EX[2] + EX[3]
-            send(("e", "y", 4), EY.at[j, y], EY.at[j, y], zpeer)
-            for d in (1, 2, 3):
-                send(("e", "y", d), EY.at[j, y], EY.at[j, y], ydev(d))
-                send(("e", "y", 4 + d), EY.at[j, y], EY.at[j, y], yzdev(d))
+            recv("ex", EX.at[pl.ds(0, 3)])
+            me = 4 * j + y
+            EY[me] = EX[0] + EX[1] + EX[2] + EX[3]
+            for dev in [zpeer] + [f(d) for d in (1, 2, 3) for f in (ydev, yzdev)]:
+                send("ey", EY.at[me], EY.at[me], dev, "ey")
 
         def energy_down():
-            for d in range(1, 8):
-                recv(("e", "y", d))
-            total = EY[0, 0]
+            recv("ey", EY.at[pl.ds(0, 7)])
+            total = EY[0]
             for n in range(1, 8):
-                total = total + EY[n // 4, n % 4]
+                total = total + EY[n]
             edn_ref[...] = total * (1.0 / width)
 
         def energy_pair():
@@ -417,24 +411,23 @@
                 v = gup_ref[:, c * 128:(c + 1) * 128]
                 total = v * v if total is None else total + v * v
             EU[0] = total
-            send(("e", "t"), EU.at[0], EU.at[1], tpeer)
+            send("et", EU.at[0], EU.at[1], tpeer, "et")
 
         def energy_up():
-            recv(("e", "t"))
+            recv("et", EU.at[1])
             eup_ref[...] = jnp.sum((EU[0] + EU[1]).T, axis=0, keepdims=True) * (1.0 / ff)
 
-        loads[0].wait()
-        send(("a2a", UP), OTH.at[UP], W.at[UP, j, y, x], rzpeer)
-        loads[1].wait()
-        send(("a2a", DN), OTH.at[DN], W.at[DN, j, y, x], rzpeer)
+        for w in (UP, DN):
+            loads[w].wait()
+            send(("a2a", w), OTH.at[w], W.at[w, j, y, x], rzpeer, "a2a")
         for c in loads[2:]:
             c.wait()
         for name in ("x", "c"):
             buf = stock[name][0]
             for i in (0, 1):
                 rows = pl.ds(i * half, half)
-                send((name, "z", i), buf.at[0, rows], buf.at[2, rows], zpeer)
-            send((name, "t"), buf.at[0], buf.at[1], tpeer)
+                send((name, "z", i), buf.at[0, rows], buf.at[2, rows], zpeer, name)
+            send((name, "t"), buf.at[0], buf.at[1], tpeer, name)
         todo = {
             "init": init, "near": near, "step2": step2, "fwd": fwd, "pass": pass_on, "turn": turn,
             "proj": project, "pull": pull_back, "mult": multiply, "ma": multiply_early,
@@ -449,15 +442,22 @@
             "ex": energy_x, "ey": energy_y, "edn": energy_down,
             "eu": energy_pair, "eup": energy_up,
         }
-        drained, marks = 0, [0] * LAG
         for name, *where in ORDER:
             todo[name](*where)
-            marks.append(len(copies))
-            for key in list(copies)[drained:marks[-LAG]]:
-                copies[key].wait_send()
-            drained = max(drained, marks[-LAG])
-        for key in list(copies)[drained:]:
-            copies[key].wait_send()
+        sent("a2a", OTH)
+        for n, name in enumerate(("x", "c")):
+            sent(name, RP.at[0])
+            sent((name, "zt"), X.at[0])
+            for h in (0, 1):
+                sent((n, h), RP.at[0, pl.ds(0, 15 * tokens // 16)])
+                sent((1, n, h), s1s.at[0])
+                sent((2, n, h), s2s.at[0])
+            sent((5, n), s3r.at[0])
+        sent("gt", PART.at[pl.ds(0, 2)])
+        sent("gz", ZS)
+        sent("ex", EX.at[pl.ds(0, 3)])
+        sent("ey", EY.at[pl.ds(0, 7)])
+        sent("et", EU.at[0])
         for c in stores:
             c.wait()
 
@@ -488,6 +488,7 @@
     dn3 = down_proj.T.reshape(2, rows // 2, hidden)
     vm = pl.BlockSpec(memory_space=pltpu.VMEM)
     full = (2, 4, 4, rows)
+    lines = rows * cols // 2048
     results = pl.pallas_call(
         make_kernel(tokens, width, cols, ff, factor),
         out_shape=(
@@ -509,32 +510,25 @@
             pltpu.VMEM((4, tokens, cols), BF),
             pltpu.VMEM((4, tokens, cols), BF),
             pltpu.VMEM((2,) + full + (cols,), F32),
-            pltpu.VMEM((4, 6, 2, rows, cols), BF),
-            pltpu.VMEM((4, 6, 2, rows, cols), BF),
-            pltpu.VMEM((4, 6, 2, 8, 128), F32),
-            pltpu.VMEM((4, 6, 2, 8, 128), F32),
-            pltpu.VMEM((4, 6, 1, rows // 2, cols), BF),
-            pltpu.VMEM((4, 6, 1, rows // 2, cols), BF),
-            pltpu.VMEM((4, 6, 1, 8, 128), F32),
-            pltpu.VMEM((4, 6, 1, 8, 128), F32),
-            pltpu.VMEM((2, 2, 1, rows, cols), BF),
-            pltpu.VMEM((2, 3, 1, rows, cols), BF),
-            pltpu.VMEM((2, 2, 8, 128), F32),
-            pltpu.VMEM((2, 3, 8, 128), F32),
+            pltpu.VMEM((4, 6, 2, lines + 1, 16, 128), BF),
+            pltpu.VMEM((4, 6, 2, lines + 1, 16, 128), BF),
+            pltpu.VMEM((4, 6, 1, lines // 2 + 1, 16, 128), BF),
+            pltpu.VMEM((4, 6, 1, lines // 2 + 1, 16, 128), BF),
+            pltpu.VMEM((2, 2, lines + 1, 16, 128), BF),
+            pltpu.VMEM((2, 3, lines + 1, 16, 128), BF),
             pltpu.VMEM((4, tokens, width), F32),
             pltpu.VMEM((2, tokens, width), F32),
-            pltpu.VMEM((1, tokens, width), BF),
-            pltpu.VMEM((1, tokens, width), BF),
-            pltpu.VMEM((2, 8, 128), F32),
+            pltpu.VMEM((tokens * width // 2048 + 1, 16, 128), BF),
+            pltpu.VMEM((tokens * width // 2048 + 1, 16, 128), BF),
             pltpu.VMEM((4, 1, hidden), F32),
-            pltpu.VMEM((2, 4, 1, hidden), F32),
+            pltpu.VMEM((8, 1, hidden), F32),
             pltpu.VMEM((2, rows, 128), F32),
             pltpu.VMEM((2, 2, rows // 2, cols), BF),
             pltpu.VMEM((tokens, width), BF),
             pltpu.VMEM((rows, hidden), F32),
             pltpu.VMEM((rows, hidden), F32),
-            pltpu.SemaphoreType.DMA((COPIES,)),
-            pltpu.SemaphoreType.DMA((COPIES,)),
+            pltpu.SemaphoreType.DMA((BATCHES,)),
+            pltpu.SemaphoreType.DMA((WAITS,)),
             pltpu.SemaphoreType.DMA((9,)),
         ],
         compiler_params=pltpu.CompilerParams(

time: 88.3 us -> 78.7 us (0.89)
  Pallas kernels: 87.5 us -> 77.9 us
    pallas_call x1, Pallas kernels: 85.4 us -> 75.7 us  [per_device(): pl.pallas_call(make_kernel(tokens, width, cols, ff, factor), out_shape=(j...]
where the time goes in v5:
time: 78.7 us; the launch traced here: 78.5 us
  Pallas kernels  77.9 us (99%)
    pallas_call x1, Pallas kernels, per_device(): pl.pallas_call(make_kernel(tokens, width, cols, ff, factor), out_shape=(j...  75.7 us
    pallas_call x1, Pallas kernels, hand_over(): pl.pallas_call(kernel, out_shape=tuple(shapes), in_specs=[vm] * 5, out_sp...  2.18 us

profile of v5, /device:TPU:1, one launch (start us, length us, event | category | flops | bytes accessed | tf_op | source)
XLA Modules:
  0.0 78.5 jit_solution(10963990425300242453)
XLA Ops:
  0.6 75.7 %shard_map.83 = (bf16[256,1024]{1,0:T(8,128)(2,1)}, f32[32,2048]{1,0:T(8,128)}, f32[32,2048]{1,0:T(8,128)}, f32[1,32]{1,0:T(1,128)}, f32[1,2048]{1,0:T(1,128)}) custom-call(bf16[256,1024]{1,0:T(8,128)(2,1)} %x_ref.1, bf16[2,16,2048]{2,1,0:T(8,128)(2,1)} %bitcast.6, bf16[2,16,2048]{2,1,0:T(8,128)(2,1)} %bitcast.7, bf16[256,1024]{1,0:T(8,128)(2,1)} %cot_ref.1), custom_call_target="tpu_custom_call" | custom-call | tf_op jit(solution)/shard_map/pallas_call | solution.py:492
  76.3 2.2 %shard_map.84 = (bf16[256,1024]{1,0:T(8,128)(2,1)}, f32[32,2048]{1,0:T(8,128)}, f32[32,2048]{1,0:T(8,128)}, f32[1,32]{1,0:T(1,128)}, f32[2048]{0:T(1024)}) custom-call(bf16[256,1024]{1,0:T(8,128)(2,1)} %get-tuple-element.15.refs_0_, f32[32,2048]{1,0:T(8,128)} %get-tuple-element.16.refs_1_, f32[32,2048]{1,0:T(8,128)} %get-tuple-element.17.refs_2_, ...), custom_call_target="tpu_custom_call" | custom-call | tf_op jit(solution)/shard_map/pallas_call | solution.py:477

commit v6 on v5

--- a/solution.py
+++ b/solution.py
@@ -17,29 +17,29 @@
 
 
 ORDER = [
-    ("init", 0, 0), ("init", 1, 0), ("turn", "x", 1), ("init", 0, 1), ("init", 1, 1), ("near", 0, 1, 0),
-    ("turn", "c", 1), ("fwd", 0, 0, 0, 0), ("near", 0, 1, 1), ("near", 0, 0, 0), ("near", 1, 0, 1),
-    ("fwd", 0, 0, 0, 1), ("near", 0, 0, 1), ("step2", 0, 1), ("near", 1, 1, 0), ("near", 1, 1, 1),
-    ("near", 1, 0, 0), ("pass", "x", 0), ("fwd", 0, 1, 0, 0), ("fwd", 0, 1, 0, 1), ("pass", "x", 1),
-    ("step2", 0, 0), ("fwd", 0, 1, 3, 0), ("fwd", 0, 1, 3, 1), ("fwd", 0, 1, 1, 0), ("turn", "x", 3),
-    ("fwd", 1, 0, 0, 1), ("fwd", 0, 0, 1, 1), ("turn", "x", 0), ("fwd", 1, 1, 0, 0), ("fwd", 0, 0, 2, 0),
-    ("fwd", 0, 1, 1, 1), ("turn", "c", 0), ("fwd", 0, 1, 2, 1), ("fwd", 0, 1, 2, 0), ("fwd", 1, 0, 2, 1),
-    ("fwd", 0, 0, 1, 0), ("step2", 1, 1), ("fwd", 1, 1, 2, 1), ("fwd", 1, 1, 0, 1), ("fwd", 1, 1, 1, 0),
-    ("fwd", 0, 0, 3, 0), ("fwd", 0, 0, 2, 1), ("fwd", 1, 1, 1, 1), ("fwd", 0, 0, 3, 1), ("turn", "x", 2),
-    ("pass", "c", 0), ("step2", 1, 0), ("proj", 0), ("fwd", 1, 0, 0, 0), ("fwd", 1, 0, 2, 0), ("fwd", 1, 0, 1, 1),
-    ("fwd", 1, 0, 3, 0), ("pass", "c", 1), ("ma", 1, 1), ("fwd", 1, 1, 3, 0), ("fwd", 1, 1, 3, 1),
-    ("fwd", 1, 0, 1, 0), ("fwd", 1, 0, 3, 1), ("proj", 1), ("fwd", 1, 1, 2, 0), ("turn", "c", 2),
-    ("turn", "c", 3), ("mult", 1, 0), ("mult", 1, 1), ("far", 1, 1, 1), ("far", 1, 0, 0), ("nl", 1, 0),
-    ("far", 1, 1, 0), ("nr", 1, 1), ("far", 1, 0, 1), ("pull", 1), ("pull", 0), ("nr", 1, 0), ("nl", 1, 1),
-    ("ip", 0), ("mult", 0, 0), ("rl", 1, 0, 0, 0), ("rl", 1, 1, 1, 1), ("rl", 1, 1, 0, 1), ("rl", 1, 0, 1, 0),
-    ("rl", 1, 1, 0, 0), ("far", 0, 0, 0), ("rl", 1, 1, 1, 0), ("far", 0, 0, 1), ("rl", 1, 0, 0, 1),
-    ("mult", 0, 1), ("far", 0, 1, 0), ("ip", 1), ("gz",), ("nr", 0, 1), ("nl", 0, 1), ("rl", 1, 0, 1, 1),
-    ("ni", 1, 1), ("rl", 0, 0, 0, 0), ("rl", 0, 0, 1, 0), ("far", 0, 1, 1), ("ni", 1, 0), ("nl", 0, 0),
-    ("st2", 1, 1), ("nr", 0, 0), ("rl", 0, 0, 1, 1), ("rl", 0, 0, 0, 1), ("st2", 1, 0), ("ni", 0, 1),
-    ("rl2", 1, 0, 1), ("rl2", 1, 0, 0), ("rl", 0, 1, 1, 1), ("rl", 0, 1, 0, 0), ("rl2", 1, 1, 1),
-    ("rl", 0, 1, 0, 1), ("rl2", 1, 1, 0), ("rl", 0, 1, 1, 0), ("ni", 0, 0), ("st3", 1, 0), ("st2", 0, 0),
-    ("st3", 1, 1), ("st2", 0, 1), ("rl2", 0, 0, 0), ("rl2", 0, 0, 1), ("rl2", 0, 1, 1), ("rl2", 0, 1, 0),
-    ("st3", 0, 0), ("fin", 1), ("ex",), ("st3", 0, 1), ("ey",), ("fin", 0), ("eu",), ("gin",), ("eup",), ("edn",),
+    ("init", 1, 0), ("init", 0, 0), ("init", 0, 1), ("init", 1, 1), ("near", 0, 0, 0), ("pass", "x", 0),
+    ("near", 0, 0, 1), ("near", 0, 1, 0), ("near", 0, 1, 1), ("fwd", 0, 0, 0, 0), ("turn", "x", 0),
+    ("near", 1, 1, 0), ("step2", 0, 0), ("fwd", 0, 1, 1, 0), ("turn", "x", 1), ("fwd", 0, 0, 2, 1),
+    ("step2", 0, 1), ("near", 1, 0, 1), ("fwd", 0, 0, 1, 1), ("near", 1, 0, 0), ("turn", "c", 0),
+    ("near", 1, 1, 1), ("fwd", 0, 0, 3, 0), ("fwd", 0, 1, 0, 1), ("fwd", 1, 1, 0, 1), ("fwd", 0, 1, 3, 0),
+    ("fwd", 0, 1, 3, 1), ("fwd", 0, 0, 3, 1), ("fwd", 0, 0, 0, 1), ("fwd", 1, 0, 0, 1), ("pass", "x", 1),
+    ("turn", "c", 1), ("fwd", 0, 1, 1, 1), ("fwd", 0, 1, 2, 0), ("fwd", 1, 0, 2, 1), ("fwd", 0, 1, 2, 1),
+    ("fwd", 0, 0, 1, 0), ("turn", "x", 2), ("fwd", 1, 1, 1, 0), ("fwd", 0, 0, 2, 0), ("fwd", 0, 1, 0, 0),
+    ("step2", 1, 0), ("step2", 1, 1), ("fwd", 1, 0, 1, 1), ("turn", "x", 3), ("fwd", 1, 1, 0, 0),
+    ("fwd", 1, 0, 2, 0), ("fwd", 1, 1, 2, 1), ("proj", 0), ("fwd", 1, 1, 2, 0), ("pass", "c", 0),
+    ("fwd", 1, 0, 0, 0), ("ma", 1, 1), ("fwd", 1, 1, 3, 1), ("fwd", 1, 1, 1, 1), ("fwd", 1, 0, 3, 0),
+    ("fwd", 1, 1, 3, 0), ("fwd", 1, 0, 1, 0), ("pass", "c", 1), ("turn", "c", 2), ("proj", 1),
+    ("fwd", 1, 0, 3, 1), ("ma", 1, 0), ("turn", "c", 3), ("mult", 1, 0), ("far", 1, 0, 0), ("mult", 1, 1),
+    ("far", 1, 1, 0), ("far", 1, 0, 1), ("far", 1, 1, 1), ("pull", 0), ("nr", 1, 1), ("nr", 1, 0), ("nl", 1, 1),
+    ("nl", 1, 0), ("pull", 1), ("ip", 0), ("rl", 1, 0, 1, 1), ("rl", 1, 0, 0, 0), ("rl", 1, 0, 0, 1),
+    ("mult", 0, 1), ("rl", 1, 1, 1, 0), ("far", 0, 1, 1), ("rl", 1, 0, 1, 0), ("mult", 0, 0), ("far", 0, 0, 0),
+    ("rl", 1, 1, 0, 0), ("far", 0, 0, 1), ("rl", 1, 1, 1, 1), ("ni", 1, 0), ("ip", 1), ("rl", 1, 1, 0, 1),
+    ("gz",), ("far", 0, 1, 0), ("nr", 0, 0), ("nl", 0, 0), ("st2", 1, 0), ("rl", 0, 0, 1, 0), ("nl", 0, 1),
+    ("nr", 0, 1), ("rl", 0, 0, 0, 1), ("rl", 0, 0, 1, 1), ("rl", 0, 0, 0, 0), ("ni", 1, 1), ("st2", 1, 1),
+    ("rl2", 1, 0, 1), ("ni", 0, 0), ("rl2", 1, 0, 0), ("rl", 0, 1, 0, 0), ("rl", 0, 1, 1, 1), ("rl", 0, 1, 0, 1),
+    ("rl", 0, 1, 1, 0), ("st2", 0, 0), ("rl2", 1, 1, 1), ("ni", 0, 1), ("st3", 1, 0), ("rl2", 1, 1, 0),
+    ("st2", 0, 1), ("rl2", 0, 0, 1), ("st3", 1, 1), ("rl2", 0, 0, 0), ("rl2", 0, 1, 1), ("rl2", 0, 1, 0),
+    ("gin",), ("st3", 0, 0), ("fin", 1), ("ex",), ("st3", 0, 1), ("ey",), ("fin", 0), ("eu",), ("eup",), ("edn",),
 ]
 
 
@@ -48,11 +48,11 @@
 
     def kernel(
         x_ref, up_ref, dn_ref, cot_ref,
-        gin_out, gup_out, gdn_out, eup_ref, edn_ref,
+        gin_ref, gup_ref, gdn_ref, eup_ref, edn_ref,
         X, C, XT, CT, W, RP, ACT, GP, G,
         s1s, s1r, s2s, s2r, s3s, s3r,
         PART, DR, ZS, ZR, EX, EY, EU,
-        OTH, gin_ref, gup_ref, gdn_ref, ssem, rsem, lsem,
+        OTH, ssem, rsem, lsem,
     ):
         r = lax.axis_index("rep")
         j = lax.axis_index("fs_0")
@@ -95,13 +95,6 @@
         for dev in peers:
             pl.semaphore_signal(barrier, inc=1, device_id=dev, device_id_type=MESH)
         pl.semaphore_wait(barrier, len(peers))
-
-        stores = []
-
-        def store(src, dst):
-            c = pltpu.make_async_copy(src, dst, lsem.at[6 + len(stores)])
-            c.start()
-            stores.append(c)
 
         arrivals, departures = {}, {}
 
@@ -360,7 +353,6 @@
                 for n, q, c in every:
                     col = pl.ds(pl.multiple_of(side * cols + n // (width // 512) * 128, 128), 128)
                     out[q, col] = (tile1(n) + tile2(n)) * factor
-            store(out, (gup_out, gdn_out)[w])
 
         def input_part(n):
             s1, s2 = ((3, 1), (2, 0))[n]
@@ -384,7 +376,6 @@
             every, tile = decoder(ZR, tokens, 4)
             for n, q, c in every:
                 gin_ref[q, c] = (PART[0, q, c] + DR[1, q, c] + tile(n)).astype(BF)
-            store(gin_ref, gin_out)
 
         def energy_x():
             EX[x] = jnp.sum(gdn_ref[...] * gdn_ref[...], axis=0, keepdims=True)
@@ -458,8 +449,6 @@
         sent("ex", EX.at[pl.ds(0, 3)])
         sent("ey", EY.at[pl.ds(0, 7)])
         sent("et", EU.at[0])
-        for c in stores:
-            c.wait()
 
     return kernel
 
@@ -467,14 +456,18 @@
 def hand_over(results):
     vm = pl.BlockSpec(memory_space=pltpu.VMEM)
     shapes = [jax.ShapeDtypeStruct(v.shape, v.dtype) for v in results]
-    shapes[4] = jax.ShapeDtypeStruct(results[4].shape[1:], F32)
 
     def kernel(*refs):
-        for src, dst in zip(refs[:4], refs[5:9]):
-            dst[...] = src[...]
-        refs[9][...] = refs[4][0]
-
-    return pl.pallas_call(kernel, out_shape=tuple(shapes), in_specs=[vm] * 5, out_specs=(vm,) * 5)(*results)
+        sem = refs[10]
+        moves = [pltpu.make_async_copy(refs[n], refs[5 + n], sem.at[n]) for n in range(5)]
+        for c in moves:
+            c.start()
+        for c in moves:
+            c.wait()
+
+    return pl.pallas_call(kernel, out_shape=tuple(shapes), in_specs=[vm] * 5, out_specs=(pl.BlockSpec(memory_space=pltpu.HBM),) * 5,
+        scratch_shapes=[pltpu.SemaphoreType.DMA((5,))],
+    )(*[pltpu.with_memory_space_constraint(v, pltpu.VMEM) for v in results])
 
 
 def per_device(inputs, up_proj, down_proj, out_cotangent):
@@ -492,14 +485,14 @@
     results = pl.pallas_call(
         make_kernel(tokens, width, cols, ff, factor),
         out_shape=(
-            jax.ShapeDtypeStruct((tokens, width), BF),
-            jax.ShapeDtypeStruct((rows, hidden), F32),
-            jax.ShapeDtypeStruct((rows, hidden), F32),
-            jax.ShapeDtypeStruct((1, rows), F32),
-            jax.ShapeDtypeStruct((1, hidden), F32),
+            pltpu.VMEM((tokens, width), BF),
+            pltpu.VMEM((rows, hidden), F32),
+            pltpu.VMEM((rows, hidden), F32),
+            pltpu.VMEM((1, rows), F32),
+            pltpu.VMEM((1, hidden), F32),
         ),
-        in_specs=[pl.BlockSpec(memory_space=pl.ANY)] * 4,
-        out_specs=(pl.BlockSpec(memory_space=pl.ANY),) * 3 + (vm, vm),
+        in_specs=[pl.BlockSpec(memory_space=pltpu.HBM)] * 4,
+        out_specs=(vm,) * 5,
         scratch_shapes=[
             pltpu.VMEM((4, tokens, width), BF),
             pltpu.VMEM((4, tokens, width), BF),
@@ -524,19 +517,16 @@
             pltpu.VMEM((8, 1, hidden), F32),
             pltpu.VMEM((2, rows, 128), F32),
             pltpu.VMEM((2, 2, rows // 2, cols), BF),
-            pltpu.VMEM((tokens, width), BF),
-            pltpu.VMEM((rows, hidden), F32),
-            pltpu.VMEM((rows, hidden), F32),
             pltpu.SemaphoreType.DMA((BATCHES,)),
             pltpu.SemaphoreType.DMA((WAITS,)),
-            pltpu.SemaphoreType.DMA((9,)),
+            pltpu.SemaphoreType.DMA((6,)),
         ],
         compiler_params=pltpu.CompilerParams(
-            collective_id=0, has_side_effects=True, vmem_limit_bytes=63 * 1024 * 1024
+            collective_id=0, has_side_effects=True, vmem_limit_bytes=52 * 1024 * 1024
         ),
-    )(inputs, up3, dn3, out_cotangent)
+    )(*[pltpu.with_memory_space_constraint(v, pltpu.HBM) for v in (inputs, up3, dn3, out_cotangent)])
     gin, gup, gdn, eup, edn = hand_over(results)
-    return gin, gup, gdn.T, eup.reshape(rows), edn
+    return gin, gup, gdn.T, eup.reshape(rows), edn.reshape(hidden)
 
 
 def solution(mesh):

time: 78.7 us -> 75.9 us (0.964)
  Pallas kernels: 77.9 us -> 74.9 us
    pallas_call x1, Pallas kernels: 75.7 us -> 73.9 us  [per_device(): pl.pallas_call(make_kernel(tokens, width, cols, ff, factor), out_shape=(p...]
    pallas_call x1, Pallas kernels: 2.18 us -> 1.01 us  [hand_over(): pl.pallas_call(kernel, out_shape=tuple(shapes), in_specs=[vm] * 5, out_sp...]
where the time goes in v6:
time: 75.9 us; the launch traced here: 75.7 us
  Pallas kernels  74.9 us (99%)
  between operations  0.8 us (1%)
    pallas_call x1, Pallas kernels, per_device(): pl.pallas_call(make_kernel(tokens, width, cols, ff, factor), out_shape=(p...  73.9 us

profile of v6, /device:TPU:1, one launch (start us, length us, event | category | flops | bytes accessed | tf_op | source)
XLA Modules:
  0.0 75.7 jit_solution(11929762004104120122)
XLA Ops:
  0.6 73.9 %shard_map.83 = (bf16[256,1024]{1,0:T(8,128)(2,1)S(1)}, f32[32,2048]{1,0:T(8,128)S(1)}, f32[32,2048]{1,0:T(8,128)S(1)}, f32[1,32]{1,0:T(1,128)S(1)}, f32[1,2048]{1,0:T(1,128)S(1)}) custom-call(bf16[256,1024]{1,0:T(8,128)(2,1)} %x_ref.1, bf16[2,16,2048]{2,1,0:T(8,128)(2,1)} %bitcast.7, bf16[2,16,2048]{2,1,0:T(8,128)(2,1)} %bitcast.8, bf16[256,1024]{1,0:T(8,128)(2,1)} %cot_ref.1), custom_call_target="tpu_custom_call" | custom-call | tf_op jit(solution)/shard_map/pallas_call | solution.py:485
  74.6 1.0 %shard_map.84 = (bf16[256,1024]{1,0:T(8,128)(2,1)}, f32[32,2048]{1,0:T(8,128)}, f32[32,2048]{1,0:T(8,128)}, f32[1,32]{1,0:T(1,128)}, f32[1,2048]{1,0:T(1,128)}) custom-call(bf16[256,1024]{1,0:T(8,128)(2,1)S(1)} %get-tuple-element.15.refs_0_, f32[32,2048]{1,0:T(8,128)S(1)} %get-tuple-element.16.refs_1_, f32[32,2048]{1,0:T(8,128)S(1)} %get-tuple-element.17.refs_2_, ...), custom_call_target="tpu_custom_call" | custom-call | tf_op jit(solution)/shard_map/pallas_call | solution.py:468

commit v7 on v6

--- a/solution.py
+++ b/solution.py
@@ -13,33 +13,36 @@
 F32 = jnp.float32
 RIGHT, LEFT = 0, 1
 UP, DN = 0, 1
-WAITS, BATCHES = 110, 26
+WAITS, BATCHES = 118, 32
 
 
 ORDER = [
-    ("init", 1, 0), ("init", 0, 0), ("init", 0, 1), ("init", 1, 1), ("near", 0, 0, 0), ("pass", "x", 0),
-    ("near", 0, 0, 1), ("near", 0, 1, 0), ("near", 0, 1, 1), ("fwd", 0, 0, 0, 0), ("turn", "x", 0),
-    ("near", 1, 1, 0), ("step2", 0, 0), ("fwd", 0, 1, 1, 0), ("turn", "x", 1), ("fwd", 0, 0, 2, 1),
-    ("step2", 0, 1), ("near", 1, 0, 1), ("fwd", 0, 0, 1, 1), ("near", 1, 0, 0), ("turn", "c", 0),
-    ("near", 1, 1, 1), ("fwd", 0, 0, 3, 0), ("fwd", 0, 1, 0, 1), ("fwd", 1, 1, 0, 1), ("fwd", 0, 1, 3, 0),
-    ("fwd", 0, 1, 3, 1), ("fwd", 0, 0, 3, 1), ("fwd", 0, 0, 0, 1), ("fwd", 1, 0, 0, 1), ("pass", "x", 1),
-    ("turn", "c", 1), ("fwd", 0, 1, 1, 1), ("fwd", 0, 1, 2, 0), ("fwd", 1, 0, 2, 1), ("fwd", 0, 1, 2, 1),
-    ("fwd", 0, 0, 1, 0), ("turn", "x", 2), ("fwd", 1, 1, 1, 0), ("fwd", 0, 0, 2, 0), ("fwd", 0, 1, 0, 0),
-    ("step2", 1, 0), ("step2", 1, 1), ("fwd", 1, 0, 1, 1), ("turn", "x", 3), ("fwd", 1, 1, 0, 0),
-    ("fwd", 1, 0, 2, 0), ("fwd", 1, 1, 2, 1), ("proj", 0), ("fwd", 1, 1, 2, 0), ("pass", "c", 0),
-    ("fwd", 1, 0, 0, 0), ("ma", 1, 1), ("fwd", 1, 1, 3, 1), ("fwd", 1, 1, 1, 1), ("fwd", 1, 0, 3, 0),
-    ("fwd", 1, 1, 3, 0), ("fwd", 1, 0, 1, 0), ("pass", "c", 1), ("turn", "c", 2), ("proj", 1),
-    ("fwd", 1, 0, 3, 1), ("ma", 1, 0), ("turn", "c", 3), ("mult", 1, 0), ("far", 1, 0, 0), ("mult", 1, 1),
-    ("far", 1, 1, 0), ("far", 1, 0, 1), ("far", 1, 1, 1), ("pull", 0), ("nr", 1, 1), ("nr", 1, 0), ("nl", 1, 1),
-    ("nl", 1, 0), ("pull", 1), ("ip", 0), ("rl", 1, 0, 1, 1), ("rl", 1, 0, 0, 0), ("rl", 1, 0, 0, 1),
-    ("mult", 0, 1), ("rl", 1, 1, 1, 0), ("far", 0, 1, 1), ("rl", 1, 0, 1, 0), ("mult", 0, 0), ("far", 0, 0, 0),
-    ("rl", 1, 1, 0, 0), ("far", 0, 0, 1), ("rl", 1, 1, 1, 1), ("ni", 1, 0), ("ip", 1), ("rl", 1, 1, 0, 1),
-    ("gz",), ("far", 0, 1, 0), ("nr", 0, 0), ("nl", 0, 0), ("st2", 1, 0), ("rl", 0, 0, 1, 0), ("nl", 0, 1),
-    ("nr", 0, 1), ("rl", 0, 0, 0, 1), ("rl", 0, 0, 1, 1), ("rl", 0, 0, 0, 0), ("ni", 1, 1), ("st2", 1, 1),
-    ("rl2", 1, 0, 1), ("ni", 0, 0), ("rl2", 1, 0, 0), ("rl", 0, 1, 0, 0), ("rl", 0, 1, 1, 1), ("rl", 0, 1, 0, 1),
-    ("rl", 0, 1, 1, 0), ("st2", 0, 0), ("rl2", 1, 1, 1), ("ni", 0, 1), ("st3", 1, 0), ("rl2", 1, 1, 0),
-    ("st2", 0, 1), ("rl2", 0, 0, 1), ("st3", 1, 1), ("rl2", 0, 0, 0), ("rl2", 0, 1, 1), ("rl2", 0, 1, 0),
-    ("gin",), ("st3", 0, 0), ("fin", 1), ("ex",), ("st3", 0, 1), ("ey",), ("fin", 0), ("eu",), ("eup",), ("edn",),
+    ("init", 1, 0), ("init", 0, 0), ("init", 0, 1), ("init", 1, 1), ("near", 0, 0, 0), ("near", 0, 0, 1),
+    ("near", 0, 1, 0), ("near", 0, 1, 1), ("near", 1, 0, 1), ("near", 1, 0, 0), ("near", 1, 1, 0),
+    ("step2", 0, 1), ("fwd", 1, 0, 0, 1), ("step2", 0, 0), ("turn", "c", 0), ("fwd", 0, 0, 0, 1),
+    ("near", 1, 1, 1), ("fwd", 0, 1, 1, 1), ("fwd", 0, 1, 1, 0), ("pass", "x", 0), ("fwd", 0, 1, 2, 1),
+    ("fwd", 0, 1, 0, 1), ("fwd", 0, 0, 1, 1), ("fwd", 1, 0, 2, 0), ("fwd", 0, 0, 1, 0), ("pass", "x", 1),
+    ("turn", "x", 0), ("fwd", 0, 0, 2, 0), ("turn", "x", 1), ("turn", "c", 1), ("fwd", 0, 1, 2, 0),
+    ("fwd", 0, 0, 2, 1), ("turn", "x", 3), ("fwd", 0, 1, 0, 0), ("step2", 1, 0), ("fwd", 0, 0, 3, 0),
+    ("fwd", 1, 1, 0, 1), ("fwd", 0, 1, 3, 0), ("turn", "x", 2), ("fwd", 0, 1, 3, 1), ("fwd", 1, 1, 2, 0),
+    ("fwd", 0, 0, 3, 1), ("pass", "c", 0), ("fwd", 1, 0, 2, 1), ("fwd", 1, 0, 1, 1), ("step2", 1, 1),
+    ("fwd", 1, 1, 1, 0), ("fwd", 0, 0, 0, 0), ("proj", 0), ("fwd", 1, 1, 3, 0), ("fwd", 1, 0, 3, 1),
+    ("fwd", 1, 1, 0, 0), ("ma", 1, 0), ("fwd", 1, 1, 3, 1), ("fwd", 1, 1, 1, 1), ("fwd", 1, 0, 3, 0),
+    ("pass", "c", 1), ("fwd", 1, 0, 1, 0), ("fwd", 1, 0, 0, 0), ("fwd", 1, 1, 2, 1), ("turn", "c", 2),
+    ("ma", 1, 1), ("proj", 1), ("turn", "c", 3), ("mult", 1, 1), ("far", 1, 1, 0), ("mult", 1, 0),
+    ("far", 1, 0, 0), ("far", 1, 1, 1), ("pull", 1), ("pull", 0), ("nr", 1, 1, 0), ("nr", 1, 0, 1),
+    ("nl", 1, 0, 1), ("ip", 0), ("far", 1, 0, 1), ("nl", 1, 1, 1), ("mult", 0, 1), ("nl", 0, 1, 1),
+    ("nr", 1, 1, 1), ("rl", 1, 0, 0, 0), ("nl", 1, 0, 0), ("nr", 1, 0, 0), ("far", 0, 1, 0), ("rl", 1, 0, 1, 0),
+    ("rl", 1, 1, 0, 0), ("rl", 1, 1, 0, 1), ("mult", 0, 0), ("ip", 1), ("nl", 1, 1, 0), ("rl", 1, 0, 1, 1),
+    ("rl", 1, 0, 0, 1), ("rl", 1, 1, 1, 1), ("nr", 0, 1, 1), ("gz",), ("nl", 0, 0, 0), ("far", 0, 0, 1),
+    ("nl", 0, 0, 1), ("rl", 1, 1, 1, 0), ("nr", 0, 0, 0), ("ni", 1, 0, 1), ("ni", 1, 0, 0), ("st2", 1, 0),
+    ("nr", 0, 0, 1), ("ni", 1, 1, 1), ("far", 0, 1, 1), ("nr", 0, 1, 0), ("rl", 0, 1, 1, 0), ("ni", 1, 1, 0),
+    ("far", 0, 0, 0), ("ni", 0, 0, 0), ("st2", 1, 1), ("rl", 0, 0, 1, 1), ("rl", 0, 0, 0, 1), ("rl2", 1, 0, 0),
+    ("rl", 0, 1, 0, 0), ("rl2", 1, 0, 1), ("rl", 0, 1, 0, 1), ("rl2", 1, 1, 1), ("nl", 0, 1, 0), ("ni", 0, 0, 1),
+    ("rl2", 1, 1, 0), ("ni", 0, 1, 1), ("rl", 0, 0, 1, 0), ("rl", 0, 0, 0, 0), ("st3", 1, 0), ("rl", 0, 1, 1, 1),
+    ("st2", 0, 0, 1), ("ni", 0, 1, 0), ("st3", 1, 1), ("st2", 0, 1, 0), ("st2", 0, 1, 1), ("st2", 0, 0, 0),
+    ("st3", 0, 0, 1), ("fin", 1), ("ex",), ("gin",), ("st3", 0, 1, 0), ("st3", 0, 0, 0), ("st3", 0, 1, 1),
+    ("ey",), ("fin", 0, 0), ("fin", 0, 1), ("eu",), ("eup",), ("edn",),
 ]
 
 
@@ -50,7 +53,7 @@
         x_ref, up_ref, dn_ref, cot_ref,
         gin_ref, gup_ref, gdn_ref, eup_ref, edn_ref,
         X, C, XT, CT, W, RP, ACT, GP, G,
-        s1s, s1r, s2s, s2r, s3s, s3r,
+        s1s, s1r, s2s, s2r, d2s, d2r, s3s, s3r, u3s, u3r,
         PART, DR, ZS, ZR, EX, EY, EU,
         OTH, ssem, rsem, lsem,
     ):
@@ -237,27 +240,32 @@
                 ref, out = product(w, h, 0, 4)
                 ref[...] = out
 
-        def tiles(rows):
-            return [(n, pl.ds(16 * (n % (rows // 16)), 16), lanes[n // (rows // 16)])
-                    for n in range(rows // 16 * len(lanes))]
-
-        def encode(src, dst, steps=3):
-            every = tiles(src.shape[0])
+        def tiles(refs):
+            every = []
+            for m, ref in enumerate(refs):
+                rows, wide = ref.shape
+                for c in range(wide // 128):
+                    for q in range(rows // 16):
+                        every.append((len(every), m, pl.ds(16 * q, 16), pl.ds(128 * c, 128)))
+            return every
+
+        def encode(refs, dst, steps=3):
+            every = tiles(refs)
             top = None
-            for _, q, c in every:
-                m = jnp.abs(src[q, c])
-                top = m if top is None else jnp.maximum(top, m)
+            for _, m, q, c in every:
+                v = jnp.abs(refs[m][q, c])
+                top = v if top is None else jnp.maximum(top, v)
             top = jnp.maximum(top, 2e-34).astype(BF)
             dst[len(every)] = top
             inv = 2.0 ** (120 >> steps) / top.astype(F32)
-            for n, q, c in every:
-                v = src[q, c] * inv
+            for n, m, q, c in every:
+                v = refs[m][q, c] * inv
                 for _ in range(steps):
                     v = v * jnp.abs(v)
                 dst[n] = v.astype(BF)
 
-        def decoder(buf, rows, steps=3):
-            every = tiles(rows)
+        def decoder(buf, refs, steps=3):
+            every = tiles(refs)
             unit = buf[len(every)].astype(F32) * 0.5 ** (120 >> steps)
 
             def tile(n):
@@ -266,92 +274,110 @@
                 return jnp.where(v < 0, -m, m) * unit
             return every, tile
 
-        def add(ref, buf):
-            every, tile = decoder(buf, ref.shape[0])
-            for n, q, c in every:
-                ref[q, c] = ref[q, c] + tile(n)
+        def add(refs, buf):
+            every, tile = decoder(buf, refs)
+            for n, m, q, c in every:
+                refs[m][q, c] = refs[m][q, c] + tile(n)
 
         class Ring:
-            def __init__(self, stage, w, h, pos, dev, parts, bufs, subs):
-                self.k = (stage, w, h)
-                self.subs = subs
-                self.pos, self.dev, self.parts = pos, dev, parts
-                self.sb, self.rb = (b.at[2 * w + h] for b in bufs)
-
-            def post(self, i, srcs, d, lo, n, group):
-                for m in range(lo, lo + n):
-                    encode(srcs[m], self.sb.at[i, m])
-                some = pl.ds(lo, n)
-                send(self.k + group, self.sb.at[i, some], self.rb.at[i, some], self.dev(d), self.k)
-
-            def far(self, lo=0):
-                self.post(0, self.parts(at(self.pos, 2), 0), 1, lo, 1, ("far", 0, lo))
-                self.post(1, self.parts(at(self.pos, 2), 1), 3, lo, 1, ("far", 1, lo))
+            def __init__(self, key, pos, dev, parts, sb, rb):
+                self.k, self.pos, self.dev, self.parts, self.sb, self.rb = key, pos, dev, parts, sb, rb
+
+            def post(self, i, place, side, d, group):
+                encode(self.parts(place, side), self.sb.at[i])
+                send(self.k + group, self.sb.at[i], self.rb.at[i], self.dev(d), self.k)
+
+            def far(self):
+                self.post(0, at(self.pos, 2), 0, 1, ("far", 0))
+                self.post(1, at(self.pos, 2), 1, 3, ("far", 1))
 
             def near_right(self):
-                self.post(2, self.parts(at(self.pos, 1), 1), 1, 0, self.subs, ("near",))
+                self.post(2, at(self.pos, 1), 1, 1, ("near",))
 
             def near_left(self):
-                self.post(3, self.parts(at(self.pos, 3), 0), 3, 0, self.subs, ("near",))
-
-            def relay(self, side, lo=0):
-                p = self.parts(at(self.pos, (1, 3)[side]), side)
-                recv(self.k + ("far", side, lo), self.rb.at[side, pl.ds(lo, 1)])
-                add(p[lo], self.rb.at[side, lo])
-                self.post(4 + side, p, (1, 3)[side], lo, 1, ("last", lo))
+                self.post(3, at(self.pos, 3), 0, 3, ("near",))
+
+            def relay(self, side):
+                place, d = at(self.pos, (1, 3)[side]), (1, 3)[side]
+                recv(self.k + ("far", side), self.rb.at[side])
+                add(self.parts(place, side), self.rb.at[side])
+                self.post(4 + side, place, side, d, ("last",))
 
             def near_in(self):
                 recv(self.k + ("near",), self.rb.at[pl.ds(2, 2)])
-                for m in range(self.subs):
-                    add(self.parts(self.pos, 0)[m], self.rb.at[3, m])
-                    add(self.parts(self.pos, 1)[m], self.rb.at[2, m])
+                add(self.parts(self.pos, 0), self.rb.at[3])
+                add(self.parts(self.pos, 1), self.rb.at[2])
 
             def last_in(self):
-                for m in range(self.subs):
-                    recv(self.k + ("last", m), self.rb.at[pl.ds(4, 2), m])
-                    add(self.parts(self.pos, 0)[m], self.rb.at[4, m])
-                    add(self.parts(self.pos, 1)[m], self.rb.at[5, m])
-
-        def ring1(w, h):
-            a, b, adev, bdev = raxes(h)
-            return Ring(1, w, h, a, adev,
-                        lambda place, side: [gblk(w, h, place, 2 * side + i) for i in (0, 1)],
-                        (s1s, s1r), 2)
-
+                recv(self.k + ("last",), self.rb.at[pl.ds(4, 2)])
+                add(self.parts(self.pos, 0), self.rb.at[4])
+                add(self.parts(self.pos, 1), self.rb.at[5])
+
+        wing = cols // 2
         hr = width // 64
 
-        def ring2(w, h):
-            a, b, adev, bdev = raxes(h)
-            return Ring(2, w, h, b, bdev,
-                        lambda place, side: [gblk(w, h, a, place).at[pl.ds(side * hr, hr)]],
-                        (s2s, s2r), 1)
-
-        first = {(w, h): ring1(w, h) for w in (UP, DN) for h in (0, 1)}
-        second = {(w, h): ring2(w, h) for w in (UP, DN) for h in (0, 1)}
-
-        def second_start(w, h):
-            first[w, h].last_in()
-            second[w, h].far()
-            second[w, h].near_right()
-            second[w, h].near_left()
-
-        def third_start(w, h):
-            second[w, h].near_in()
-            second[w, h].last_in()
+        def ring1(w, h, c):
+            a, _, adev, _ = raxes(h)
+            return Ring((1, w, h, c), a, adev,
+                        lambda place, side: [gblk(w, h, place, 2 * side + i).at[:, pl.ds(c * wing, wing)] for i in (0, 1)],
+                        s1s.at[2 * w + h, c], s1r.at[2 * w + h, c])
+
+        def ring2(h):
+            a, b, _, bdev = raxes(h)
+            return Ring((2, DN, h), b, bdev,
+                        lambda place, side: [gblk(DN, h, a, place).at[pl.ds(side * hr, hr)]],
+                        s2s.at[h], s2r.at[h])
+
+        first = {(w, h, c): ring1(w, h, c) for w in (UP, DN) for h in (0, 1) for c in (0, 1)}
+        second = [ring2(h) for h in (0, 1)]
+
+        def part(h, c, place):
+            return gblk(UP, h, raxes(h)[0], place).at[:, pl.ds(c * wing, wing)]
+
+        def second_start(w, h, c=None):
+            if w == DN:
+                for c in (0, 1):
+                    first[w, h, c].last_in()
+                second[h].far()
+                second[h].near_right()
+                second[h].near_left()
+                return
+            first[w, h, c].last_in()
+            _, b, _, bdev = raxes(h)
+            for d in (2, 1, 3):
+                encode([part(h, c, at(b, d))], d2s.at[h, c, d - 1])
+                send(("d2", h, c), d2s.at[h, c, d - 1], d2r.at[h, c, d - 1], bdev(d), ("d2", h, c))
+
+        def third_start(w, h, c=None):
             a, b, _, _ = raxes(h)
-            encode(gblk(w, h, a, b), s3s.at[w, h])
             peers_ = [(0, rpeer)] if h == 0 else [(1, zpeer), (2, rzpeer)]
+            if w == DN:
+                second[h].near_in()
+                second[h].last_in()
+                encode([gblk(w, h, a, b)], s3s.at[h])
+                for i, dev in peers_:
+                    send((5, w), s3s.at[h], s3r.at[i], dev, (5, w))
+                return
+            recv(("d2", h, c), d2r.at[h, c])
+            for d in range(3):
+                add([part(h, c, b)], d2r.at[h, c, d])
+            encode([part(h, c, b)], u3s.at[c, h])
             for i, dev in peers_:
-                send((5, w), s3s.at[w, h], s3r.at[w, i], dev, (5, w))
-
-        def finish(w):
-            out = (gup_ref, gdn_ref)[w]
-            recv((5, w), s3r.at[w])
-            for side, one, two in ((j, s3s.at[w, 0], s3r.at[w, 0]), (1 - j, s3r.at[w, 1], s3r.at[w, 2])):
-                every, tile1 = decoder(one, width // 32)
-                _, tile2 = decoder(two, width // 32)
-                for n, q, c in every:
-                    col = pl.ds(pl.multiple_of(side * cols + n // (width // 512) * 128, 128), 128)
+                send((5, w, c), u3s.at[c, h], u3r.at[c, i], dev, (5, w, c))
+
+        def finish(w, c=None):
+            if w == DN:
+                out, mine, theirs, at_, wide = gdn_ref, s3s, s3r, 0, cols
+                recv((5, w), s3r)
+            else:
+                out, mine, theirs, at_, wide = gup_ref, u3s.at[c], u3r.at[c], c * wing, wing
+                recv((5, w, c), u3r.at[c])
+            for side, one, two in ((j, mine.at[0], theirs.at[0]), (1 - j, theirs.at[1], theirs.at[2])):
+                like = [out.at[:, pl.ds(0, wide)]]
+                every, tile1 = decoder(one, like)
+                _, tile2 = decoder(two, like)
+                for n, _, q, _ in every:
+                    col = pl.ds(pl.multiple_of(side * cols + at_ + n // (width // 512) * 128, 128), 128)
                     out[q, col] = (tile1(n) + tile2(n)) * factor
 
         def input_part(n):
@@ -367,14 +393,14 @@
         def input_send():
             recv(("g", "t", 0), DR.at[0])
             PART[2] = PART[2] + DR[0]
-            encode(PART.at[2], ZS, 4)
+            encode([PART.at[2]], ZS, 4)
             send("gz", ZS, ZR, zpeer, "gz")
 
         def input_sum():
             recv(("g", "t", 1), DR.at[1])
             recv("gz", ZR)
-            every, tile = decoder(ZR, tokens, 4)
-            for n, q, c in every:
+            every, tile = decoder(ZR, [PART.at[2]], 4)
+            for n, _, q, c in every:
                 gin_ref[q, c] = (PART[0, q, c] + DR[1, q, c] + tile(n)).astype(BF)
 
         def energy_x():
@@ -422,13 +448,13 @@
         todo = {
             "init": init, "near": near, "step2": step2, "fwd": fwd, "pass": pass_on, "turn": turn,
             "proj": project, "pull": pull_back, "mult": multiply, "ma": multiply_early,
-            "far": lambda w, h, lo: first[w, h].far(lo),
-            "nr": lambda w, h: first[w, h].near_right(),
-            "nl": lambda w, h: first[w, h].near_left(),
-            "rl": lambda w, h, side, lo: first[w, h].relay(side, lo),
-            "ni": lambda w, h: first[w, h].near_in(),
+            "far": lambda w, h, c: first[w, h, c].far(),
+            "nr": lambda w, h, c: first[w, h, c].near_right(),
+            "nl": lambda w, h, c: first[w, h, c].near_left(),
+            "rl": lambda w, h, side, c: first[w, h, c].relay(side),
+            "ni": lambda w, h, c: first[w, h, c].near_in(),
             "st2": second_start,
-            "rl2": lambda w, h, side: second[w, h].relay(side),
+            "rl2": lambda w, h, side: second[h].relay(side),
             "st3": third_start, "fin": finish, "ip": input_part, "gz": input_send, "gin": input_sum,
             "ex": energy_x, "ey": energy_y, "edn": energy_down,
             "eu": energy_pair, "eup": energy_up,
@@ -441,9 +467,15 @@
             sent((name, "zt"), X.at[0])
             for h in (0, 1):
                 sent((n, h), RP.at[0, pl.ds(0, 15 * tokens // 16)])
-                sent((1, n, h), s1s.at[0])
-                sent((2, n, h), s2s.at[0])
-            sent((5, n), s3r.at[0])
+                for c in (0, 1):
+                    sent((1, n, h, c), s1s.at[0, 0])
+                    if n == UP:
+                        sent(("d2", h, c), d2s.at[0, 0])
+                if n == DN:
+                    sent((2, n, h), s2s.at[0])
+        sent((5, DN), s3r)
+        for c in (0, 1):
+            sent((5, UP, c), u3r.at[0])
         sent("gt", PART.at[pl.ds(0, 2)])
         sent("gz", ZS)
         sent("ex", EX.at[pl.ds(0, 3)])
@@ -503,12 +535,16 @@
             pltpu.VMEM((4, tokens, cols), BF),
             pltpu.VMEM((4, tokens, cols), BF),
             pltpu.VMEM((2,) + full + (cols,), F32),
-            pltpu.VMEM((4, 6, 2, lines + 1, 16, 128), BF),
-            pltpu.VMEM((4, 6, 2, lines + 1, 16, 128), BF),
-            pltpu.VMEM((4, 6, 1, lines // 2 + 1, 16, 128), BF),
-            pltpu.VMEM((4, 6, 1, lines // 2 + 1, 16, 128), BF),
-            pltpu.VMEM((2, 2, lines + 1, 16, 128), BF),
-            pltpu.VMEM((2, 3, lines + 1, 16, 128), BF),
+            pltpu.VMEM((4, 2, 6, lines + 1, 16, 128), BF),
+            pltpu.VMEM((4, 2, 6, lines + 1, 16, 128), BF),
+            pltpu.VMEM((2, 6, lines // 2 + 1, 16, 128), BF),
+            pltpu.VMEM((2, 6, lines // 2 + 1, 16, 128), BF),
+            pltpu.VMEM((2, 2, 3, lines // 2 + 1, 16, 128), BF),
+            pltpu.VMEM((2, 2, 3, lines // 2 + 1, 16, 128), BF),
+            pltpu.VMEM((2, lines + 1, 16, 128), BF),
+            pltpu.VMEM((3, lines + 1, 16, 128), BF),
+            pltpu.VMEM((2, 2, lines // 2 + 1, 16, 128), BF),
+            pltpu.VMEM((2, 3, lines // 2 + 1, 16, 128), BF),
             pltpu.VMEM((4, tokens, width), F32),
             pltpu.VMEM((2, tokens, width), F32),
             pltpu.VMEM((tokens * width // 2048 + 1, 16, 128), BF),

time: 75.9 us -> 75.7 us (level)
  no operation moved by 1% of the time
where the time goes in v7:
time: 75.7 us; the launch traced here: 75.6 us
  Pallas kernels  74.8 us (99%)
  between operations  0.8 us (1%)
    pallas_call x1, Pallas kernels, per_device(): pl.pallas_call(make_kernel(tokens, width, cols, ff, factor), out_shape=(p...  73.7 us

profile of v7, /device:TPU:1, one launch (start us, length us, event | category | flops | bytes accessed | tf_op | source)
XLA Modules:
  0.0 75.6 jit_solution(2081214411241320188)
XLA Ops:
  0.6 73.7 %shard_map.83 = (bf16[256,1024]{1,0:T(8,128)(2,1)S(1)}, f32[32,2048]{1,0:T(8,128)S(1)}, f32[32,2048]{1,0:T(8,128)S(1)}, f32[1,32]{1,0:T(1,128)S(1)}, f32[1,2048]{1,0:T(1,128)S(1)}) custom-call(bf16[256,1024]{1,0:T(8,128)(2,1)} %x_ref.1, bf16[2,16,2048]{2,1,0:T(8,128)(2,1)} %bitcast.7, bf16[2,16,2048]{2,1,0:T(8,128)(2,1)} %bitcast.8, bf16[256,1024]{1,0:T(8,128)(2,1)} %cot_ref.1), custom_call_target="tpu_custom_call" | custom-call | tf_op jit(solution)/shard_map/pallas_call | solution.py:517
  74.4 1.0 %shard_map.84 = (bf16[256,1024]{1,0:T(8,128)(2,1)}, f32[32,2048]{1,0:T(8,128)}, f32[32,2048]{1,0:T(8,128)}, f32[1,32]{1,0:T(1,128)}, f32[1,2048]{1,0:T(1,128)}) custom-call(bf16[256,1024]{1,0:T(8,128)(2,1)S(1)} %get-tuple-element.15.refs_0_, f32[32,2048]{1,0:T(8,128)S(1)} %get-tuple-element.16.refs_1_, f32[32,2048]{1,0:T(8,128)S(1)} %get-tuple-element.17.refs_2_, ...), custom_call_target="tpu_custom_call" | custom-call | tf_op jit(solution)/shard_map/pallas_call | solution.py:500

commit v8 on v7

--- a/solution.py
+++ b/solution.py
@@ -17,32 +17,31 @@
 
 
 ORDER = [
-    ("init", 1, 0), ("init", 0, 0), ("init", 0, 1), ("init", 1, 1), ("near", 0, 0, 0), ("near", 0, 0, 1),
-    ("near", 0, 1, 0), ("near", 0, 1, 1), ("near", 1, 0, 1), ("near", 1, 0, 0), ("near", 1, 1, 0),
-    ("step2", 0, 1), ("fwd", 1, 0, 0, 1), ("step2", 0, 0), ("turn", "c", 0), ("fwd", 0, 0, 0, 1),
-    ("near", 1, 1, 1), ("fwd", 0, 1, 1, 1), ("fwd", 0, 1, 1, 0), ("pass", "x", 0), ("fwd", 0, 1, 2, 1),
-    ("fwd", 0, 1, 0, 1), ("fwd", 0, 0, 1, 1), ("fwd", 1, 0, 2, 0), ("fwd", 0, 0, 1, 0), ("pass", "x", 1),
-    ("turn", "x", 0), ("fwd", 0, 0, 2, 0), ("turn", "x", 1), ("turn", "c", 1), ("fwd", 0, 1, 2, 0),
-    ("fwd", 0, 0, 2, 1), ("turn", "x", 3), ("fwd", 0, 1, 0, 0), ("step2", 1, 0), ("fwd", 0, 0, 3, 0),
-    ("fwd", 1, 1, 0, 1), ("fwd", 0, 1, 3, 0), ("turn", "x", 2), ("fwd", 0, 1, 3, 1), ("fwd", 1, 1, 2, 0),
-    ("fwd", 0, 0, 3, 1), ("pass", "c", 0), ("fwd", 1, 0, 2, 1), ("fwd", 1, 0, 1, 1), ("step2", 1, 1),
-    ("fwd", 1, 1, 1, 0), ("fwd", 0, 0, 0, 0), ("proj", 0), ("fwd", 1, 1, 3, 0), ("fwd", 1, 0, 3, 1),
-    ("fwd", 1, 1, 0, 0), ("ma", 1, 0), ("fwd", 1, 1, 3, 1), ("fwd", 1, 1, 1, 1), ("fwd", 1, 0, 3, 0),
-    ("pass", "c", 1), ("fwd", 1, 0, 1, 0), ("fwd", 1, 0, 0, 0), ("fwd", 1, 1, 2, 1), ("turn", "c", 2),
-    ("ma", 1, 1), ("proj", 1), ("turn", "c", 3), ("mult", 1, 1), ("far", 1, 1, 0), ("mult", 1, 0),
-    ("far", 1, 0, 0), ("far", 1, 1, 1), ("pull", 1), ("pull", 0), ("nr", 1, 1, 0), ("nr", 1, 0, 1),
-    ("nl", 1, 0, 1), ("ip", 0), ("far", 1, 0, 1), ("nl", 1, 1, 1), ("mult", 0, 1), ("nl", 0, 1, 1),
-    ("nr", 1, 1, 1), ("rl", 1, 0, 0, 0), ("nl", 1, 0, 0), ("nr", 1, 0, 0), ("far", 0, 1, 0), ("rl", 1, 0, 1, 0),
-    ("rl", 1, 1, 0, 0), ("rl", 1, 1, 0, 1), ("mult", 0, 0), ("ip", 1), ("nl", 1, 1, 0), ("rl", 1, 0, 1, 1),
-    ("rl", 1, 0, 0, 1), ("rl", 1, 1, 1, 1), ("nr", 0, 1, 1), ("gz",), ("nl", 0, 0, 0), ("far", 0, 0, 1),
-    ("nl", 0, 0, 1), ("rl", 1, 1, 1, 0), ("nr", 0, 0, 0), ("ni", 1, 0, 1), ("ni", 1, 0, 0), ("st2", 1, 0),
-    ("nr", 0, 0, 1), ("ni", 1, 1, 1), ("far", 0, 1, 1), ("nr", 0, 1, 0), ("rl", 0, 1, 1, 0), ("ni", 1, 1, 0),
-    ("far", 0, 0, 0), ("ni", 0, 0, 0), ("st2", 1, 1), ("rl", 0, 0, 1, 1), ("rl", 0, 0, 0, 1), ("rl2", 1, 0, 0),
-    ("rl", 0, 1, 0, 0), ("rl2", 1, 0, 1), ("rl", 0, 1, 0, 1), ("rl2", 1, 1, 1), ("nl", 0, 1, 0), ("ni", 0, 0, 1),
-    ("rl2", 1, 1, 0), ("ni", 0, 1, 1), ("rl", 0, 0, 1, 0), ("rl", 0, 0, 0, 0), ("st3", 1, 0), ("rl", 0, 1, 1, 1),
-    ("st2", 0, 0, 1), ("ni", 0, 1, 0), ("st3", 1, 1), ("st2", 0, 1, 0), ("st2", 0, 1, 1), ("st2", 0, 0, 0),
-    ("st3", 0, 0, 1), ("fin", 1), ("ex",), ("gin",), ("st3", 0, 1, 0), ("st3", 0, 0, 0), ("st3", 0, 1, 1),
-    ("ey",), ("fin", 0, 0), ("fin", 0, 1), ("eu",), ("eup",), ("edn",),
+    ("init", 1, 0), ("init", 0, 0), ("init", 0, 1), ("init", 1, 1), ("turn", "c", 0), ("near", 0, 0, 1),
+    ("near", 0, 0, 0), ("near", 0, 1, 1), ("near", 0, 1, 0), ("fwd", 0, 0, 2, 1), ("near", 1, 1, 1),
+    ("near", 1, 1, 0), ("step2", 0, 0), ("near", 1, 0, 0), ("step2", 0, 1), ("pass", "x", 0), ("turn", "x", 1),
+    ("fwd", 0, 0, 1, 0), ("near", 1, 0, 1), ("fwd", 0, 1, 2, 1), ("pass", "x", 1), ("fwd", 0, 0, 2, 0),
+    ("fwd", 0, 0, 1, 1), ("fwd", 1, 1, 2, 0), ("fwd", 0, 1, 0, 1), ("fwd", 0, 1, 0, 0), ("fwd", 0, 1, 2, 0),
+    ("fwd", 1, 1, 0, 1), ("fwd", 0, 0, 3, 0), ("fwd", 0, 1, 3, 1), ("turn", "x", 3), ("fwd", 0, 1, 1, 1),
+    ("fwd", 0, 1, 3, 0), ("fwd", 0, 0, 0, 1), ("fwd", 1, 1, 2, 1), ("fwd", 0, 0, 0, 0), ("turn", "c", 1),
+    ("fwd", 0, 0, 3, 1), ("fwd", 0, 1, 1, 0), ("turn", "x", 0), ("fwd", 1, 1, 1, 0), ("pass", "c", 0),
+    ("turn", "x", 2), ("fwd", 1, 0, 2, 0), ("fwd", 1, 0, 0, 1), ("step2", 1, 1), ("step2", 1, 0), ("proj", 0),
+    ("ma", 1, 1), ("fwd", 1, 1, 0, 0), ("ma", 1, 0), ("fwd", 1, 0, 1, 1), ("pass", "c", 1), ("fwd", 1, 0, 0, 0),
+    ("fwd", 1, 1, 3, 1), ("fwd", 1, 0, 3, 1), ("fwd", 1, 0, 2, 1), ("fwd", 1, 0, 3, 0), ("proj", 1),
+    ("fwd", 1, 1, 3, 0), ("fwd", 1, 0, 1, 0), ("fwd", 1, 1, 1, 1), ("turn", "c", 2), ("turn", "c", 3),
+    ("mult", 1, 0), ("nr", 1, 0, 0), ("far", 1, 0, 0), ("mult", 1, 1), ("far", 1, 1, 1), ("far", 1, 0, 1),
+    ("far", 1, 1, 0), ("nr", 1, 1, 1), ("pull", 1), ("nl", 1, 0, 1), ("pull", 0), ("ip", 0), ("nr", 1, 0, 1),
+    ("nl", 1, 0, 0), ("nl", 1, 1, 0), ("rl", 1, 0, 1, 1), ("nl", 1, 1, 1), ("nr", 1, 1, 0), ("rl", 1, 0, 0, 0),
+    ("mult", 0, 0), ("rl", 1, 0, 1, 0), ("rl", 1, 1, 0, 1), ("rl", 1, 1, 1, 1), ("rl", 1, 0, 0, 1), ("ip", 1),
+    ("gz",), ("rl", 1, 1, 0, 0), ("rl", 1, 1, 1, 0), ("far", 0, 0, 0), ("mult", 0, 1), ("far", 0, 1, 0),
+    ("ni", 1, 0, 0), ("far", 0, 0, 1), ("nr", 0, 0, 0), ("ni", 1, 0, 1), ("st2", 1, 0), ("nl", 0, 0, 0),
+    ("far", 0, 1, 1), ("ni", 1, 1, 0), ("ni", 1, 1, 1), ("st2", 1, 1), ("rl", 0, 1, 0, 0), ("rl2", 1, 0, 1),
+    ("rl2", 1, 0, 0), ("nl", 0, 1, 0), ("rl", 0, 1, 1, 0), ("nr", 0, 1, 0), ("rl", 0, 0, 1, 0), ("nr", 0, 1, 1),
+    ("rl", 0, 0, 0, 0), ("rl2", 1, 1, 0), ("rl2", 1, 1, 1), ("rl", 0, 0, 1, 1), ("nl", 0, 1, 1), ("nr", 0, 0, 1),
+    ("rl", 0, 0, 0, 1), ("nl", 0, 0, 1), ("ni", 0, 0, 0), ("rl", 0, 1, 1, 1), ("rl", 0, 1, 0, 1), ("st3", 1, 0),
+    ("st3", 1, 1), ("st2", 0, 0, 0), ("ni", 0, 1, 0), ("st2", 0, 1, 0), ("ni", 0, 0, 1), ("ni", 0, 1, 1),
+    ("st2", 0, 0, 1), ("st2", 0, 1, 1), ("gin",), ("fin", 1), ("ex",), ("st3", 0, 0, 0), ("st3", 0, 1, 0),
+    ("st3", 0, 0, 1), ("ey",), ("st3", 0, 1, 1), ("fin", 0, 0), ("fin", 0, 1), ("eu",), ("eup",), ("edn",),
 ]
 
 

time: 75.7 us -> 74.4 us (0.983)
  Pallas kernels: 74.8 us -> 73.5 us
    pallas_call x1, Pallas kernels: 73.7 us -> 72.4 us  [per_device(): pl.pallas_call(make_kernel(tokens, width, cols, ff, factor), out_shape=(p...]
where the time goes in v8:
time: 74.4 us; the launch traced here: 74.3 us
  Pallas kernels  73.5 us (99%)
  between operations  0.8 us (1%)
    pallas_call x1, Pallas kernels, per_device(): pl.pallas_call(make_kernel(tokens, width, cols, ff, factor), out_shape=(p...  72.4 us

profile of v8, /device:TPU:1, one launch (start us, length us, event | category | flops | bytes accessed | tf_op | source)
XLA Modules:
  0.0 74.3 jit_solution(5100704556698828870)
XLA Ops:
  0.6 72.4 %shard_map.83 = (bf16[256,1024]{1,0:T(8,128)(2,1)S(1)}, f32[32,2048]{1,0:T(8,128)S(1)}, f32[32,2048]{1,0:T(8,128)S(1)}, f32[1,32]{1,0:T(1,128)S(1)}, f32[1,2048]{1,0:T(1,128)S(1)}) custom-call(bf16[256,1024]{1,0:T(8,128)(2,1)} %x_ref.1, bf16[2,16,2048]{2,1,0:T(8,128)(2,1)} %bitcast.7, bf16[2,16,2048]{2,1,0:T(8,128)(2,1)} %bitcast.8, bf16[256,1024]{1,0:T(8,128)(2,1)} %cot_ref.1), custom_call_target="tpu_custom_call" | custom-call | tf_op jit(solution)/shard_map/pallas_call | solution.py:516
  73.1 1.0 %shard_map.84 = (bf16[256,1024]{1,0:T(8,128)(2,1)}, f32[32,2048]{1,0:T(8,128)}, f32[32,2048]{1,0:T(8,128)}, f32[1,32]{1,0:T(1,128)}, f32[1,2048]{1,0:T(1,128)}) custom-call(bf16[256,1024]{1,0:T(8,128)(2,1)S(1)} %get-tuple-element.15.refs_0_, f32[32,2048]{1,0:T(8,128)S(1)} %get-tuple-element.16.refs_1_, f32[32,2048]{1,0:T(8,128)S(1)} %get-tuple-element.17.refs_2_, ...), custom_call_target="tpu_custom_call" | custom-call | tf_op jit(solution)/shard_map/pallas_call | solution.py:499

commit v9 on v8

--- a/solution.py
+++ b/solution.py
@@ -13,7 +13,7 @@
 F32 = jnp.float32
 RIGHT, LEFT = 0, 1
 UP, DN = 0, 1
-WAITS, BATCHES = 118, 32
+WAITS, BATCHES = 109, 14
 
 
 ORDER = [
@@ -130,22 +130,22 @@
             ref = blk(W, w, h, a, b)
             if h == 1:
                 recv(("a2a", w), ref)
-            send((1, w, h, 0), ref, ref, adev(1), (w, h))
-            send((1, w, h, 1), ref, ref, adev(3), (w, h))
+            send((1, w, h, 0), ref, ref, adev(1), "w")
+            send((1, w, h, 1), ref, ref, adev(3), "w")
             spread(w, h, 0, a)
 
         def spread(w, h, s, a2):
             _, b, _, bdev = axes(h)
             ref = blk(W, w, h, a2, b)
-            send((2, w, h, s, 0), ref, ref, bdev(1), (w, h))
-            send((2, w, h, s, 1), ref, ref, bdev(3), (w, h))
+            send((2, w, h, s, 0), ref, ref, bdev(1), "w")
+            send((2, w, h, s, 1), ref, ref, bdev(3), "w")
 
         def near(w, h, side):
             a, b, adev, _ = axes(h)
             place, away = ((at(a, 3), 1), (at(a, 1), 3))[side]
             ref = blk(W, w, h, place, b)
             recv((1, w, h, side), ref)
-            send((1, w, h, 2), ref.at[side], ref.at[side], adev(away), (w, h))
+            send((1, w, h, 2), ref.at[side], ref.at[side], adev(away), "w")
             spread(w, h, 1 + side, place)
 
         def step2(w, h):
@@ -159,7 +159,7 @@
             place, away = ((at(b, 3), 1), (at(b, 1), 3))[side]
             ref = blk(W, w, h, a2, place)
             recv((2, w, h, s, side), ref)
-            send((3, w), ref.at[side], ref.at[side], bdev(away), (w, h))
+            send((3, w), ref.at[side], ref.at[side], bdev(away), "w")
 
         whole = set()
 
@@ -174,7 +174,7 @@
             rows = pl.ds(i * half, half)
             buf = stock[name][0]
             recv((name, "z", i), buf.at[2, rows])
-            send((name, "zt"), buf.at[2, rows], buf.at[3, rows], tpeer, (name, "zt"))
+            send((name, "zt"), buf.at[2, rows], buf.at[3, rows], tpeer, "zt")
 
         def turn(name, slot):
             src, dst = stock[name]
@@ -284,7 +284,7 @@
 
             def post(self, i, place, side, d, group):
                 encode(self.parts(place, side), self.sb.at[i])
-                send(self.k + group, self.sb.at[i], self.rb.at[i], self.dev(d), self.k)
+                send(self.k + group, self.sb.at[i], self.rb.at[i], self.dev(d), self.k[0])
 
             def far(self):
                 self.post(0, at(self.pos, 2), 0, 1, ("far", 0))
@@ -345,7 +345,7 @@
             _, b, _, bdev = raxes(h)
             for d in (2, 1, 3):
                 encode([part(h, c, at(b, d))], d2s.at[h, c, d - 1])
-                send(("d2", h, c), d2s.at[h, c, d - 1], d2r.at[h, c, d - 1], bdev(d), ("d2", h, c))
+                send(("d2", h, c), d2s.at[h, c, d - 1], d2r.at[h, c, d - 1], bdev(d), "d2")
 
         def third_start(w, h, c=None):
             a, b, _, _ = raxes(h)
@@ -355,14 +355,14 @@
                 second[h].last_in()
                 encode([gblk(w, h, a, b)], s3s.at[h])
                 for i, dev in peers_:
-                    send((5, w), s3s.at[h], s3r.at[i], dev, (5, w))
+                    send((5, w), s3s.at[h], s3r.at[i], dev, "d3")
                 return
             recv(("d2", h, c), d2r.at[h, c])
             for d in range(3):
                 add([part(h, c, b)], d2r.at[h, c, d])
             encode([part(h, c, b)], u3s.at[c, h])
             for i, dev in peers_:
-                send((5, w, c), u3s.at[c, h], u3r.at[c, i], dev, (5, w, c))
+                send((5, w, c), u3s.at[c, h], u3r.at[c, i], dev, "u3")
 
         def finish(w, c=None):
             if w == DN:
@@ -442,8 +442,8 @@
             buf = stock[name][0]
             for i in (0, 1):
                 rows = pl.ds(i * half, half)
-                send((name, "z", i), buf.at[0, rows], buf.at[2, rows], zpeer, name)
-            send((name, "t"), buf.at[0], buf.at[1], tpeer, name)
+                send((name, "z", i), buf.at[0, rows], buf.at[2, rows], zpeer, "own")
+            send((name, "t"), buf.at[0], buf.at[1], tpeer, "own")
         todo = {
             "init": init, "near": near, "step2": step2, "fwd": fwd, "pass": pass_on, "turn": turn,
             "proj": project, "pull": pull_back, "mult": multiply, "ma": multiply_early,
@@ -460,21 +460,12 @@
         }
         for name, *where in ORDER:
             todo[name](*where)
-        sent("a2a", OTH)
-        for n, name in enumerate(("x", "c")):
-            sent(name, RP.at[0])
-            sent((name, "zt"), X.at[0])
-            for h in (0, 1):
-                sent((n, h), RP.at[0, pl.ds(0, 15 * tokens // 16)])
-                for c in (0, 1):
-                    sent((1, n, h, c), s1s.at[0, 0])
-                    if n == UP:
-                        sent(("d2", h, c), d2s.at[0, 0])
-                if n == DN:
-                    sent((2, n, h), s2s.at[0])
-        sent((5, DN), s3r)
-        for c in (0, 1):
-            sent((5, UP, c), u3r.at[0])
+        for batch, ref in (
+            ("a2a", OTH), ("own", RP.at[pl.ds(0, 2)]), ("zt", X.at[pl.ds(0, 2)]),
+            ("w", RP.at[:, pl.ds(0, 15 * tokens // 16)]),
+            (1, s1s), (2, s2s), ("d2", d2s), ("d3", s3r), ("u3", u3r),
+        ):
+            sent(batch, ref)
         sent("gt", PART.at[pl.ds(0, 2)])
         sent("gz", ZS)
         sent("ex", EX.at[pl.ds(0, 3)])

time: 74.4 us -> 74.1 us (level)
  no operation moved by 1% of the time
where the time goes in v9:
time: 74.1 us; the launch traced here: 74 us
  Pallas kernels  73.2 us (99%)
  between operations  0.8 us (1%)
    pallas_call x1, Pallas kernels, per_device(): pl.pallas_call(make_kernel(tokens, width, cols, ff, factor), out_shape=(p...  72.2 us

profile of v9, /device:TPU:1, one launch (start us, length us, event | category | flops | bytes accessed | tf_op | source)
XLA Modules:
  0.0 74.0 jit_solution(16239321914693988796)
XLA Ops:
  0.6 72.2 %shard_map.83 = (bf16[256,1024]{1,0:T(8,128)(2,1)S(1)}, f32[32,2048]{1,0:T(8,128)S(1)}, f32[32,2048]{1,0:T(8,128)S(1)}, f32[1,32]{1,0:T(1,128)S(1)}, f32[1,2048]{1,0:T(1,128)S(1)}) custom-call(bf16[256,1024]{1,0:T(8,128)(2,1)} %x_ref.1, bf16[2,16,2048]{2,1,0:T(8,128)(2,1)} %bitcast.7, bf16[2,16,2048]{2,1,0:T(8,128)(2,1)} %bitcast.8, bf16[256,1024]{1,0:T(8,128)(2,1)} %cot_ref.1), custom_call_target="tpu_custom_call" | custom-call | tf_op jit(solution)/shard_map/pallas_call | solution.py:507
  72.8 1.0 %shard_map.84 = (bf16[256,1024]{1,0:T(8,128)(2,1)}, f32[32,2048]{1,0:T(8,128)}, f32[32,2048]{1,0:T(8,128)}, f32[1,32]{1,0:T(1,128)}, f32[1,2048]{1,0:T(1,128)}) custom-call(bf16[256,1024]{1,0:T(8,128)(2,1)S(1)} %get-tuple-element.15.refs_0_, f32[32,2048]{1,0:T(8,128)S(1)} %get-tuple-element.16.refs_1_, f32[32,2048]{1,0:T(8,128)S(1)} %get-tuple-element.17.refs_2_, ...), custom_call_target="tpu_custom_call" | custom-call | tf_op jit(solution)/shard_map/pallas_call | solution.py:490

commit v10 on v9

--- a/solution.py
+++ b/solution.py
@@ -17,31 +17,32 @@
 
 
 ORDER = [
-    ("init", 1, 0), ("init", 0, 0), ("init", 0, 1), ("init", 1, 1), ("turn", "c", 0), ("near", 0, 0, 1),
-    ("near", 0, 0, 0), ("near", 0, 1, 1), ("near", 0, 1, 0), ("fwd", 0, 0, 2, 1), ("near", 1, 1, 1),
-    ("near", 1, 1, 0), ("step2", 0, 0), ("near", 1, 0, 0), ("step2", 0, 1), ("pass", "x", 0), ("turn", "x", 1),
-    ("fwd", 0, 0, 1, 0), ("near", 1, 0, 1), ("fwd", 0, 1, 2, 1), ("pass", "x", 1), ("fwd", 0, 0, 2, 0),
-    ("fwd", 0, 0, 1, 1), ("fwd", 1, 1, 2, 0), ("fwd", 0, 1, 0, 1), ("fwd", 0, 1, 0, 0), ("fwd", 0, 1, 2, 0),
-    ("fwd", 1, 1, 0, 1), ("fwd", 0, 0, 3, 0), ("fwd", 0, 1, 3, 1), ("turn", "x", 3), ("fwd", 0, 1, 1, 1),
-    ("fwd", 0, 1, 3, 0), ("fwd", 0, 0, 0, 1), ("fwd", 1, 1, 2, 1), ("fwd", 0, 0, 0, 0), ("turn", "c", 1),
-    ("fwd", 0, 0, 3, 1), ("fwd", 0, 1, 1, 0), ("turn", "x", 0), ("fwd", 1, 1, 1, 0), ("pass", "c", 0),
-    ("turn", "x", 2), ("fwd", 1, 0, 2, 0), ("fwd", 1, 0, 0, 1), ("step2", 1, 1), ("step2", 1, 0), ("proj", 0),
-    ("ma", 1, 1), ("fwd", 1, 1, 0, 0), ("ma", 1, 0), ("fwd", 1, 0, 1, 1), ("pass", "c", 1), ("fwd", 1, 0, 0, 0),
-    ("fwd", 1, 1, 3, 1), ("fwd", 1, 0, 3, 1), ("fwd", 1, 0, 2, 1), ("fwd", 1, 0, 3, 0), ("proj", 1),
-    ("fwd", 1, 1, 3, 0), ("fwd", 1, 0, 1, 0), ("fwd", 1, 1, 1, 1), ("turn", "c", 2), ("turn", "c", 3),
-    ("mult", 1, 0), ("nr", 1, 0, 0), ("far", 1, 0, 0), ("mult", 1, 1), ("far", 1, 1, 1), ("far", 1, 0, 1),
-    ("far", 1, 1, 0), ("nr", 1, 1, 1), ("pull", 1), ("nl", 1, 0, 1), ("pull", 0), ("ip", 0), ("nr", 1, 0, 1),
-    ("nl", 1, 0, 0), ("nl", 1, 1, 0), ("rl", 1, 0, 1, 1), ("nl", 1, 1, 1), ("nr", 1, 1, 0), ("rl", 1, 0, 0, 0),
-    ("mult", 0, 0), ("rl", 1, 0, 1, 0), ("rl", 1, 1, 0, 1), ("rl", 1, 1, 1, 1), ("rl", 1, 0, 0, 1), ("ip", 1),
-    ("gz",), ("rl", 1, 1, 0, 0), ("rl", 1, 1, 1, 0), ("far", 0, 0, 0), ("mult", 0, 1), ("far", 0, 1, 0),
-    ("ni", 1, 0, 0), ("far", 0, 0, 1), ("nr", 0, 0, 0), ("ni", 1, 0, 1), ("st2", 1, 0), ("nl", 0, 0, 0),
-    ("far", 0, 1, 1), ("ni", 1, 1, 0), ("ni", 1, 1, 1), ("st2", 1, 1), ("rl", 0, 1, 0, 0), ("rl2", 1, 0, 1),
-    ("rl2", 1, 0, 0), ("nl", 0, 1, 0), ("rl", 0, 1, 1, 0), ("nr", 0, 1, 0), ("rl", 0, 0, 1, 0), ("nr", 0, 1, 1),
-    ("rl", 0, 0, 0, 0), ("rl2", 1, 1, 0), ("rl2", 1, 1, 1), ("rl", 0, 0, 1, 1), ("nl", 0, 1, 1), ("nr", 0, 0, 1),
-    ("rl", 0, 0, 0, 1), ("nl", 0, 0, 1), ("ni", 0, 0, 0), ("rl", 0, 1, 1, 1), ("rl", 0, 1, 0, 1), ("st3", 1, 0),
-    ("st3", 1, 1), ("st2", 0, 0, 0), ("ni", 0, 1, 0), ("st2", 0, 1, 0), ("ni", 0, 0, 1), ("ni", 0, 1, 1),
-    ("st2", 0, 0, 1), ("st2", 0, 1, 1), ("gin",), ("fin", 1), ("ex",), ("st3", 0, 0, 0), ("st3", 0, 1, 0),
-    ("st3", 0, 0, 1), ("ey",), ("st3", 0, 1, 1), ("fin", 0, 0), ("fin", 0, 1), ("eu",), ("eup",), ("edn",),
+    ("init", 0, 0), ("init", 1, 0), ("init", 0, 1), ("init", 1, 1), ("near", 0, 0, 1), ("near", 0, 0, 0),
+    ("near", 0, 1, 0), ("near", 0, 1, 1), ("turn", "c", 1), ("step2", 0, 0), ("fwd", 0, 0, 2, 1),
+    ("near", 1, 1, 1), ("near", 1, 0, 1), ("near", 1, 1, 0), ("step2", 0, 1), ("fwd", 0, 0, 2, 0),
+    ("fwd", 0, 1, 2, 0), ("fwd", 1, 1, 2, 0), ("near", 1, 0, 0), ("pass", "x", 0), ("fwd", 0, 1, 2, 1),
+    ("fwd", 0, 0, 0, 1), ("fwd", 0, 1, 0, 1), ("fwd", 1, 0, 0, 0), ("fwd", 1, 1, 0, 0), ("turn", "x", 1),
+    ("pass", "x", 1), ("fwd", 1, 1, 1, 1), ("fwd", 0, 1, 0, 0), ("fwd", 0, 0, 1, 0), ("fwd", 0, 1, 3, 0),
+    ("fwd", 0, 0, 3, 0), ("fwd", 1, 0, 2, 0), ("turn", "x", 0), ("fwd", 0, 0, 1, 1), ("fwd", 0, 1, 3, 1),
+    ("fwd", 0, 0, 3, 1), ("fwd", 0, 1, 1, 1), ("turn", "x", 3), ("turn", "c", 0), ("fwd", 0, 0, 0, 0),
+    ("fwd", 1, 0, 2, 1), ("fwd", 0, 1, 1, 0), ("fwd", 1, 1, 1, 0), ("step2", 1, 1), ("fwd", 1, 1, 2, 1),
+    ("turn", "x", 2), ("pass", "c", 0), ("step2", 1, 0), ("proj", 0), ("ma", 1, 1), ("fwd", 1, 1, 0, 1),
+    ("fwd", 1, 0, 3, 0), ("fwd", 1, 0, 3, 1), ("ma", 1, 0), ("pass", "c", 1), ("fwd", 1, 1, 3, 0),
+    ("fwd", 1, 0, 1, 0), ("turn", "c", 2), ("fwd", 1, 1, 3, 1), ("fwd", 1, 0, 1, 1), ("fwd", 1, 0, 0, 1),
+    ("proj", 1), ("turn", "c", 3), ("mult", 1, 0), ("far", 1, 0, 0), ("far", 1, 0, 1), ("mult", 1, 1),
+    ("nr", 1, 0, 0), ("far", 1, 1, 0), ("pull", 0), ("nr", 1, 1, 0), ("nl", 1, 0, 0), ("pull", 1),
+    ("far", 1, 1, 1), ("ip", 0), ("rl", 1, 0, 0, 0), ("nl", 1, 0, 1), ("nl", 1, 1, 0), ("nr", 1, 1, 1),
+    ("rl", 1, 1, 1, 0), ("rl", 1, 0, 1, 1), ("nr", 1, 0, 1), ("nl", 1, 1, 1), ("mult", 0, 0), ("rl", 1, 0, 1, 0),
+    ("rl", 1, 1, 0, 0), ("rl", 1, 0, 0, 1), ("ip", 1), ("gz",), ("rl", 1, 1, 0, 1), ("far", 0, 0, 1),
+    ("rl", 1, 1, 1, 1), ("mult", 0, 1), ("nr", 0, 1, 0), ("ni", 1, 0, 0), ("far", 0, 1, 0), ("ni", 1, 0, 1),
+    ("far", 0, 0, 0), ("ni", 1, 1, 0), ("ni", 1, 1, 1), ("nl", 0, 0, 0), ("nr", 0, 0, 0), ("st2", 1, 0),
+    ("st2", 1, 1), ("far", 0, 1, 1), ("rl", 0, 0, 1, 0), ("rl", 0, 0, 0, 0), ("rl2", 1, 0, 1), ("nl", 0, 1, 0),
+    ("rl", 0, 1, 1, 0), ("rl2", 1, 0, 0), ("rl", 0, 1, 0, 0), ("rl2", 1, 1, 1), ("nl", 0, 1, 1), ("rl2", 1, 1, 0),
+    ("nr", 0, 1, 1), ("nr", 0, 0, 1), ("rl", 0, 1, 1, 1), ("ni", 0, 0, 0), ("nl", 0, 0, 1), ("rl", 0, 0, 0, 1),
+    ("rl", 0, 1, 0, 1), ("rl", 0, 0, 1, 1), ("st2", 0, 0, 0), ("st3", 1, 0), ("st3", 1, 1), ("ni", 0, 1, 0),
+    ("ni", 0, 0, 1), ("st2", 0, 1, 0), ("ni", 0, 1, 1), ("st2", 0, 0, 1), ("st2", 0, 1, 1), ("fin", 1), ("ex",),
+    ("st3", 0, 1, 0), ("gin",), ("st3", 0, 0, 0), ("st3", 0, 0, 1), ("ey",), ("st3", 0, 1, 1), ("fin", 0, 0),
+    ("fin", 0, 1), ("eu",), ("eup",), ("edn",),
 ]
 
 

time: 74.1 us -> 74.1 us (level)
  no operation moved by 1% of the time
where the time goes in v10:
time: 74.1 us; the launch traced here: 74 us
  Pallas kernels  73.2 us (99%)
  between operations  0.8 us (1%)
    pallas_call x1, Pallas kernels, per_device(): pl.pallas_call(make_kernel(tokens, width, cols, ff, factor), out_shape=(p...  72.1 us

profile of v10, /device:TPU:1, one launch (start us, length us, event | category | flops | bytes accessed | tf_op | source)
XLA Modules:
  0.0 74.0 jit_solution(18030046566042395661)
XLA Ops:
  0.6 72.1 %shard_map.83 = (bf16[256,1024]{1,0:T(8,128)(2,1)S(1)}, f32[32,2048]{1,0:T(8,128)S(1)}, f32[32,2048]{1,0:T(8,128)S(1)}, f32[1,32]{1,0:T(1,128)S(1)}, f32[1,2048]{1,0:T(1,128)S(1)}) custom-call(bf16[256,1024]{1,0:T(8,128)(2,1)} %x_ref.1, bf16[2,16,2048]{2,1,0:T(8,128)(2,1)} %bitcast.7, bf16[2,16,2048]{2,1,0:T(8,128)(2,1)} %bitcast.8, bf16[256,1024]{1,0:T(8,128)(2,1)} %cot_ref.1), custom_call_target="tpu_custom_call" | custom-call | tf_op jit(solution)/shard_map/pallas_call | solution.py:508
  72.8 1.0 %shard_map.84 = (bf16[256,1024]{1,0:T(8,128)(2,1)}, f32[32,2048]{1,0:T(8,128)}, f32[32,2048]{1,0:T(8,128)}, f32[1,32]{1,0:T(1,128)}, f32[1,2048]{1,0:T(1,128)}) custom-call(bf16[256,1024]{1,0:T(8,128)(2,1)S(1)} %get-tuple-element.15.refs_0_, f32[32,2048]{1,0:T(8,128)S(1)} %get-tuple-element.16.refs_1_, f32[32,2048]{1,0:T(8,128)S(1)} %get-tuple-element.17.refs_2_, ...), custom_call_target="tpu_custom_call" | custom-call | tf_op jit(solution)/shard_map/pallas_call | solution.py:491
